TPU v7x, 32 devices: a whole 2x2x4 slice. The times are simulated.
32 devices in a mesh: grp: 2 (over x), fs: 4 (over z), tp: 4 (over y, core).
Axes of the slice: x: 2, y: 2, z: 4, core: 2. Of those that a mesh axis runs over, the one named last changes fastest.
Arguments:
- stream: bfloat16 [2048, 2048], P(('grp', 'fs'), 'tp'), parts along dimension 0, may hold values from -80 to 80
- mixed: bfloat16 [2048, 2048], P(('grp', 'fs'), 'tp'), parts along dimension 0, may hold values from -6 to 6
- out_weight: bfloat16 [2048, 2048], P('fs', 'tp'), may hold values from -0.125 to 0.125
- norm_gain: bfloat16 [2048], P('tp'), may hold values from 0.099609375 to 1.8984375
- up_weight: bfloat16 [2048, 8192], P('fs', 'tp'), may hold values from -0.125 to 0.125
- down_weight: bfloat16 [8192, 2048], P('tp', 'fs'), may hold values from -0.09375 to 0.09375
Outputs:
- result: bfloat16 [2048, 2048], P(('grp', 'fs'), 'tp'), parts along dimension 0
There are 2 independent parts, one for each index of `grp`. A program takes and returns all parts, laid end to end along the dimension named above; an argument that names none is the same for every part. Nothing has to cross between parts.
All inputs are finite; a program needn't handle non-finite values.
Results may differ from a plain program's by a relative error of at most 0.01.
Values may be sent and summed in bfloat16 or wider, within the bound.
No kernel may reach another device: no remote copies, remote signals or barrier semaphores. Data moves between devices by JAX's collectives and lax.ppermute only.
A program may use at most 64 MiB of HBM per device.

v0:
```python
import jax
import jax.numpy as jnp
from jax import lax
from jax.sharding import PartitionSpec as P

epsilon = 1e-06


def fold_product(left, portion):
    return jnp.dot(left, portion, preferred_element_type=jnp.float32)


def body(stream, mixed, out_weight, norm_gain, up_weight, down_weight):
    mixed_whole = lax.all_gather(mixed, "tp", axis=1, tiled=True)
    projected = fold_product(mixed_whole, lax.all_gather(out_weight, "fs", axis=0, tiled=True))
    resid = (stream.astype(jnp.float32) + projected).astype(jnp.bfloat16)
    widened = resid.astype(jnp.float32)
    resid_whole, gain_whole = (
        lax.all_gather(resid, "tp", axis=1, tiled=True),
        lax.all_gather(norm_gain, "tp", axis=0, tiled=True),
    )
    stream_wide = resid_whole.astype(jnp.float32)
    energy = jnp.mean(stream_wide * stream_wide, axis=1, keepdims=True)
    normed_whole = (
        stream_wide * lax.rsqrt(energy + epsilon) * gain_whole.astype(jnp.float32)
    ).astype(jnp.bfloat16)
    up_full = lax.all_gather(up_weight, "fs", axis=0, tiled=True)
    up_values = jnp.dot(normed_whole, up_full, preferred_element_type=jnp.float32)
    activated = jnp.square(jax.nn.relu(up_values)).astype(jnp.bfloat16)
    partials = jnp.dot(
        activated,
        lax.all_gather(down_weight, "fs", axis=1, tiled=True),
        preferred_element_type=jnp.float32,
    )
    branch = lax.psum_scatter(partials, "tp", scatter_dimension=1, tiled=True)
    return (widened + branch).astype(jnp.bfloat16)


def solution(mesh):
    placed = (
        P(("grp", "fs"), "tp"),
        P(("grp", "fs"), "tp"),
        P("fs", "tp"),
        P("tp"),
        P("fs", "tp"),
        P("tp", "fs"),
    )
    return jax.shard_map(
        body, mesh=mesh, in_specs=placed, out_specs=P(("grp", "fs"), "tp"), check_vma=False
    )
```

profile of v0, /device:TPU:0, one launch (start us, length us, event | category | flops | bytes accessed | tf_op | source)
XLA Modules:
  0.0 445.1 jit_solution(17761984811447888567)
XLA Ops:
  6.5 0.0 all-gather.7.cloned.1.call-start
  6.5 0.7 all-gather.7.cloned.1.call-update
  7.3 0.0 all-gather.9.cloned.1.call-start
  7.3 0.7 all-gather.9.cloned.1.call-update
  8.0 0.0 all-gather.11.cloned.1.call-start
  8.1 20.3 %all-gather.7.cloned.1.call-done = bf16[256,2048]{1,0:T(8,128)(2,1)} async-done(((bf16[256,512]{1,0:T(8,128)(2,1)}), bf16[256,2048]{1,0:T(8,128)(2,1)}) %all-gather.7.cloned.1.call-update) | async-done | bytes 1048592 | tf_op jit(solution)/shard_map/all_gather | solution.py:14
  28.4 47.3 %all-gather.9.cloned.1.call-done = bf16[2048,512]{1,0:T(8,128)(2,1)} async-done(((bf16[512,512]{1,0:T(8,128)(2,1)}), bf16[2048,512]{1,0:T(8,128)(2,1)}) %all-gather.9.cloned.1.call-update) | async-done | bytes 2097168 | tf_op jit(solution)/shard_map/all_gather | solution.py:15
  75.6 3.3 fusion.5
  78.9 0.0 all-gather.11.cloned.1.call-update
  78.9 0.0 copy-start.1
  78.9 0.0 all-gather.13.cloned.1.call-start
  79.0 0.5 all-gather.13.cloned.1.call-update
  79.5 0.0 all-gather.15.cloned.1.call-start
  79.6 0.5 all-gather.15.cloned.1.call-update
  80.1 0.0 reduce-scatter.2.cloned.1.call-start
  80.2 5.2 %all-gather = bf16[4,1,512]{2,1,0:T(2,128)(2,1)S(1)} all-gather(bf16[1,1,512]{2,1,0:T(2,128)(2,1)S(1)} %reshape.9), channel_id=1, replica_groups=mesh['grp'=2,'fs'=4,'tp'=4] {'tp'}, dimensions={0}, use_global_device_ids=true | all-gather | bytes 5120 | tf_op jit(solution)/shard_map/all_gather | solution.py:20
  85.4 9.2 %all-gather.11.cloned.1.call-done = bf16[256,2048]{1,0:T(8,128)(2,1)} async-done(((bf16[256,512]{1,0:T(8,128)(2,1)}), bf16[256,2048]{1,0:T(8,128)(2,1)}) %all-gather.11.cloned.1.call-update) | async-done | bytes 1048592 | tf_op jit(solution)/shard_map/all_gather | solution.py:19
  94.6 1.5 fusion.2
  96.1 149.5 %all-gather.13.cloned.1.call-done = bf16[2048,2048]{1,0:T(8,128)(2,1)} async-done(((bf16[512,2048]{1,0:T(8,128)(2,1)}), bf16[2048,2048]{1,0:T(8,128)(2,1)}) %all-gather.13.cloned.1.call-update) | async-done | bytes 8388624 | tf_op jit(solution)/shard_map/all_gather | solution.py:27
  245.7 149.2 %all-gather.15.cloned.1.call-done = bf16[2048,2048]{1,0:T(8,128)(2,1)} async-done(((bf16[2048,512]{1,0:T(8,128)(2,1)}), bf16[2048,2048]{1,0:T(8,128)(2,1)}) %all-gather.15.cloned.1.call-update) | async-done | bytes 8388624 | tf_op jit(solution)/shard_map/all_gather | solution.py:32
  394.9 11.9 %fusion.10 = f32[256,2048]{1,0:T(8,128)} fusion(bf16[2048,2048]{1,0:T(8,128)(2,1)} %all-gather.15.cloned.1.call-done, bf16[2048,2048]{1,0:T(8,128)(2,1)} %all-gather.13.cloned.1.call-done, bf16[256,2048]{1,0:T(8,128)(2,1)} %all-gather.11.cloned.1.call-done, f32[2048]{0:T(1024)S(1)} %bitcast.5, f32[256]{0:T(256)S(1)} %add_rsqrt_fusion), kind=kOutput, calls=%fused_computation.12 | convolution fusion | flops 4298637312 | bytes 19932160 | tf_op jit(solution)/shard_map/dot_general | solution.py:30
  406.9 0.0 reduce-scatter.2.cloned.1.call-update
  406.9 29.5 %reduce-scatter.2.cloned.1.call-done = f32[256,512]{1,0:T(8,128)} async-done(((f32[256,2048]{1,0:T(8,128)}), f32[256,512]{1,0:T(8,128)}) %reduce-scatter.2.cloned.1.call-update) | async-done | bytes 524304 | tf_op jit(solution)/shard_map/reduce_scatter | solution.py:35
  436.4 1.8 add_convert_fusion
  (6 shorter events, 0.0 us)
Async XLA Ops:
  6.5 21.8 %all-gather.7.cloned.1.call-start = ((), (), s32[]{:S(2)}) async-start(), calls=%async_computation.1 | async-start | bytes 1310720 | tf_op jit(solution)/shard_map/all_gather | solution.py:14
  7.3 68.3 %all-gather.9.cloned.1.call-start = ((), (), s32[]{:S(2)}) async-start(), calls=%async_computation.2 | async-start | bytes 2621440 | tf_op jit(solution)/shard_map/all_gather | solution.py:15
  8.0 86.6 %all-gather.11.cloned.1.call-start = ((), (), s32[]{:S(2)}) async-start(), calls=%async_computation.3 | async-start | bytes 1310720 | tf_op jit(solution)/shard_map/all_gather | solution.py:19
  78.9 1.2 copy-start.1
  78.9 166.7 %all-gather.13.cloned.1.call-start = ((), (), s32[]{:S(2)}) async-start(), calls=%async_computation.4 | async-start | bytes 10485760 | tf_op jit(solution)/shard_map/all_gather | solution.py:27
  79.5 315.4 %all-gather.15.cloned.1.call-start = ((), (), s32[]{:S(2)}) async-start(), calls=%async_computation.5 | async-start | bytes 10485760 | tf_op jit(solution)/shard_map/all_gather | solution.py:32
  80.1 356.3 %reduce-scatter.2.cloned.1.call-start = ((), (), s32[]{:S(2)}) async-start(), calls=%async_computation.6 | async-start | bytes 2621440 | tf_op jit(solution)/shard_map/reduce_scatter | solution.py:35
  406.9 29.6 %copy-start = (bf16[256,512]{1,0:T(8,128)(2,1)S(1)}, bf16[256,512]{1,0:T(8,128)(2,1)}, u32[]{:S(2)}) copy-start(bf16[256,512]{1,0:T(8,128)(2,1)} %fusion.5) | copy-start | bytes 786436
Sparse Core Ops, SparseCore 0:
  8.9 19.4 all-gather.6
  29.9 45.6 all-gather.8
  79.1 15.4 all-gather.10
  96.0 149.5 all-gather.12
  247.1 147.7 all-gather.14
  407.0 29.3 reduce-scatter.1
where the time goes:
time: 445 us
  waiting for transfers between devices  408 us (92%)
  matrix products  15.3 us (3%)
  between operations  13.5 us (3%)
  blocking collectives  5.19 us (1%)
    all_gather x1, waiting for transfers between devices, body(): up_full = lax.all_gather(up_weight, 'fs', axis=0, tiled=True)  150 us
    all_gather x1, waiting for transfers between devices, body(): lax.all_gather(down_weight, 'fs', axis=1, tiled=True)  149 us
    all_gather x1, waiting for transfers between devices, body(): lax.all_gather(out_weight, 'fs', axis=0, tiled=True)  47.3 us
    reduce_scatter x1, waiting for transfers between devices, body(): branch = lax.psum_scatter(partials, 'tp', scatter_dimension=1, tiled=True)  29.5 us
    all_gather x1, waiting for transfers between devices, body(): mixed_whole = lax.all_gather(mixed, 'tp', axis=1, tiled=True)  20.3 us
    dot_general x1, matrix products, body(): jnp.dot(activated, lax.all_gather(down_weight, 'fs', axis=1, tiled=True),...  11.9 us
    all_gather x1, waiting for transfers between devices, body(): lax.all_gather(resid, 'tp', axis=1, tiled=True)  9.21 us
  transfers between devices with their start and end apart: 6, of which 6 were waited for; matrix products, arithmetic and copies ran while one was open for 0% of the time, Pallas kernels for 0%

commit v1 on v0

v1 whole, which is shorter than its diff:
```python
import functools

import jax
import jax.numpy as jnp
from jax import lax
from jax.experimental import pallas as pl
from jax.experimental.pallas import tpu as pltpu
from jax.sharding import PartitionSpec as P

epsilon = 1e-06


def fold_product(left, portion):
    return jnp.dot(left, portion, preferred_element_type=jnp.float32)


def gathered_weights(stream, mixed, out_weight, norm_gain, up_weight, down_weight):
    mixed_whole = lax.all_gather(mixed, "tp", axis=1, tiled=True)
    projected = fold_product(mixed_whole, lax.all_gather(out_weight, "fs", axis=0, tiled=True))
    resid = (stream.astype(jnp.float32) + projected).astype(jnp.bfloat16)
    widened = resid.astype(jnp.float32)
    resid_whole, gain_whole = (
        lax.all_gather(resid, "tp", axis=1, tiled=True),
        lax.all_gather(norm_gain, "tp", axis=0, tiled=True),
    )
    stream_wide = resid_whole.astype(jnp.float32)
    energy = jnp.mean(stream_wide * stream_wide, axis=1, keepdims=True)
    normed_whole = (
        stream_wide * lax.rsqrt(energy + epsilon) * gain_whole.astype(jnp.float32)
    ).astype(jnp.bfloat16)
    up_full = lax.all_gather(up_weight, "fs", axis=0, tiled=True)
    up_values = fold_product(normed_whole, up_full)
    activated = jnp.square(jax.nn.relu(up_values)).astype(jnp.bfloat16)
    partials = fold_product(activated, lax.all_gather(down_weight, "fs", axis=1, tiled=True))
    branch = lax.psum_scatter(partials, "tp", scatter_dimension=1, tiled=True)
    return (widened + branch).astype(jnp.bfloat16)


def dot_of(left, right):
    return jnp.dot(left, right, preferred_element_type=jnp.float32)


def first_projection_kernel(at, mixed, flip1, flip2, flip3, weight, piece, stacked, near, far):
    half = piece.shape[1]
    for flip, block in enumerate((mixed, flip1, flip2, flip3)):
        stacked[flip] = block[...]
    mine = weight[:, pl.ds(pl.multiple_of(at[4] * half, half), half)]
    other = weight[:, pl.ds(pl.multiple_of((1 - at[4]) * half, half), half)]
    near[...] = dot_of(stacked[at[0]], mine) + dot_of(stacked[at[1]], piece[...])
    far[...] = dot_of(stacked[at[0]], other)


def second_projection_kernel(at, stacked, piece, near, out):
    out[...] = near[...] + dot_of(stacked[at[3]], piece[...])


def third_projection_kernel(at, stacked, piece2, far1, far3, near, far, near_out, far_out):
    near_out[...] = near[...] + dot_of(stacked[at[2]], piece2[...])
    far_out[...] = far[...] + dot_of(stacked[at[1]], far1[...]) + dot_of(stacked[at[3]], far3[...])


def last_projection_kernel(at, stacked, far2, near, far, stream, gain, resid, scaled):
    half = far2.shape[1]
    other = far[...] + dot_of(stacked[at[2]], far2[...])
    for side, value in ((at[4], near[...]), (1 - at[4], other)):
        columns = pl.ds(pl.multiple_of(side * half, half), half)
        kept = (stream[:, columns].astype(jnp.float32) + value).astype(jnp.bfloat16)
        resid[:, columns] = kept
        scaled[:, columns] = (kept.astype(jnp.float32) * gain[:, columns].astype(jnp.float32)).astype(jnp.bfloat16)


def inverse_kernel(features, one, two, out):
    out[...] = 1.0 / ((one[...] + two[...]) / features + epsilon)


def hidden_kernel(place, own_a, pair_a, others_a, own_b, pair_b, others_b, *rest):
    near, far, out, weights = rest[:4], rest[4:6], rest[6], rest[7]
    depth, half = near[0].shape
    for slot, piece in enumerate(near):
        rows = pl.ds(pl.multiple_of(place[slot] * depth, depth), depth)
        weights[rows, :half] = piece[...]
        weights[rows, half:] = far[0][...] if slot == 0 else far[1][slot - 1]
    count = own_a.shape[0]
    for group, (own, pair, others) in enumerate(((own_a, pair_a, others_a), (own_b, pair_b, others_b))):
        total = jnp.zeros((count, 2 * half), jnp.float32)
        for flip, block in enumerate((own, others, pair, others)):
            left = block[flip // 2] if flip % 2 else block[...]
            total += jnp.dot(
                left, weights[flip * depth : (flip + 1) * depth, :], preferred_element_type=jnp.float32
            )
        out[group * count : (group + 1) * count, :] = jnp.square(jnp.maximum(total, 0.0)).astype(jnp.bfloat16)


def branch_products(hidden, weights, keep, give):
    for flip in (1, 3, 0, 2):
        value = jnp.dot(hidden, weights[flip], preferred_element_type=jnp.float32)
        target = give if flip % 2 else keep
        target[flip // 2] = value.astype(target.dtype)


def first_branch_kernel(count, place, hidden, *rest):
    near, far, keep, give, weights = rest[:4], rest[4:8], rest[8], rest[9], rest[10]
    half = near[0].shape[0]
    for slot in range(len(near)):
        weights[place[slot], :half, :] = near[slot][...]
        weights[place[slot], half:, :] = far[slot][...]
    branch_products(hidden[:count, :], weights, keep, give)


def second_branch_kernel(count, hidden, weights, keep, give):
    branch_products(hidden[count:, :], weights, keep, give)


def local_call(kernel, outs, *operands, flops, scratch=()):
    specs = [
        pl.BlockSpec(memory_space=pltpu.SMEM if x.dtype == jnp.int32 else pltpu.VMEM) for x in operands
    ]
    return pl.pallas_call(
        kernel,
        out_shape=outs,
        in_specs=specs,
        out_specs=jax.tree.map(lambda _: pl.BlockSpec(memory_space=pltpu.VMEM), outs),
        scratch_shapes=scratch,
        cost_estimate=pl.CostEstimate(flops=flops, bytes_accessed=1 << 20, transcendentals=0),
    )(*operands)


def gathered_tokens(parts, stream, mixed, out_weight, norm_gain, up_weight, down_weight):
    tokens, width = stream.shape
    half = width // 2
    unit = up_weight.shape[1] // parts
    part, row, column = lax.axis_index("grp"), lax.axis_index("fs"), lax.axis_index("tp")
    shifts = (1, 3, 2)

    def along_rows(value, shift):
        return lax.ppermute(value, "fs", [(i, (i + shift) % parts) for i in range(parts)])

    def across_parts(value):
        return lax.ppermute(value, "grp", [(0, 1), (1, 0)])

    def across_columns(value, flip):
        return lax.ppermute(value, "tp", [(i, i ^ flip) for i in range(parts)])

    def rows_at(value, begin, size):
        return lax.dynamic_slice_in_dim(value, begin, size, 0)

    def columns_at(value, begin, size):
        return lax.dynamic_slice_in_dim(value, begin, size, 1)

    at = jnp.stack([column ^ ((row - s) % parts) for s in range(parts)] + [part]).astype(jnp.int32)
    out_mine = columns_at(out_weight, part * half, half)
    out_near = {s: along_rows(out_mine, s) for s in shifts}
    flipped = [across_columns(mixed, flip) for flip in (1, 2, 3)]
    out_far = {s: across_parts(out_near[s]) for s in shifts}
    sums = jax.ShapeDtypeStruct((tokens, half), jnp.float32)
    flops = 2 * tokens * width * half
    stacked, near, far = local_call(
        first_projection_kernel,
        (jax.ShapeDtypeStruct((parts, tokens, width), jnp.bfloat16), sums, sums),
        at, mixed, *flipped, out_weight, out_near[1],
        flops=3 * flops,
    )
    near = local_call(second_projection_kernel, sums, at, stacked, out_near[3], near, flops=flops)
    near, far = local_call(
        third_projection_kernel, (sums, sums),
        at, stacked, out_near[2], out_far[1], out_far[3], near, far,
        flops=3 * flops,
    )
    resid, scaled = local_call(
        last_projection_kernel,
        (jax.ShapeDtypeStruct((tokens, width), jnp.bfloat16),) * 2,
        at, stacked, out_far[2], near, far, stream, norm_gain.reshape(1, width),
        flops=flops,
    )
    widened = resid.astype(jnp.float32)
    power = jnp.sum(widened * widened, axis=1).reshape(-1, 128)
    power += across_columns(power, 1)
    inverse = local_call(
        functools.partial(inverse_kernel, parts * width),
        jax.ShapeDtypeStruct(power.shape, jnp.float32),
        power, across_columns(power, 2),
        flops=1024,
    )

    def up_piece(s, side):
        return columns_at(up_weight, ((row + s) % parts) * unit + side * (unit // 2), unit // 2)

    def down_piece(s, side):
        return rows_at(down_weight, ((row + s) % parts) * unit + side * (unit // 2), unit // 2)

    up_near = {s: along_rows(up_piece(s, part), s) for s in shifts}
    up_far = across_parts(jnp.stack([up_near[s] for s in (1, 2, 3)]))
    down_near = {s: along_rows(down_piece(s, part), s) for s in shifts}
    down_far = {s: across_parts(down_near[s]) for s in shifts}
    place = jnp.stack([column ^ ((row - s) % parts) for s in range(parts)]).astype(jnp.int32)

    pairs = {0: across_columns(scaled, 2)}
    rows = {0: scaled} | {s: along_rows(scaled, s) for s in shifts}
    pairs[2] = across_columns(rows[2], 2)
    odd = jnp.concatenate([rows[1], rows[3]])
    even = jnp.concatenate([rows[0], rows[2]])
    even_pair = jnp.concatenate([pairs[0], pairs[2]])
    odd_pair = across_columns(odd, 2)
    even_others = across_columns(jnp.stack([even, even_pair]), 1)
    odd_others = across_columns(jnp.stack([odd, odd_pair]), 1)
    flops = 2 * parts * tokens * parts * width * unit
    hidden = local_call(
        hidden_kernel,
        jax.ShapeDtypeStruct((parts * tokens, unit), jnp.bfloat16),
        place, even, even_pair, even_others, odd, odd_pair, odd_others,
        up_piece(0, part), up_near[1], up_near[2], up_near[3], up_piece(0, 1 - part), up_far,
        flops=flops,
        scratch=[pltpu.VMEM((parts * width, unit), jnp.bfloat16)],
    )
    count = 2 * tokens
    halves = (
        jax.ShapeDtypeStruct((2, count, width), jnp.float32),
        jax.ShapeDtypeStruct((2, count, width), jnp.bfloat16),
    )
    keep_a, give_a, down_whole = local_call(
        functools.partial(first_branch_kernel, count),
        (*halves, jax.ShapeDtypeStruct((parts, unit, width), jnp.bfloat16)),
        place, hidden,
        down_piece(0, part), down_near[1], down_near[2], down_near[3],
        down_piece(0, 1 - part), down_far[1], down_far[2], down_far[3],
        flops=flops // 2,
    )
    keep_b, give_b = local_call(
        functools.partial(second_branch_kernel, count), halves, hidden, down_whole, flops=flops // 2
    )
    got_a = across_columns(give_a, 1)
    got_b = across_columns(give_b, 1)
    even_give = (keep_a[1] + got_a[1]).astype(jnp.bfloat16)
    odd_give = (keep_b[1] + got_b[1]).astype(jnp.bfloat16)
    even_keep, odd_keep = keep_a[0] + got_a[0], keep_b[0] + got_b[0]
    two = even_keep[tokens:] + across_columns(even_give[tokens:], 2)
    odd_sum = (odd_keep + across_columns(odd_give, 2)).astype(jnp.bfloat16)
    branch = even_keep[:tokens] + across_columns(even_give[:tokens], 2)
    branch += along_rows(two.astype(jnp.bfloat16), -2)
    branch += along_rows(odd_sum[:tokens], -1)
    branch += along_rows(odd_sum[tokens:], -3)
    return (widened + branch * inverse.reshape(tokens, 1)).astype(jnp.bfloat16)


def solution(mesh):
    shape = mesh.shape
    placed = (
        P(("grp", "fs"), "tp"),
        P(("grp", "fs"), "tp"),
        P("fs", "tp"),
        P("tp"),
        P("fs", "tp"),
        P("tp", "fs"),
    )

    cut = shape["grp"] == 2 and shape["fs"] == 4 and shape["tp"] == 4

    def body(*blocks):
        if not cut:
            return gathered_weights(*blocks)
        return gathered_tokens(shape["fs"], *blocks)

    return jax.shard_map(
        body, mesh=mesh, in_specs=placed, out_specs=P(("grp", "fs"), "tp"), check_vma=False
    )
```

time: 445 us -> 202 us (0.45)
  waiting for transfers between devices: 408 us -> 97.1 us
  starting transfers between devices: 0.2 us -> 58.8 us
  Pallas kernels: 0 us -> 27.7 us
  matrix products: 15.3 us -> 0 us
  between operations: 13.5 us -> 0.42 us
  local copies, waits for them, and re-layouts: 0.01 us -> 11.6 us
  blocking collectives: 5.19 us -> 0 us
    all_gather x5 -> x0, waiting for transfers between devices: 376 us -> none  [the longest x1 150 us: body(): up_full = lax.all_gather(up_weight, 'fs', axis=0, tiled=True)]
    ppermute x0 -> x37, waiting for transfers between devices: none -> 97.1 us  [the longest x15 64.1 us: along_rows(): lax.ppermute(value, 'fs', [(i, (i + shift) % parts) for i in range(parts)])]
    ppermute x0 -> x37, starting transfers between devices: none -> 58.8 us  [the longest x15 37.2 us: along_rows(): lax.ppermute(value, 'fs', [(i, (i + shift) % parts) for i in range(parts)])]
    reduce_scatter x1 -> x0, waiting for transfers between devices: 29.5 us -> none  [body(): branch = lax.psum_scatter(partials, 'tp', scatter_dimension=1, tiled=True)]
    pallas_call x0 -> x8, Pallas kernels: none -> 27.7 us  [local_call(): pl.pallas_call(kernel, out_shape=outs, in_specs=specs, out_specs=jax.tree...]
    dot_general x2 -> x0, matrix products: 15.3 us -> none  [the longest x1 11.9 us: body(): jnp.dot(activated, lax.all_gather(down_weight, 'fs', axis=1, tiled=True),...]
    unnamed x5 -> x71, local copies, waits for them, and re-layouts: 0.01 us -> 6.72 us
    all_gather x1 -> x0, blocking collectives: 5.19 us -> none  [body(): lax.all_gather(norm_gain, 'tp', axis=0, tiled=True)]
  transfers between devices with their start and end apart: 6 -> 37, of which waited for: 6 -> 18; matrix products, arithmetic and copies ran while one was open for 0% -> 4% of each run, Pallas kernels for 0% -> 8%
where the time goes in v1:
time: 202 us; the launch traced here: 200 us
  waiting for transfers between devices  97.1 us (48%)
  starting transfers between devices  58.8 us (29%)
  Pallas kernels  27.7 us (14%)
  local copies, waits for them, and re-layouts  11.6 us (6%)
  other arithmetic  4.85 us (2%)
    ppermute x15, waiting for transfers between devices, along_rows(): lax.ppermute(value, 'fs', [(i, (i + shift) % parts) for i in range(parts)])  64.1 us
    ppermute x15, starting transfers between devices, along_rows(): lax.ppermute(value, 'fs', [(i, (i + shift) % parts) for i in range(parts)])  37.2 us
    ppermute x15, waiting for transfers between devices, across_columns(): return lax.ppermute(value, 'tp', [(i, i ^ flip) for i in range(parts)])  29.4 us
    pallas_call x8, Pallas kernels, local_call(): pl.pallas_call(kernel, out_shape=outs, in_specs=specs, out_specs=jax.tree...  27.7 us
    ppermute x15, starting transfers between devices, across_columns(): return lax.ppermute(value, 'tp', [(i, i ^ flip) for i in range(parts)])  12.6 us
    ppermute x7, starting transfers between devices, across_parts(): return lax.ppermute(value, 'grp', [(0, 1), (1, 0)])  8.97 us
    unnamed x71, local copies, waits for them, and re-layouts  6.72 us
  transfers between devices with their start and end apart: 37, of which 18 were waited for; matrix products, arithmetic and copies ran while one was open for 4% of the time, Pallas kernels for 8%

profile of v1, /device:TPU:0, one launch (start us, length us, event | category | flops | bytes accessed | tf_op | source)
XLA Modules:
  0.0 200.5 jit_solution(1906544131222829047)
XLA Ops:
  1.5 2.6 %collective-permute-start.3 = (bf16[512,256]{1,0:T(8,128)(2,1)S(1)}, bf16[512,256]{1,0:T(8,128)(2,1)S(1)}, u32[]{:S(2)}, u32[]{:S(2)}) collective-permute-start(bf16[512,256]{1,0:T(8,128)(2,1)S(1)} %constant_dynamic-slice_fusion.10), channel_id=1, source_target_pairs={{0,4},{4,8},{8,12},{12,0},{1,5},{5,9},{9,13},{13,1},{2,6},{6,10},{... | collective-permute-start | bytes 786440 | tf_op jit(solution)/shard_map/ppermute | solution.py:136
  8.7 4.7 %collective-permute-done.3.piece = bf16[512,256]{1,0:T(8,128)(2,1)S(1)} collective-permute-done((bf16[512,256]{1,0:T(8,128)(2,1)S(1)}, bf16[512,256]{1,0:T(8,128)(2,1)S(1)}, u32[]{:S(2)}, u32[]{:S(2)}) %collective-permute-start.3) | collective-permute-done | bytes 262176 | tf_op jit(solution)/shard_map/ppermute | solution.py:136
  15.0 3.1 %collective-permute-done.7.piece = bf16[512,256]{1,0:T(8,128)(2,1)S(1)} collective-permute-done((bf16[512,256]{1,0:T(8,128)(2,1)S(1)}, bf16[512,256]{1,0:T(8,128)(2,1)S(1)}, u32[]{:S(2)}, u32[]{:S(2)}) %collective-permute-start.7) | collective-permute-done | bytes 262176 | tf_op jit(solution)/shard_map/ppermute | solution.py:136
  19.6 10.3 %collective-permute-done.4.piece2 = bf16[512,256]{1,0:T(8,128)(2,1)S(1)} collective-permute-done((bf16[512,256]{1,0:T(8,128)(2,1)S(1)}, bf16[512,256]{1,0:T(8,128)(2,1)S(1)}, u32[]{:S(2)}, u32[]{:S(2)}) %collective-permute-start.4) | collective-permute-done | bytes 262176 | tf_op jit(solution)/shard_map/ppermute | solution.py:136
  34.8 2.7 %shard_map.64 = (bf16[4,256,512]{2,1,0:T(8,128)(2,1)}, f32[256,256]{1,0:T(8,128)}, f32[256,256]{1,0:T(8,128)}) custom-call(s32[5]{0:T(128)} %stack.60.at, bf16[256,512]{1,0:T(8,128)(2,1)} %mixed.1, bf16[256,512]{1,0:T(8,128)(2,1)} %copy-done.13, bf16[256,512]{1,0:T(8,128)(2,1)} %copy-done.16, bf16[256,512]{1,0:T(8,128)(2,1)} %copy-done.17, ...), custom_call_target="tpu_custom_call" | custom-call | flops 201326592 | bytes 1048576 | tf_op jit(solution)/shard_map/pallas_call | solution.py:118
  40.6 2.9 %shard_map.66 = (f32[256,256]{1,0:T(8,128)}, f32[256,256]{1,0:T(8,128)}) custom-call(s32[5]{0:T(128)} %stack.60.at, bf16[4,256,512]{2,1,0:T(8,128)(2,1)} %get-tuple-element.17.stacked, bf16[512,256]{1,0:T(8,128)(2,1)} %copy-done.9, bf16[512,256]{1,0:T(8,128)(2,1)} %copy-done.10, bf16[512,256]{1,0:T(8,128)(2,1)} %copy-done.11, f32[256,256]{1,0:T(8,128)} %shard_map.65.near, ...), custom_call_target="tpu_custom_call" | custom-call | flops 201326592 | bytes 1048576 | tf_op jit(solution)/shard_map/pallas_call | solution.py:118
  44.1 2.5 %shard_map.67 = (bf16[256,512]{1,0:T(8,128)(2,1)}, bf16[256,512]{1,0:T(8,128)(2,1)}) custom-call(s32[5]{0:T(128)} %stack.60.at, bf16[4,256,512]{2,1,0:T(8,128)(2,1)} %get-tuple-element.17.stacked, bf16[512,256]{1,0:T(8,128)(2,1)} %copy-done.21, f32[256,256]{1,0:T(8,128)} %get-tuple-element.20.near, f32[256,256]{1,0:T(8,128)} %get-tuple-element.21.far, ...), custom_call_target="tpu_custom_call" | custom-call | flops 67108864 | bytes 1048576 | tf_op jit(solution)/shard_map/pallas_call | solution.py:118
  53.5 4.5 %collective-permute-done.13 = bf16[256,512]{1,0:T(8,128)(2,1)S(1)} collective-permute-done((bf16[256,512]{1,0:T(8,128)(2,1)}, bf16[256,512]{1,0:T(8,128)(2,1)S(1)}, u32[]{:S(2)}, u32[]{:S(2)}) %collective-permute-start.13) | collective-permute-done | bytes 262176 | tf_op jit(solution)/shard_map/ppermute | solution.py:136
  59.5 5.6 %collective-permute-done.14 = bf16[256,512]{1,0:T(8,128)(2,1)S(1)} collective-permute-done((bf16[256,512]{1,0:T(8,128)(2,1)}, bf16[256,512]{1,0:T(8,128)(2,1)S(1)}, u32[]{:S(2)}, u32[]{:S(2)}) %collective-permute-start.14) | collective-permute-done | bytes 262176 | tf_op jit(solution)/shard_map/ppermute | solution.py:136
  70.8 4.6 %collective-permute-start.19 = (bf16[512,256]{1,0:T(8,128)(2,1)S(1)}, bf16[512,256]{1,0:T(8,128)(2,1)S(1)}, u32[]{:S(2)}, u32[]{:S(2)}) collective-permute-start(bf16[512,256]{1,0:T(8,128)(2,1)S(1)} %get-tuple-element.40), channel_id=1, source_target_pairs={{0,12},{4,0},{8,4},{12,8},{1,13},{5,1},{9,5},{13,9},{2,14},{6,2},{... | collective-permute-start | bytes 786440 | tf_op jit(solution)/shard_map/ppermute | solution.py:136
  75.4 7.5 %collective-permute-done.11 = bf16[256,512]{1,0:T(8,128)(2,1)S(1)} collective-permute-done((bf16[256,512]{1,0:T(8,128)(2,1)S(1)}, bf16[256,512]{1,0:T(8,128)(2,1)S(1)}, u32[]{:S(2)}, u32[]{:S(2)}) %collective-permute-start.11) | collective-permute-done | bytes 262176 | tf_op jit(solution)/shard_map/ppermute | solution.py:142
  83.8 6.7 %collective-permute-done.18.rest_2_ = bf16[512,256]{1,0:T(8,128)(2,1)S(1)} collective-permute-done((bf16[512,256]{1,0:T(8,128)(2,1)S(1)}, bf16[512,256]{1,0:T(8,128)(2,1)S(1)}, u32[]{:S(2)}, u32[]{:S(2)}) %collective-permute-start.18) | collective-permute-done | bytes 262176 | tf_op jit(solution)/shard_map/ppermute | solution.py:136
  90.5 4.7 %collective-permute-done.19.rest_3_ = bf16[512,256]{1,0:T(8,128)(2,1)S(1)} collective-permute-done((bf16[512,256]{1,0:T(8,128)(2,1)S(1)}, bf16[512,256]{1,0:T(8,128)(2,1)S(1)}, u32[]{:S(2)}, u32[]{:S(2)}) %collective-permute-start.19) | collective-permute-done | bytes 262176 | tf_op jit(solution)/shard_map/ppermute | solution.py:136
  96.9 9.8 %collective-permute-start.21 = (bf16[256,512]{1,0:T(8,128)(2,1)S(1)}, bf16[256,512]{1,0:T(8,128)(2,1)S(1)}, u32[]{:S(2)}, u32[]{:S(2)}) collective-permute-start(bf16[256,512]{1,0:T(8,128)(2,1)S(1)} %get-tuple-element.33), channel_id=1, source_target_pairs={{0,4},{4,8},{8,12},{12,0},{1,5},{5,9},{9,13},{13,1},{2,6},{6,10},{... | collective-permute-start | bytes 786440 | tf_op jit(solution)/shard_map/ppermute | solution.py:136
  106.6 6.7 %collective-permute-done.21.rest_1_ = bf16[256,512]{1,0:T(8,128)(2,1)S(1)} collective-permute-done((bf16[256,512]{1,0:T(8,128)(2,1)S(1)}, bf16[256,512]{1,0:T(8,128)(2,1)S(1)}, u32[]{:S(2)}, u32[]{:S(2)}) %collective-permute-start.21) | collective-permute-done | bytes 262176 | tf_op jit(solution)/shard_map/ppermute | solution.py:136
  113.3 7.2 %collective-permute-done.22.rest_2_ = bf16[256,512]{1,0:T(8,128)(2,1)S(1)} collective-permute-done((bf16[256,512]{1,0:T(8,128)(2,1)S(1)}, bf16[256,512]{1,0:T(8,128)(2,1)S(1)}, u32[]{:S(2)}, u32[]{:S(2)}) %collective-permute-start.22) | collective-permute-done | bytes 262176 | tf_op jit(solution)/shard_map/ppermute | solution.py:136
  122.1 3.0 %collective-permute-done.23.rest_3_ = bf16[256,512]{1,0:T(8,128)(2,1)S(1)} collective-permute-done((bf16[256,512]{1,0:T(8,128)(2,1)S(1)}, bf16[256,512]{1,0:T(8,128)(2,1)S(1)}, u32[]{:S(2)}, u32[]{:S(2)}) %collective-permute-start.23) | collective-permute-done | bytes 262176 | tf_op jit(solution)/shard_map/ppermute | solution.py:136
  129.9 6.3 %shard_map.68.hidden = bf16[1024,512]{1,0:T(8,128)(2,1)} custom-call(s32[4]{0:T(128)} %pad_add_fusion.place, bf16[512,512]{1,0:T(8,128)(2,1)} %copy-done.4, bf16[512,512]{1,0:T(8,128)(2,1)} %copy-done.2, bf16[2,512,512]{2,1,0:T(8,128)(2,1)} %copy-done.24, bf16[512,512]{1,0:T(8,128)(2,1)} %copy-done.3, bf16[512,512]{1,0:T(8,128)(2,1)} %copy-done.8, ...), custom_call_target="tpu_custom_call" | custom-call | flops 2147483648 | bytes 1048576 | tf_op jit(solution)/shard_map/pallas_call | solution.py:118
  136.3 3.6 %collective-permute-done.26.rest_7_ = bf16[256,512]{1,0:T(8,128)(2,1)S(1)} collective-permute-done((bf16[256,512]{1,0:T(8,128)(2,1)S(1)}, bf16[256,512]{1,0:T(8,128)(2,1)S(1)}, u32[]{:S(2)}, u32[]{:S(2)}) %collective-permute-start.26) | collective-permute-done | bytes 262176 | tf_op jit(solution)/shard_map/ppermute | solution.py:139
  140.6 5.1 %shard_map.69 = (f32[2,512,512]{2,1,0:T(8,128)}, bf16[2,512,512]{2,1,0:T(8,128)(2,1)}, bf16[4,512,512]{2,1,0:T(8,128)(2,1)}) custom-call(s32[4]{0:T(128)} %pad_add_fusion.place, bf16[1024,512]{1,0:T(8,128)(2,1)} %shard_map.68.hidden, bf16[256,512]{1,0:T(8,128)(2,1)} %get-tuple-element.34.rest_0_, bf16[256,512]{1,0:T(8,128)(2,1)} %copy-done.28, ...), custom_call_target="tpu_custom_call" | custom-call | flops 1073741824 | bytes 1048576 | tf_op jit(solution)/shard_map/pallas_call | solution.py:118
  145.8 4.7 %shard_map.70 = (f32[2,512,512]{2,1,0:T(8,128)}, bf16[2,512,512]{2,1,0:T(8,128)(2,1)}) custom-call(bf16[1024,512]{1,0:T(8,128)(2,1)} %shard_map.68.hidden, bf16[4,512,512]{2,1,0:T(8,128)(2,1)} %get-tuple-element.26.weights), custom_call_target="tpu_custom_call" | custom-call | flops 1073741824 | bytes 1048576 | tf_op jit(solution)/shard_map/pallas_call | solution.py:118
  158.9 16.3 %collective-permute-done.29 = bf16[256,512]{1,0:T(8,128)(2,1)S(1)} collective-permute-done((bf16[256,512]{1,0:T(8,128)(2,1)S(1)}, bf16[256,512]{1,0:T(8,128)(2,1)S(1)}, u32[]{:S(2)}, u32[]{:S(2)}) %collective-permute-start.29) | collective-permute-done | bytes 262176 | tf_op jit(solution)/shard_map/ppermute | solution.py:142
  176.1 10.9 %collective-permute-start.34 = (bf16[256,512]{1,0:T(8,128)(2,1)S(1)}, bf16[256,512]{1,0:T(8,128)(2,1)S(1)}, u32[]{:S(2)}, u32[]{:S(2)}) collective-permute-start(bf16[256,512]{1,0:T(8,128)(2,1)S(1)} %get-tuple-element.44), channel_id=1, source_target_pairs={{0,4},{4,8},{8,12},{12,0},{1,5},{5,9},{9,13},{13,1},{2,6},{6,10},{... | collective-permute-start | bytes 786440 | tf_op jit(solution)/shard_map/ppermute | solution.py:136
  193.9 5.1 %collective-permute-done.34 = bf16[256,512]{1,0:T(8,128)(2,1)S(1)} collective-permute-done((bf16[256,512]{1,0:T(8,128)(2,1)S(1)}, bf16[256,512]{1,0:T(8,128)(2,1)S(1)}, u32[]{:S(2)}, u32[]{:S(2)}) %collective-permute-start.34) | collective-permute-done | bytes 262176 | tf_op jit(solution)/shard_map/ppermute | solution.py:136
  (150 shorter events, 58.9 us)
Async XLA Ops:
  4.1 14.1 %collective-permute-start.7 = (bf16[512,256]{1,0:T(8,128)(2,1)S(1)}, bf16[512,256]{1,0:T(8,128)(2,1)S(1)}, u32[]{:S(2)}, u32[]{:S(2)}) collective-permute-start(bf16[512,256]{1,0:T(8,128)(2,1)S(1)} %constant_dynamic-slice_fusion.10), channel_id=1, source_target_pairs={{0,12},{4,0},{8,4},{12,8},{1,13},{5,1},{9,5},{13,9},{2,14},{6,2},{... | collective-permute-start | bytes 786440 | tf_op jit(solution)/shard_map/ppermute | solution.py:136
  6.2 23.8 %collective-permute-start.4 = (bf16[512,256]{1,0:T(8,128)(2,1)S(1)}, bf16[512,256]{1,0:T(8,128)(2,1)S(1)}, u32[]{:S(2)}, u32[]{:S(2)}) collective-permute-start(bf16[512,256]{1,0:T(8,128)(2,1)S(1)} %constant_dynamic-slice_fusion.10), channel_id=1, source_target_pairs={{0,8},{4,12},{8,0},{12,4},{1,9},{5,13},{9,1},{13,5},{2,10},{6,14},... | collective-permute-start | bytes 786440 | tf_op jit(solution)/shard_map/ppermute | solution.py:136
  7.1 26.2 %collective-permute-start.1 = (bf16[256,512]{1,0:T(8,128)(2,1)}, bf16[256,512]{1,0:T(8,128)(2,1)S(1)}, u32[]{:S(2)}, u32[]{:S(2)}) collective-permute-start(bf16[256,512]{1,0:T(8,128)(2,1)} %mixed.1), channel_id=1, source_target_pairs={{0,2},{1,3},{2,0},{3,1},{4,6},{5,7},{6,4},{7,5},{8,10},{9,11},{10,... | collective-permute-start | bytes 786440 | tf_op jit(solution)/shard_map/ppermute | solution.py:142
  8.6 24.7 %collective-permute-start.2 = (bf16[256,512]{1,0:T(8,128)(2,1)}, bf16[256,512]{1,0:T(8,128)(2,1)S(1)}, u32[]{:S(2)}, u32[]{:S(2)}) collective-permute-start(bf16[256,512]{1,0:T(8,128)(2,1)} %mixed.1), channel_id=1, source_target_pairs={{0,3},{1,2},{2,1},{3,0},{4,7},{5,6},{6,5},{7,4},{8,11},{9,10},{10,... | collective-permute-start | bytes 786440 | tf_op jit(solution)/shard_map/ppermute | solution.py:142
  13.3 26.5 %collective-permute-start.6 = (bf16[512,256]{1,0:T(8,128)(2,1)S(1)}, bf16[512,256]{1,0:T(8,128)(2,1)S(1)}, u32[]{:S(2)}, u32[]{:S(2)}) collective-permute-start(bf16[512,256]{1,0:T(8,128)(2,1)S(1)} %collective-permute-done.3.piece), channel_id=1, source_target_pairs={{0,16},{16,0},{1,17},{17,1},{2,18},{18,2},{3,19},{19,3},{4,20},{20... | collective-permute-start | bytes 786440 | tf_op jit(solution)/shard_map/ppermute | solution.py:139
  18.1 21.6 %collective-permute-start.8 = (bf16[512,256]{1,0:T(8,128)(2,1)S(1)}, bf16[512,256]{1,0:T(8,128)(2,1)S(1)}, u32[]{:S(2)}, u32[]{:S(2)}) collective-permute-start(bf16[512,256]{1,0:T(8,128)(2,1)S(1)} %collective-permute-done.7.piece), channel_id=1, source_target_pairs={{0,16},{16,0},{1,17},{17,1},{2,18},{18,2},{3,19},{19,3},{4,20},{20... | collective-permute-start | bytes 786440 | tf_op jit(solution)/shard_map/ppermute | solution.py:139
  46.7 22.5 %collective-permute-start.9 = (bf16[256,512]{1,0:T(8,128)(2,1)}, bf16[256,512]{1,0:T(8,128)(2,1)S(1)}, u32[]{:S(2)}, u32[]{:S(2)}) collective-permute-start(bf16[256,512]{1,0:T(8,128)(2,1)} %get-tuple-element.23), channel_id=1, source_target_pairs={{0,8},{4,12},{8,0},{12,4},{1,9},{5,13},{9,1},{13,5},{2,10},{6,14},... | collective-permute-start | bytes 786440 | tf_op jit(solution)/shard_map/ppermute | solution.py:136
  48.8 16.2 %collective-permute-start.14 = (bf16[256,512]{1,0:T(8,128)(2,1)}, bf16[256,512]{1,0:T(8,128)(2,1)S(1)}, u32[]{:S(2)}, u32[]{:S(2)}) collective-permute-start(bf16[256,512]{1,0:T(8,128)(2,1)} %get-tuple-element.23), channel_id=1, source_target_pairs={{0,12},{4,0},{8,4},{12,8},{1,13},{5,1},{9,5},{13,9},{2,14},{6,2},{... | collective-permute-start | bytes 786440 | tf_op jit(solution)/shard_map/ppermute | solution.py:136
  51.4 32.4 %collective-permute-start.17 = (bf16[512,256]{1,0:T(8,128)(2,1)S(1)}, bf16[512,256]{1,0:T(8,128)(2,1)S(1)}, u32[]{:S(2)}, u32[]{:S(2)}) collective-permute-start(bf16[512,256]{1,0:T(8,128)(2,1)S(1)} %get-tuple-element.38), channel_id=1, source_target_pairs={{0,4},{4,8},{8,12},{12,0},{1,5},{5,9},{9,13},{13,1},{2,6},{6,10},{... | collective-permute-start | bytes 786440 | tf_op jit(solution)/shard_map/ppermute | solution.py:136
  52.0 38.5 %collective-permute-start.18 = (bf16[512,256]{1,0:T(8,128)(2,1)S(1)}, bf16[512,256]{1,0:T(8,128)(2,1)S(1)}, u32[]{:S(2)}, u32[]{:S(2)}) collective-permute-start(bf16[512,256]{1,0:T(8,128)(2,1)S(1)} %get-tuple-element.37), channel_id=1, source_target_pairs={{0,8},{4,12},{8,0},{12,4},{1,9},{5,13},{9,1},{13,5},{2,10},{6,14},... | collective-permute-start | bytes 786440 | tf_op jit(solution)/shard_map/ppermute | solution.py:136
  65.1 18.0 %collective-permute-start.15 = (bf16[512,512]{1,0:T(8,128)(2,1)S(1)}, bf16[512,512]{1,0:T(8,128)(2,1)S(1)}, u32[]{:S(2)}, u32[]{:S(2)}) collective-permute-start(bf16[512,512]{1,0:T(8,128)(2,1)S(1)} %constant_dynamic-update-slice_fusion.4.own_b), channel_id=1, source_target_pairs={{0,2},{1,3},{2,0},{3,1},{4,6},{5,7},{6,4},{7,5},{8,10},{9,11},{10,... | collective-permute-start | bytes 1572872 | tf_op jit(solution)/shard_map/ppermute | solution.py:142
  69.2 13.7 %collective-permute-start.11 = (bf16[256,512]{1,0:T(8,128)(2,1)S(1)}, bf16[256,512]{1,0:T(8,128)(2,1)S(1)}, u32[]{:S(2)}, u32[]{:S(2)}) collective-permute-start(bf16[256,512]{1,0:T(8,128)(2,1)S(1)} %collective-permute-done.9), channel_id=1, source_target_pairs={{0,2},{1,3},{2,0},{3,1},{4,6},{5,7},{6,4},{7,5},{8,10},{9,11},{10,... | collective-permute-start | bytes 786440 | tf_op jit(solution)/shard_map/ppermute | solution.py:142
  70.8 24.5 %collective-permute-start.19 = (bf16[512,256]{1,0:T(8,128)(2,1)S(1)}, bf16[512,256]{1,0:T(8,128)(2,1)S(1)}, u32[]{:S(2)}, u32[]{:S(2)}) collective-permute-start(bf16[512,256]{1,0:T(8,128)(2,1)S(1)} %get-tuple-element.40), channel_id=1, source_target_pairs={{0,12},{4,0},{8,4},{12,8},{1,13},{5,1},{9,5},{13,9},{2,14},{6,2},{... | collective-permute-start | bytes 786440 | tf_op jit(solution)/shard_map/ppermute | solution.py:136
  83.0 44.9 %collective-permute-start.12 = (bf16[2,512,512]{2,1,0:T(8,128)(2,1)S(1)}, bf16[2,512,512]{2,1,0:T(8,128)(2,1)S(1)}, u32[]{:S(2)}, u32[]{:S(2)}) collective-permute-start(bf16[2,512,512]{2,1,0:T(8,128)(2,1)S(1)} %pad_maximum_fusion), channel_id=1, source_target_pairs={{0,1},{1,0},{2,3},{3,2},{4,5},{5,4},{6,7},{7,6},{8,9},{9,8},{10,11... | collective-permute-start | bytes 3145736 | tf_op jit(solution)/shard_map/ppermute | solution.py:142
  83.7 44.2 %collective-permute-start.16 = (bf16[2,512,512]{2,1,0:T(8,128)(2,1)S(1)}, bf16[2,512,512]{2,1,0:T(8,128)(2,1)S(1)}, u32[]{:S(2)}, u32[]{:S(2)}) collective-permute-start(bf16[2,512,512]{2,1,0:T(8,128)(2,1)S(1)} %pad_maximum_fusion.1), channel_id=1, source_target_pairs={{0,1},{1,0},{2,3},{3,2},{4,5},{5,4},{6,7},{7,6},{8,9},{9,8},{10,11... | collective-permute-start | bytes 3145736 | tf_op jit(solution)/shard_map/ppermute | solution.py:142
  95.3 31.8 %collective-permute-start.20 = (bf16[3,512,256]{2,1,0:T(8,128)(2,1)S(1)}, bf16[3,512,256]{2,1,0:T(8,128)(2,1)S(1)}, u32[]{:S(2)}, u32[]{:S(2)}) collective-permute-start(bf16[3,512,256]{2,1,0:T(8,128)(2,1)S(1)} %pad_maximum_fusion.2), channel_id=1, source_target_pairs={{0,16},{16,0},{1,17},{17,1},{2,18},{18,2},{3,19},{19,3},{4,20},{20... | collective-permute-start | bytes 2359304 | tf_op jit(solution)/shard_map/ppermute | solution.py:139
  96.9 16.5 %collective-permute-start.21 = (bf16[256,512]{1,0:T(8,128)(2,1)S(1)}, bf16[256,512]{1,0:T(8,128)(2,1)S(1)}, u32[]{:S(2)}, u32[]{:S(2)}) collective-permute-start(bf16[256,512]{1,0:T(8,128)(2,1)S(1)} %get-tuple-element.33), channel_id=1, source_target_pairs={{0,4},{4,8},{8,12},{12,0},{1,5},{5,9},{9,13},{13,1},{2,6},{6,10},{... | collective-permute-start | bytes 786440 | tf_op jit(solution)/shard_map/ppermute | solution.py:136
  106.6 13.9 %collective-permute-start.22 = (bf16[256,512]{1,0:T(8,128)(2,1)S(1)}, bf16[256,512]{1,0:T(8,128)(2,1)S(1)}, u32[]{:S(2)}, u32[]{:S(2)}) collective-permute-start(bf16[256,512]{1,0:T(8,128)(2,1)S(1)} %get-tuple-element.32), channel_id=1, source_target_pairs={{0,8},{4,12},{8,0},{12,4},{1,9},{5,13},{9,1},{13,5},{2,10},{6,14},... | collective-permute-start | bytes 786440 | tf_op jit(solution)/shard_map/ppermute | solution.py:136
  120.6 15.7 %collective-permute-start.24 = (bf16[256,512]{1,0:T(8,128)(2,1)S(1)}, bf16[256,512]{1,0:T(8,128)(2,1)S(1)}, u32[]{:S(2)}, u32[]{:S(2)}) collective-permute-start(bf16[256,512]{1,0:T(8,128)(2,1)S(1)} %collective-permute-done.21.rest_1_), channel_id=1, source_target_pairs={{0,16},{16,0},{1,17},{17,1},{2,18},{18,2},{3,19},{19,3},{4,20},{20... | collective-permute-start | bytes 786440 | tf_op jit(solution)/shard_map/ppermute | solution.py:139
  154.8 21.0 %collective-permute-start.32 = (bf16[512,512]{1,0:T(8,128)(2,1)S(1)}, bf16[512,512]{1,0:T(8,128)(2,1)S(1)}, u32[]{:S(2)}, u32[]{:S(2)}) collective-permute-start(bf16[512,512]{1,0:T(8,128)(2,1)S(1)} %fusion.3), channel_id=1, source_target_pairs={{0,2},{1,3},{2,0},{3,1},{4,6},{5,7},{6,4},{7,5},{8,10},{9,11},{10,... | collective-permute-start | bytes 1572872 | tf_op jit(solution)/shard_map/ppermute | solution.py:142
  156.8 18.4 %collective-permute-start.29 = (bf16[256,512]{1,0:T(8,128)(2,1)S(1)}, bf16[256,512]{1,0:T(8,128)(2,1)S(1)}, u32[]{:S(2)}, u32[]{:S(2)}) collective-permute-start(bf16[256,512]{1,0:T(8,128)(2,1)S(1)} %get-tuple-element.42), channel_id=1, source_target_pairs={{0,2},{1,3},{2,0},{3,1},{4,6},{5,7},{6,4},{7,5},{8,10},{9,11},{10,... | collective-permute-start | bytes 786440 | tf_op jit(solution)/shard_map/ppermute | solution.py:142
  157.4 36.5 %collective-permute-start.28 = (bf16[256,512]{1,0:T(8,128)(2,1)S(1)}, bf16[256,512]{1,0:T(8,128)(2,1)S(1)}, u32[]{:S(2)}, u32[]{:S(2)}) collective-permute-start(bf16[256,512]{1,0:T(8,128)(2,1)S(1)} %get-tuple-element.41), channel_id=1, source_target_pairs={{0,2},{1,3},{2,0},{3,1},{4,6},{5,7},{6,4},{7,5},{8,10},{9,11},{10,... | collective-permute-start | bytes 786440 | tf_op jit(solution)/shard_map/ppermute | solution.py:142
  175.3 18.5 %collective-permute-start.30 = (bf16[256,512]{1,0:T(8,128)(2,1)S(1)}, bf16[256,512]{1,0:T(8,128)(2,1)S(1)}, u32[]{:S(2)}, u32[]{:S(2)}) collective-permute-start(bf16[256,512]{1,0:T(8,128)(2,1)S(1)} %fusion.5), channel_id=1, source_target_pairs={{0,8},{4,12},{8,0},{12,4},{1,9},{5,13},{9,1},{13,5},{2,10},{6,14},... | collective-permute-start | bytes 786440 | tf_op jit(solution)/shard_map/ppermute | solution.py:136
  176.1 22.8 %collective-permute-start.34 = (bf16[256,512]{1,0:T(8,128)(2,1)S(1)}, bf16[256,512]{1,0:T(8,128)(2,1)S(1)}, u32[]{:S(2)}, u32[]{:S(2)}) collective-permute-start(bf16[256,512]{1,0:T(8,128)(2,1)S(1)} %get-tuple-element.44), channel_id=1, source_target_pairs={{0,4},{4,8},{8,12},{12,0},{1,5},{5,9},{9,13},{13,1},{2,6},{6,10},{... | collective-permute-start | bytes 786440 | tf_op jit(solution)/shard_map/ppermute | solution.py:136
  (47 other events, 420.9 us)

commit v2 on v1

--- a/solution.py
+++ b/solution.py
@@ -69,49 +69,78 @@
         scaled[:, columns] = (kept.astype(jnp.float32) * gain[:, columns].astype(jnp.float32)).astype(jnp.bfloat16)
 
 
-def inverse_kernel(features, one, two, out):
-    out[...] = 1.0 / ((one[...] + two[...]) / features + epsilon)
-
-
-def hidden_kernel(place, own_a, pair_a, others_a, own_b, pair_b, others_b, *rest):
+def mean_kernel(features, one, two, out):
+    out[...] = (one[...] + two[...]) / features
+
+
+def inverse_kernel(energy, out):
+    out[...] = 1.0 / (energy[...] + epsilon)
+
+
+def hidden_products(own, pair, others, weights, out):
+    depth = own.shape[1]
+    total = None
+    for flip, block in enumerate((own, others, pair, others)):
+        left = block[flip // 2] if flip % 2 else block[...]
+        term = dot_of(left, weights[flip * depth : (flip + 1) * depth, :])
+        total = term if total is None else total + term
+    out[...] = jnp.square(jnp.maximum(total, 0.0)).astype(jnp.bfloat16)
+
+
+def first_hidden_kernel(place, own, pair, others, *rest):
     near, far, out, weights = rest[:4], rest[4:6], rest[6], rest[7]
     depth, half = near[0].shape
     for slot, piece in enumerate(near):
         rows = pl.ds(pl.multiple_of(place[slot] * depth, depth), depth)
         weights[rows, :half] = piece[...]
         weights[rows, half:] = far[0][...] if slot == 0 else far[1][slot - 1]
-    count = own_a.shape[0]
-    for group, (own, pair, others) in enumerate(((own_a, pair_a, others_a), (own_b, pair_b, others_b))):
-        total = jnp.zeros((count, 2 * half), jnp.float32)
-        for flip, block in enumerate((own, others, pair, others)):
-            left = block[flip // 2] if flip % 2 else block[...]
-            total += jnp.dot(
-                left, weights[flip * depth : (flip + 1) * depth, :], preferred_element_type=jnp.float32
-            )
-        out[group * count : (group + 1) * count, :] = jnp.square(jnp.maximum(total, 0.0)).astype(jnp.bfloat16)
+    hidden_products(own, pair, others, weights, out)
+
+
+def second_hidden_kernel(own, pair, others, weights, out):
+    hidden_products(own, pair, others, weights, out)
 
 
 def branch_products(hidden, weights, keep, give):
     for flip in (1, 3, 0, 2):
-        value = jnp.dot(hidden, weights[flip], preferred_element_type=jnp.float32)
+        value = dot_of(hidden, weights[flip])
         target = give if flip % 2 else keep
         target[flip // 2] = value.astype(target.dtype)
 
 
-def first_branch_kernel(count, place, hidden, *rest):
+def first_branch_kernel(place, hidden, *rest):
     near, far, keep, give, weights = rest[:4], rest[4:8], rest[8], rest[9], rest[10]
     half = near[0].shape[0]
+    tokens = keep.shape[1]
     for slot in range(len(near)):
         weights[place[slot], :half, :] = near[slot][...]
         weights[place[slot], half:, :] = far[slot][...]
-    branch_products(hidden[:count, :], weights, keep, give)
-
-
-def second_branch_kernel(count, hidden, weights, keep, give):
-    branch_products(hidden[count:, :], weights, keep, give)
-
-
-def local_call(kernel, outs, *operands, flops, scratch=()):
+    branch_products(hidden[tokens:, :], weights, keep, give)
+
+
+def second_branch_kernel(hidden, weights, keep, give):
+    branch_products(hidden[...], weights, keep, give)
+
+
+def third_branch_kernel(hidden, weights, keep, give):
+    branch_products(hidden[: keep.shape[1], :], weights, keep, give)
+
+
+def half_sum_kernel(keep, got, *outs):
+    blocks = len(outs) // 2
+    tokens = outs[0].shape[0]
+    for block in range(blocks):
+        rows = slice(block * tokens, (block + 1) * tokens)
+        for side in range(2):
+            out = outs[side * blocks + block]
+            out[...] = (keep[side, rows, :] + got[side, rows, :].astype(jnp.float32)).astype(out.dtype)
+
+
+def pair_sum_kernel(keep, got, out):
+    out[...] = (keep[...] + got[...].astype(jnp.float32)).astype(out.dtype)
+
+
+def local_call(kernel, outs, *operands, flops, scratch=(), room=8):
     specs = [
         pl.BlockSpec(memory_space=pltpu.SMEM if x.dtype == jnp.int32 else pltpu.VMEM) for x in operands
     ]
@@ -121,6 +150,7 @@
         in_specs=specs,
         out_specs=jax.tree.map(lambda _: pl.BlockSpec(memory_space=pltpu.VMEM), outs),
         scratch_shapes=scratch,
+        compiler_params=pltpu.CompilerParams(vmem_limit_bytes=room << 20),
         cost_estimate=pl.CostEstimate(flops=flops, bytes_accessed=1 << 20, transcendentals=0),
     )(*operands)
 
@@ -132,8 +162,14 @@
     part, row, column = lax.axis_index("grp"), lax.axis_index("fs"), lax.axis_index("tp")
     shifts = (1, 3, 2)
 
-    def along_rows(value, shift):
-        return lax.ppermute(value, "fs", [(i, (i + shift) % parts) for i in range(parts)])
+    def along_rows(value, shift, around=True):
+        moves = [(i, (i + shift) % parts) for i in range(parts)]
+        if not around:
+            moves = [(i, j) for i, j in moves if abs(i - j) < 3]
+        return lax.ppermute(value, "fs", moves)
+
+    def onward(value):
+        return lax.ppermute(value, "fs", [(1, 0), (parts - 2, parts - 1)])
 
     def across_parts(value):
         return lax.ppermute(value, "grp", [(0, 1), (1, 0)])
@@ -175,12 +211,11 @@
     widened = resid.astype(jnp.float32)
     power = jnp.sum(widened * widened, axis=1).reshape(-1, 128)
     power += across_columns(power, 1)
-    inverse = local_call(
-        functools.partial(inverse_kernel, parts * width),
-        jax.ShapeDtypeStruct(power.shape, jnp.float32),
-        power, across_columns(power, 2),
-        flops=1024,
-    )
+    small = jax.ShapeDtypeStruct(power.shape, jnp.float32)
+    energy = local_call(
+        functools.partial(mean_kernel, parts * width), small, power, across_columns(power, 2), flops=1024
+    )
+    inverse = local_call(inverse_kernel, small, energy, flops=1024)
 
     def up_piece(s, side):
         return columns_at(up_weight, ((row + s) % parts) * unit + side * (unit // 2), unit // 2)
@@ -195,50 +230,71 @@
     place = jnp.stack([column ^ ((row - s) % parts) for s in range(parts)]).astype(jnp.int32)
 
     pairs = {0: across_columns(scaled, 2)}
-    rows = {0: scaled} | {s: along_rows(scaled, s) for s in shifts}
+    rows = {0: scaled} | {s: along_rows(scaled, s, around=False) for s in shifts}
+    end = onward(rows[2])
+    rows[1] = jnp.where(row == 0, end, rows[1])
+    rows[3] = jnp.where(row == parts - 1, end, rows[3])
     pairs[2] = across_columns(rows[2], 2)
     odd = jnp.concatenate([rows[1], rows[3]])
     even = jnp.concatenate([rows[0], rows[2]])
     even_pair = jnp.concatenate([pairs[0], pairs[2]])
     odd_pair = across_columns(odd, 2)
-    even_others = across_columns(jnp.stack([even, even_pair]), 1)
+    even_both = jnp.stack([even, even_pair])
+    even_others = across_columns(even_both, 1)
     odd_others = across_columns(jnp.stack([odd, odd_pair]), 1)
-    flops = 2 * parts * tokens * parts * width * unit
-    hidden = local_call(
-        hidden_kernel,
-        jax.ShapeDtypeStruct((parts * tokens, unit), jnp.bfloat16),
-        place, even, even_pair, even_others, odd, odd_pair, odd_others,
+    flops = 4 * tokens * parts * width * unit
+    some = jax.ShapeDtypeStruct((2 * tokens, unit), jnp.bfloat16)
+    hidden_even, up_whole = local_call(
+        first_hidden_kernel,
+        (some, jax.ShapeDtypeStruct((parts * width, unit), jnp.bfloat16)),
+        place, even, even_pair, even_others,
         up_piece(0, part), up_near[1], up_near[2], up_near[3], up_piece(0, 1 - part), up_far,
         flops=flops,
-        scratch=[pltpu.VMEM((parts * width, unit), jnp.bfloat16)],
-    )
-    count = 2 * tokens
-    halves = (
-        jax.ShapeDtypeStruct((2, count, width), jnp.float32),
-        jax.ShapeDtypeStruct((2, count, width), jnp.bfloat16),
-    )
-    keep_a, give_a, down_whole = local_call(
-        functools.partial(first_branch_kernel, count),
-        (*halves, jax.ShapeDtypeStruct((parts, unit, width), jnp.bfloat16)),
-        place, hidden,
+        room=14,
+    )
+    hidden_odd = local_call(second_hidden_kernel, some, odd, odd_pair, odd_others, up_whole, flops=flops, room=14)
+
+    def halves(count):
+        shape = (2, count, width)
+        return jax.ShapeDtypeStruct(shape, jnp.float32), jax.ShapeDtypeStruct(shape, jnp.bfloat16)
+
+    keep_two, give_two, down_whole = local_call(
+        first_branch_kernel,
+        (*halves(tokens), jax.ShapeDtypeStruct((parts, unit, width), jnp.bfloat16)),
+        place, hidden_even,
         down_piece(0, part), down_near[1], down_near[2], down_near[3],
         down_piece(0, 1 - part), down_far[1], down_far[2], down_far[3],
         flops=flops // 2,
-    )
-    keep_b, give_b = local_call(
-        functools.partial(second_branch_kernel, count), halves, hidden, down_whole, flops=flops // 2
-    )
-    got_a = across_columns(give_a, 1)
-    got_b = across_columns(give_b, 1)
-    even_give = (keep_a[1] + got_a[1]).astype(jnp.bfloat16)
-    odd_give = (keep_b[1] + got_b[1]).astype(jnp.bfloat16)
-    even_keep, odd_keep = keep_a[0] + got_a[0], keep_b[0] + got_b[0]
-    two = even_keep[tokens:] + across_columns(even_give[tokens:], 2)
-    odd_sum = (odd_keep + across_columns(odd_give, 2)).astype(jnp.bfloat16)
-    branch = even_keep[:tokens] + across_columns(even_give[:tokens], 2)
-    branch += along_rows(two.astype(jnp.bfloat16), -2)
-    branch += along_rows(odd_sum[:tokens], -1)
-    branch += along_rows(odd_sum[tokens:], -3)
+        room=14,
+    )
+    keep_odd, give_odd = local_call(
+        second_branch_kernel, halves(2 * tokens), hidden_odd, down_whole, flops=flops, room=14
+    )
+    keep_own, give_own = local_call(
+        third_branch_kernel, halves(tokens), hidden_even, down_whole, flops=flops // 2, room=14
+    )
+
+    block = (tokens, width)
+
+    def halved(keep, give):
+        blocks = keep.shape[1] // tokens
+        outs = [jax.ShapeDtypeStruct(block, kind) for kind in (jnp.float32, jnp.bfloat16) for _ in range(blocks)]
+        return local_call(half_sum_kernel, outs, keep, across_columns(give, 1), flops=1024)
+
+    def summed(keep, give):
+        out = jax.ShapeDtypeStruct(block, jnp.bfloat16)
+        return local_call(pair_sum_kernel, out, keep, across_columns(give, 2), flops=1024)
+
+    keep_two, give_two = halved(keep_two, give_two)
+    keep_one, keep_three, give_one, give_three = halved(keep_odd, give_odd)
+    keep_own, give_own = halved(keep_own, give_own)
+    two = summed(keep_two, give_two)
+    one = summed(keep_one, give_one)
+    three = summed(keep_three, give_three)
+    branch = keep_own + across_columns(give_own, 2)
+    branch += along_rows(two, -2)
+    branch += along_rows(one, -1)
+    branch += along_rows(three, -3)
     return (widened + branch * inverse.reshape(tokens, 1)).astype(jnp.bfloat16)
 
 

time: 202 us -> 173 us (0.86)
  Pallas kernels: 27.7 us -> 10.4 us
  starting transfers between devices: 58.8 us -> 51 us
  waiting for transfers between devices: 97.1 us -> 104 us
  local copies, waits for them, and re-layouts: 11.6 us -> 5.32 us
  other arithmetic: 4.85 us -> 1.53 us
    pallas_call x8 -> x17, Pallas kernels: 27.7 us -> 10.4 us  [local_call(): pl.pallas_call(kernel, out_shape=outs, in_specs=specs, out_specs=jax.tree...]
    ppermute x7, waiting for transfers between devices: 3.67 us -> 14.2 us  [across_parts(): return lax.ppermute(value, 'grp', [(0, 1), (1, 0)])]
    ppermute x15 -> x16, starting transfers between devices: 37.2 us -> 30.4 us  [the longest x15 29.2 us: along_rows(): return lax.ppermute(value, 'fs', moves)]
    unnamed x71 -> x10, local copies, waits for them, and re-layouts: 6.72 us -> 2.03 us
    ppermute x15 -> x16, waiting for transfers between devices: 64.1 us -> 60.3 us  [the longest x15 52.7 us: along_rows(): return lax.ppermute(value, 'fs', moves)]
    convert_element_type x4 -> x0, other arithmetic: 2.17 us -> none  [the longest x1 1.42 us: gathered_tokens(): odd_give = (keep_b[1] + got_b[1]).astype(jnp.bfloat16)]
    ppermute x15 -> x17, starting transfers between devices: 12.6 us -> 10.8 us  [across_columns(): return lax.ppermute(value, 'tp', [(i, i ^ flip) for i in range(parts)])]
    ppermute x15 -> x17, waiting for transfers between devices: 29.4 us -> 29.3 us  [across_columns(): return lax.ppermute(value, 'tp', [(i, i ^ flip) for i in range(parts)])]
  transfers between devices with their start and end apart: 37 -> 40, of which waited for: 18 -> 22; matrix products, arithmetic and copies ran while one was open for 4% -> 2% of each run, Pallas kernels for 8% -> 4%
where the time goes in v2:
time: 173 us; the launch traced here: 172 us
  waiting for transfers between devices  104 us (60%)
  starting transfers between devices  51 us (29%)
  Pallas kernels  10.4 us (6%)
  local copies, waits for them, and re-layouts  5.32 us (3%)
    ppermute x15, waiting for transfers between devices, along_rows(): return lax.ppermute(value, 'fs', moves)  52.7 us
    ppermute x17, waiting for transfers between devices, across_columns(): return lax.ppermute(value, 'tp', [(i, i ^ flip) for i in range(parts)])  29.3 us
    ppermute x15, starting transfers between devices, along_rows(): return lax.ppermute(value, 'fs', moves)  29.2 us
    ppermute x7, waiting for transfers between devices, across_parts(): return lax.ppermute(value, 'grp', [(0, 1), (1, 0)])  14.2 us
    ppermute x17, starting transfers between devices, across_columns(): return lax.ppermute(value, 'tp', [(i, i ^ flip) for i in range(parts)])  10.8 us
    pallas_call x17, Pallas kernels, local_call(): pl.pallas_call(kernel, out_shape=outs, in_specs=specs, out_specs=jax.tree...  10.4 us
    ppermute x7, starting transfers between devices, across_parts(): return lax.ppermute(value, 'grp', [(0, 1), (1, 0)])  9.77 us
    ppermute x1, waiting for transfers between devices, onward(): return lax.ppermute(value, 'fs', [(1, 0), (parts - 2, parts - 1)])  7.6 us
  transfers between devices with their start and end apart: 40, of which 22 were waited for; matrix products, arithmetic and copies ran while one was open for 2% of the time, Pallas kernels for 4%

profile of v2, /device:TPU:0, one launch (start us, length us, event | category | flops | bytes accessed | tf_op | source)
XLA Modules:
  0.0 172.4 jit_solution(13649725908747003087)
XLA Ops:
  1.0 3.1 %collective-permute-start.3 = (bf16[512,256]{1,0:T(8,128)(2,1)S(1)}, bf16[512,256]{1,0:T(8,128)(2,1)S(1)}, u32[]{:S(2)}, u32[]{:S(2)}) collective-permute-start(bf16[512,256]{1,0:T(8,128)(2,1)S(1)} %constant_dynamic-slice_fusion.10), channel_id=1, source_target_pairs={{0,4},{4,8},{8,12},{12,0},{1,5},{5,9},{9,13},{13,1},{2,6},{6,10},{... | collective-permute-start | bytes 786440 | tf_op jit(solution)/shard_map/ppermute | solution.py:169
  4.1 2.2 %collective-permute-start.7 = (bf16[512,256]{1,0:T(8,128)(2,1)S(1)}, bf16[512,256]{1,0:T(8,128)(2,1)S(1)}, u32[]{:S(2)}, u32[]{:S(2)}) collective-permute-start(bf16[512,256]{1,0:T(8,128)(2,1)S(1)} %constant_dynamic-slice_fusion.10), channel_id=1, source_target_pairs={{0,12},{4,0},{8,4},{12,8},{1,13},{5,1},{9,5},{13,9},{2,14},{6,2},{... | collective-permute-start | bytes 786440 | tf_op jit(solution)/shard_map/ppermute | solution.py:169
  8.6 4.7 %collective-permute-done.3.piece = bf16[512,256]{1,0:T(8,128)(2,1)S(1)} collective-permute-done((bf16[512,256]{1,0:T(8,128)(2,1)S(1)}, bf16[512,256]{1,0:T(8,128)(2,1)S(1)}, u32[]{:S(2)}, u32[]{:S(2)}) %collective-permute-start.3) | collective-permute-done | bytes 262176 | tf_op jit(solution)/shard_map/ppermute | solution.py:169
  15.0 3.0 %collective-permute-done.7.piece = bf16[512,256]{1,0:T(8,128)(2,1)S(1)} collective-permute-done((bf16[512,256]{1,0:T(8,128)(2,1)S(1)}, bf16[512,256]{1,0:T(8,128)(2,1)S(1)}, u32[]{:S(2)}, u32[]{:S(2)}) %collective-permute-start.7) | collective-permute-done | bytes 262176 | tf_op jit(solution)/shard_map/ppermute | solution.py:169
  19.5 9.7 %collective-permute-done.4.piece2 = bf16[512,256]{1,0:T(8,128)(2,1)S(1)} collective-permute-done((bf16[512,256]{1,0:T(8,128)(2,1)S(1)}, bf16[512,256]{1,0:T(8,128)(2,1)S(1)}, u32[]{:S(2)}, u32[]{:S(2)}) %collective-permute-start.4) | collective-permute-done | bytes 262176 | tf_op jit(solution)/shard_map/ppermute | solution.py:169
  38.3 7.8 %collective-permute-start.9 = (bf16[256,512]{1,0:T(8,128)(2,1)S(1)}, bf16[256,512]{1,0:T(8,128)(2,1)S(1)}, u32[]{:S(2)}, u32[]{:S(2)}) collective-permute-start(bf16[256,512]{1,0:T(8,128)(2,1)S(1)} %get-tuple-element.35), channel_id=1, source_target_pairs={{0,8},{4,12},{8,0},{12,4},{1,9},{5,13},{9,1},{13,5},{2,10},{6,14},... | collective-permute-start | bytes 786440 | tf_op jit(solution)/shard_map/ppermute | solution.py:169
  48.7 10.2 %collective-permute-done.9 = bf16[256,512]{1,0:T(8,128)(2,1)S(1)} collective-permute-done((bf16[256,512]{1,0:T(8,128)(2,1)S(1)}, bf16[256,512]{1,0:T(8,128)(2,1)S(1)}, u32[]{:S(2)}, u32[]{:S(2)}) %collective-permute-start.9) | collective-permute-done | bytes 262176 | tf_op jit(solution)/shard_map/ppermute | solution.py:169
  61.6 2.7 %collective-permute-start.13 = (bf16[512,256]{1,0:T(8,128)(2,1)S(1)}, bf16[512,256]{1,0:T(8,128)(2,1)S(1)}, u32[]{:S(2)}, u32[]{:S(2)}) collective-permute-start(bf16[512,256]{1,0:T(8,128)(2,1)S(1)} %get-tuple-element.60), channel_id=1, source_target_pairs={{0,4},{4,8},{8,12},{12,0},{1,5},{5,9},{9,13},{13,1},{2,6},{6,10},{... | collective-permute-start | bytes 786440 | tf_op jit(solution)/shard_map/ppermute | solution.py:169
  64.3 2.5 %collective-permute-start.15 = (bf16[512,256]{1,0:T(8,128)(2,1)S(1)}, bf16[512,256]{1,0:T(8,128)(2,1)S(1)}, u32[]{:S(2)}, u32[]{:S(2)}) collective-permute-start(bf16[512,256]{1,0:T(8,128)(2,1)S(1)} %get-tuple-element.62), channel_id=1, source_target_pairs={{0,12},{4,0},{8,4},{12,8},{1,13},{5,1},{9,5},{13,9},{2,14},{6,2},{... | collective-permute-start | bytes 786440 | tf_op jit(solution)/shard_map/ppermute | solution.py:169
  68.1 7.6 %collective-permute-done.28 = bf16[256,512]{1,0:T(8,128)(2,1)S(1)} collective-permute-done((bf16[256,512]{1,0:T(8,128)(2,1)S(1)}, bf16[256,512]{1,0:T(8,128)(2,1)S(1)}, u32[]{:S(2)}, u32[]{:S(2)}) %collective-permute-start.28) | collective-permute-done | bytes 262176 | tf_op jit(solution)/shard_map/ppermute | solution.py:172
  78.0 6.9 %collective-permute-done.11 = bf16[256,512]{1,0:T(8,128)(2,1)S(1)} collective-permute-done((bf16[256,512]{1,0:T(8,128)(2,1)S(1)}, bf16[256,512]{1,0:T(8,128)(2,1)S(1)}, u32[]{:S(2)}, u32[]{:S(2)}) %collective-permute-start.11) | collective-permute-done | bytes 262176 | tf_op jit(solution)/shard_map/ppermute | solution.py:178
  87.2 5.5 %collective-permute-done.31.pair = bf16[512,512]{1,0:T(8,128)(2,1)S(1)} collective-permute-done((bf16[512,512]{1,0:T(8,128)(2,1)S(1)}, bf16[512,512]{1,0:T(8,128)(2,1)S(1)}, u32[]{:S(2)}, u32[]{:S(2)}) %collective-permute-start.31) | collective-permute-done | bytes 524320 | tf_op jit(solution)/shard_map/ppermute | solution.py:178
  93.4 10.8 %collective-permute-done.17.rest_1_ = bf16[256,512]{1,0:T(8,128)(2,1)S(1)} collective-permute-done((bf16[256,512]{1,0:T(8,128)(2,1)S(1)}, bf16[256,512]{1,0:T(8,128)(2,1)S(1)}, u32[]{:S(2)}, u32[]{:S(2)}) %collective-permute-start.17) | collective-permute-done | bytes 262176 | tf_op jit(solution)/shard_map/ppermute | solution.py:169
  104.2 10.4 %collective-permute-done.18.rest_2_ = bf16[256,512]{1,0:T(8,128)(2,1)S(1)} collective-permute-done((bf16[256,512]{1,0:T(8,128)(2,1)S(1)}, bf16[256,512]{1,0:T(8,128)(2,1)S(1)}, u32[]{:S(2)}, u32[]{:S(2)}) %collective-permute-start.18) | collective-permute-done | bytes 262176 | tf_op jit(solution)/shard_map/ppermute | solution.py:169
  120.3 3.5 %collective-permute-done.20.rest_5_ = bf16[256,512]{1,0:T(8,128)(2,1)S(1)} collective-permute-done((bf16[256,512]{1,0:T(8,128)(2,1)S(1)}, bf16[256,512]{1,0:T(8,128)(2,1)S(1)}, u32[]{:S(2)}, u32[]{:S(2)}) %collective-permute-start.20) | collective-permute-done | bytes 262176 | tf_op jit(solution)/shard_map/ppermute | solution.py:175
  123.8 5.6 %collective-permute-done.21.rest_6_ = bf16[256,512]{1,0:T(8,128)(2,1)S(1)} collective-permute-done((bf16[256,512]{1,0:T(8,128)(2,1)S(1)}, bf16[256,512]{1,0:T(8,128)(2,1)S(1)}, u32[]{:S(2)}, u32[]{:S(2)}) %collective-permute-start.21) | collective-permute-done | bytes 262176 | tf_op jit(solution)/shard_map/ppermute | solution.py:175
  129.4 3.8 %collective-permute-done.22.rest_7_ = bf16[256,512]{1,0:T(8,128)(2,1)S(1)} collective-permute-done((bf16[256,512]{1,0:T(8,128)(2,1)S(1)}, bf16[256,512]{1,0:T(8,128)(2,1)S(1)}, u32[]{:S(2)}, u32[]{:S(2)}) %collective-permute-start.22) | collective-permute-done | bytes 262176 | tf_op jit(solution)/shard_map/ppermute | solution.py:175
  138.5 2.0 %collective-permute-done.25.got = bf16[2,256,512]{2,1,0:T(8,128)(2,1)S(1)} collective-permute-done((bf16[2,256,512]{2,1,0:T(8,128)(2,1)S(1)}, bf16[2,256,512]{2,1,0:T(8,128)(2,1)S(1)}, u32[]{:S(2)}, u32[]{:S(2)}) %collective-permute-start.25) | collective-permute-done | bytes 524320 | tf_op jit(solution)/shard_map/ppermute | solution.py:178
  145.2 4.7 %collective-permute-done.26.got = bf16[256,512]{1,0:T(8,128)(2,1)S(1)} collective-permute-done((bf16[256,512]{1,0:T(8,128)(2,1)S(1)}, bf16[256,512]{1,0:T(8,128)(2,1)S(1)}, u32[]{:S(2)}, u32[]{:S(2)}) %collective-permute-start.26) | collective-permute-done | bytes 262176 | tf_op jit(solution)/shard_map/ppermute | solution.py:178
  150.0 5.5 %collective-permute-done.34.got = bf16[256,512]{1,0:T(8,128)(2,1)S(1)} collective-permute-done((bf16[256,512]{1,0:T(8,128)(2,1)S(1)}, bf16[256,512]{1,0:T(8,128)(2,1)S(1)}, u32[]{:S(2)}, u32[]{:S(2)}) %collective-permute-start.34) | collective-permute-done | bytes 262176 | tf_op jit(solution)/shard_map/ppermute | solution.py:178
  155.6 4.9 %collective-permute-start.35 = (bf16[256,512]{1,0:T(8,128)(2,1)S(1)}, bf16[256,512]{1,0:T(8,128)(2,1)S(1)}, u32[]{:S(2)}, u32[]{:S(2)}) collective-permute-start(bf16[256,512]{1,0:T(8,128)(2,1)S(1)} %shard_map.77), channel_id=1, source_target_pairs={{0,12},{4,0},{8,4},{12,8},{1,13},{5,1},{9,5},{13,9},{2,14},{6,2},{... | collective-permute-start | bytes 786440 | tf_op jit(solution)/shard_map/ppermute | solution.py:169
  161.2 2.1 %collective-permute-start.37 = (bf16[256,512]{1,0:T(8,128)(2,1)S(1)}, bf16[256,512]{1,0:T(8,128)(2,1)S(1)}, u32[]{:S(2)}, u32[]{:S(2)}) collective-permute-start(bf16[256,512]{1,0:T(8,128)(2,1)S(1)} %shard_map.78), channel_id=1, source_target_pairs={{0,4},{4,8},{8,12},{12,0},{1,5},{5,9},{9,13},{13,1},{2,6},{6,10},{... | collective-permute-start | bytes 786440 | tf_op jit(solution)/shard_map/ppermute | solution.py:169
  165.4 2.9 %collective-permute-done.39.two = f32[2,128]{1,0:T(2,128)S(1)} collective-permute-done((f32[2,128]{1,0:T(2,128)S(1)}, f32[2,128]{1,0:T(2,128)S(1)}, u32[]{:S(2)}, u32[]{:S(2)}) %collective-permute-start.39) | collective-permute-done | bytes 1056 | tf_op jit(solution)/shard_map/ppermute | solution.py:178
  168.3 3.2 %collective-permute-done.35 = bf16[256,512]{1,0:T(8,128)(2,1)S(1)} collective-permute-done((bf16[256,512]{1,0:T(8,128)(2,1)S(1)}, bf16[256,512]{1,0:T(8,128)(2,1)S(1)}, u32[]{:S(2)}, u32[]{:S(2)}) %collective-permute-start.35) | collective-permute-done | bytes 262176 | tf_op jit(solution)/shard_map/ppermute | solution.py:169
  (99 shorter events, 46.7 us)
Async XLA Ops:
  4.1 13.9 %collective-permute-start.7 = (bf16[512,256]{1,0:T(8,128)(2,1)S(1)}, bf16[512,256]{1,0:T(8,128)(2,1)S(1)}, u32[]{:S(2)}, u32[]{:S(2)}) collective-permute-start(bf16[512,256]{1,0:T(8,128)(2,1)S(1)} %constant_dynamic-slice_fusion.10), channel_id=1, source_target_pairs={{0,12},{4,0},{8,4},{12,8},{1,13},{5,1},{9,5},{13,9},{2,14},{6,2},{... | collective-permute-start | bytes 786440 | tf_op jit(solution)/shard_map/ppermute | solution.py:169
  6.2 23.0 %collective-permute-start.4 = (bf16[512,256]{1,0:T(8,128)(2,1)S(1)}, bf16[512,256]{1,0:T(8,128)(2,1)S(1)}, u32[]{:S(2)}, u32[]{:S(2)}) collective-permute-start(bf16[512,256]{1,0:T(8,128)(2,1)S(1)} %constant_dynamic-slice_fusion.10), channel_id=1, source_target_pairs={{0,8},{4,12},{8,0},{12,4},{1,9},{5,13},{9,1},{13,5},{2,10},{6,14},... | collective-permute-start | bytes 786440 | tf_op jit(solution)/shard_map/ppermute | solution.py:169
  7.1 24.4 %collective-permute-start.1 = (bf16[256,512]{1,0:T(8,128)(2,1)}, bf16[256,512]{1,0:T(8,128)(2,1)S(1)}, u32[]{:S(2)}, u32[]{:S(2)}) collective-permute-start(bf16[256,512]{1,0:T(8,128)(2,1)} %mixed.1), channel_id=1, source_target_pairs={{0,2},{1,3},{2,0},{3,1},{4,6},{5,7},{6,4},{7,5},{8,10},{9,11},{10,... | collective-permute-start | bytes 786440 | tf_op jit(solution)/shard_map/ppermute | solution.py:178
  13.3 18.2 %collective-permute-start.2 = (bf16[256,512]{1,0:T(8,128)(2,1)}, bf16[256,512]{1,0:T(8,128)(2,1)S(1)}, u32[]{:S(2)}, u32[]{:S(2)}) collective-permute-start(bf16[256,512]{1,0:T(8,128)(2,1)} %mixed.1), channel_id=1, source_target_pairs={{0,3},{1,2},{2,1},{3,0},{4,7},{5,6},{6,5},{7,4},{8,11},{9,10},{10,... | collective-permute-start | bytes 786440 | tf_op jit(solution)/shard_map/ppermute | solution.py:178
  13.3 22.0 %collective-permute-start.6 = (bf16[512,256]{1,0:T(8,128)(2,1)S(1)}, bf16[512,256]{1,0:T(8,128)(2,1)S(1)}, u32[]{:S(2)}, u32[]{:S(2)}) collective-permute-start(bf16[512,256]{1,0:T(8,128)(2,1)S(1)} %collective-permute-done.3.piece), channel_id=1, source_target_pairs={{0,16},{16,0},{1,17},{17,1},{2,18},{18,2},{3,19},{19,3},{4,20},{20... | collective-permute-start | bytes 786440 | tf_op jit(solution)/shard_map/ppermute | solution.py:175
  18.0 17.3 %collective-permute-start.8 = (bf16[512,256]{1,0:T(8,128)(2,1)S(1)}, bf16[512,256]{1,0:T(8,128)(2,1)S(1)}, u32[]{:S(2)}, u32[]{:S(2)}) collective-permute-start(bf16[512,256]{1,0:T(8,128)(2,1)S(1)} %collective-permute-done.7.piece), channel_id=1, source_target_pairs={{0,16},{16,0},{1,17},{17,1},{2,18},{18,2},{3,19},{19,3},{4,20},{20... | collective-permute-start | bytes 786440 | tf_op jit(solution)/shard_map/ppermute | solution.py:175
  38.3 20.6 %collective-permute-start.9 = (bf16[256,512]{1,0:T(8,128)(2,1)S(1)}, bf16[256,512]{1,0:T(8,128)(2,1)S(1)}, u32[]{:S(2)}, u32[]{:S(2)}) collective-permute-start(bf16[256,512]{1,0:T(8,128)(2,1)S(1)} %get-tuple-element.35), channel_id=1, source_target_pairs={{0,8},{4,12},{8,0},{12,4},{1,9},{5,13},{9,1},{13,5},{2,10},{6,14},... | collective-permute-start | bytes 786440 | tf_op jit(solution)/shard_map/ppermute | solution.py:169
  46.1 18.2 %collective-permute-start.29 = (bf16[256,512]{1,0:T(8,128)(2,1)S(1)}, bf16[256,512]{1,0:T(8,128)(2,1)S(1)}, u32[]{:S(2)}, u32[]{:S(2)}) collective-permute-start(bf16[256,512]{1,0:T(8,128)(2,1)S(1)} %get-tuple-element.35), channel_id=1, source_target_pairs={{0,4},{4,8},{8,12},{1,5},{5,9},{9,13},{2,6},{6,10},{10,14},{3,7},{... | collective-permute-start | bytes 786440 | tf_op jit(solution)/shard_map/ppermute | solution.py:169
  47.4 19.4 %collective-permute-start.30 = (bf16[256,512]{1,0:T(8,128)(2,1)S(1)}, bf16[256,512]{1,0:T(8,128)(2,1)S(1)}, u32[]{:S(2)}, u32[]{:S(2)}) collective-permute-start(bf16[256,512]{1,0:T(8,128)(2,1)S(1)} %get-tuple-element.35), channel_id=1, source_target_pairs={{4,0},{8,4},{12,8},{5,1},{9,5},{13,9},{6,2},{10,6},{14,10},{7,3},{... | collective-permute-start | bytes 786440 | tf_op jit(solution)/shard_map/ppermute | solution.py:169
  58.9 16.8 %collective-permute-start.28 = (bf16[256,512]{1,0:T(8,128)(2,1)S(1)}, bf16[256,512]{1,0:T(8,128)(2,1)S(1)}, u32[]{:S(2)}, u32[]{:S(2)}) collective-permute-start(bf16[256,512]{1,0:T(8,128)(2,1)S(1)} %collective-permute-done.9), channel_id=1, source_target_pairs={{4,0},{8,12},{5,1},{9,13},{6,2},{10,14},{7,3},{11,15},{20,16},{24,... | collective-permute-start | bytes 786440 | tf_op jit(solution)/shard_map/ppermute | solution.py:172
  61.6 23.5 %collective-permute-start.13 = (bf16[512,256]{1,0:T(8,128)(2,1)S(1)}, bf16[512,256]{1,0:T(8,128)(2,1)S(1)}, u32[]{:S(2)}, u32[]{:S(2)}) collective-permute-start(bf16[512,256]{1,0:T(8,128)(2,1)S(1)} %get-tuple-element.60), channel_id=1, source_target_pairs={{0,4},{4,8},{8,12},{12,0},{1,5},{5,9},{9,13},{13,1},{2,6},{6,10},{... | collective-permute-start | bytes 786440 | tf_op jit(solution)/shard_map/ppermute | solution.py:169
  64.3 20.8 %collective-permute-start.14 = (bf16[512,256]{1,0:T(8,128)(2,1)S(1)}, bf16[512,256]{1,0:T(8,128)(2,1)S(1)}, u32[]{:S(2)}, u32[]{:S(2)}) collective-permute-start(bf16[512,256]{1,0:T(8,128)(2,1)S(1)} %get-tuple-element.59), channel_id=1, source_target_pairs={{0,8},{4,12},{8,0},{12,4},{1,9},{5,13},{9,1},{13,5},{2,10},{6,14},... | collective-permute-start | bytes 786440 | tf_op jit(solution)/shard_map/ppermute | solution.py:169
  64.3 21.3 %collective-permute-start.15 = (bf16[512,256]{1,0:T(8,128)(2,1)S(1)}, bf16[512,256]{1,0:T(8,128)(2,1)S(1)}, u32[]{:S(2)}, u32[]{:S(2)}) collective-permute-start(bf16[512,256]{1,0:T(8,128)(2,1)S(1)} %get-tuple-element.62), channel_id=1, source_target_pairs={{0,12},{4,0},{8,4},{12,8},{1,13},{5,1},{9,5},{13,9},{2,14},{6,2},{... | collective-permute-start | bytes 786440 | tf_op jit(solution)/shard_map/ppermute | solution.py:169
  77.0 15.8 %collective-permute-start.31 = (bf16[512,512]{1,0:T(8,128)(2,1)S(1)}, bf16[512,512]{1,0:T(8,128)(2,1)S(1)}, u32[]{:S(2)}, u32[]{:S(2)}) collective-permute-start(bf16[512,512]{1,0:T(8,128)(2,1)S(1)} %get-tuple-element.64.own), channel_id=1, source_target_pairs={{0,2},{1,3},{2,0},{3,1},{4,6},{5,7},{6,4},{7,5},{8,10},{9,11},{10,... | collective-permute-start | bytes 1572872 | tf_op jit(solution)/shard_map/ppermute | solution.py:178
  85.0 33.3 %collective-permute-start.12 = (bf16[2,512,512]{2,1,0:T(8,128)(2,1)S(1)}, bf16[2,512,512]{2,1,0:T(8,128)(2,1)S(1)}, u32[]{:S(2)}, u32[]{:S(2)}) collective-permute-start(bf16[2,512,512]{2,1,0:T(8,128)(2,1)S(1)} %pad_maximum_fusion), channel_id=1, source_target_pairs={{0,1},{1,0},{2,3},{3,2},{4,5},{5,4},{6,7},{7,6},{8,9},{9,8},{10,11... | collective-permute-start | bytes 3145736 | tf_op jit(solution)/shard_map/ppermute | solution.py:178
  85.7 32.0 %collective-permute-start.16 = (bf16[3,512,256]{2,1,0:T(8,128)(2,1)S(1)}, bf16[3,512,256]{2,1,0:T(8,128)(2,1)S(1)}, u32[]{:S(2)}, u32[]{:S(2)}) collective-permute-start(bf16[3,512,256]{2,1,0:T(8,128)(2,1)S(1)} %pad_maximum_fusion.2), channel_id=1, source_target_pairs={{0,16},{16,0},{1,17},{17,1},{2,18},{18,2},{3,19},{19,3},{4,20},{20... | collective-permute-start | bytes 2359304 | tf_op jit(solution)/shard_map/ppermute | solution.py:175
  92.9 41.7 %collective-permute-start.32 = (bf16[2,512,512]{2,1,0:T(8,128)(2,1)S(1)}, bf16[2,512,512]{2,1,0:T(8,128)(2,1)S(1)}, u32[]{:S(2)}, u32[]{:S(2)}) collective-permute-start(bf16[2,512,512]{2,1,0:T(8,128)(2,1)S(1)} %pad_maximum_fusion.1), channel_id=1, source_target_pairs={{0,1},{1,0},{2,3},{3,2},{4,5},{5,4},{6,7},{7,6},{8,9},{9,8},{10,11... | collective-permute-start | bytes 3145736 | tf_op jit(solution)/shard_map/ppermute | solution.py:178
  93.2 21.4 %collective-permute-start.18 = (bf16[256,512]{1,0:T(8,128)(2,1)S(1)}, bf16[256,512]{1,0:T(8,128)(2,1)S(1)}, u32[]{:S(2)}, u32[]{:S(2)}) collective-permute-start(bf16[256,512]{1,0:T(8,128)(2,1)S(1)} %get-tuple-element.54), channel_id=1, source_target_pairs={{0,8},{4,12},{8,0},{12,4},{1,9},{5,13},{9,1},{13,5},{2,10},{6,14},... | collective-permute-start | bytes 786440 | tf_op jit(solution)/shard_map/ppermute | solution.py:169
  117.7 15.5 %collective-permute-start.22 = (bf16[256,512]{1,0:T(8,128)(2,1)S(1)}, bf16[256,512]{1,0:T(8,128)(2,1)S(1)}, u32[]{:S(2)}, u32[]{:S(2)}) collective-permute-start(bf16[256,512]{1,0:T(8,128)(2,1)S(1)} %collective-permute-done.19.rest_3_), channel_id=1, source_target_pairs={{0,16},{16,0},{1,17},{17,1},{2,18},{18,2},{3,19},{19,3},{4,20},{20... | collective-permute-start | bytes 786440 | tf_op jit(solution)/shard_map/ppermute | solution.py:175
  141.8 13.7 %collective-permute-start.34 = (bf16[256,512]{1,0:T(8,128)(2,1)S(1)}, bf16[256,512]{1,0:T(8,128)(2,1)S(1)}, u32[]{:S(2)}, u32[]{:S(2)}) collective-permute-start(bf16[256,512]{1,0:T(8,128)(2,1)S(1)} %get-tuple-element.50), channel_id=1, source_target_pairs={{0,2},{1,3},{2,0},{3,1},{4,6},{5,7},{6,4},{7,5},{8,10},{9,11},{10,... | collective-permute-start | bytes 786440 | tf_op jit(solution)/shard_map/ppermute | solution.py:178
  143.0 18.1 %collective-permute-start.36 = (bf16[256,512]{1,0:T(8,128)(2,1)S(1)}, bf16[256,512]{1,0:T(8,128)(2,1)S(1)}, u32[]{:S(2)}, u32[]{:S(2)}) collective-permute-start(bf16[256,512]{1,0:T(8,128)(2,1)S(1)} %get-tuple-element.52), channel_id=1, source_target_pairs={{0,2},{1,3},{2,0},{3,1},{4,6},{5,7},{6,4},{7,5},{8,10},{9,11},{10,... | collective-permute-start | bytes 786440 | tf_op jit(solution)/shard_map/ppermute | solution.py:178
  144.0 24.2 %collective-permute-start.24 = (bf16[256,512]{1,0:T(8,128)(2,1)S(1)}, bf16[256,512]{1,0:T(8,128)(2,1)S(1)}, u32[]{:S(2)}, u32[]{:S(2)}) collective-permute-start(bf16[256,512]{1,0:T(8,128)(2,1)S(1)} %get-tuple-element.41), channel_id=1, source_target_pairs={{0,2},{1,3},{2,0},{3,1},{4,6},{5,7},{6,4},{7,5},{8,10},{9,11},{10,... | collective-permute-start | bytes 786440 | tf_op jit(solution)/shard_map/ppermute | solution.py:178
  149.9 18.3 %collective-permute-start.27 = (bf16[256,512]{1,0:T(8,128)(2,1)S(1)}, bf16[256,512]{1,0:T(8,128)(2,1)S(1)}, u32[]{:S(2)}, u32[]{:S(2)}) collective-permute-start(bf16[256,512]{1,0:T(8,128)(2,1)S(1)} %shard_map.73), channel_id=1, source_target_pairs={{0,8},{4,12},{8,0},{12,4},{1,9},{5,13},{9,1},{13,5},{2,10},{6,14},... | collective-permute-start | bytes 786440 | tf_op jit(solution)/shard_map/ppermute | solution.py:169
  155.6 15.9 %collective-permute-start.35 = (bf16[256,512]{1,0:T(8,128)(2,1)S(1)}, bf16[256,512]{1,0:T(8,128)(2,1)S(1)}, u32[]{:S(2)}, u32[]{:S(2)}) collective-permute-start(bf16[256,512]{1,0:T(8,128)(2,1)S(1)} %shard_map.77), channel_id=1, source_target_pairs={{0,12},{4,0},{8,4},{12,8},{1,13},{5,1},{9,5},{13,9},{2,14},{6,2},{... | collective-permute-start | bytes 786440 | tf_op jit(solution)/shard_map/ppermute | solution.py:169
  (20 other events, 145.6 us)

commit v3 on v2

v3 whole, which is shorter than its diff:
```python
import functools

import jax
import jax.numpy as jnp
from jax import lax
from jax.experimental import pallas as pl
from jax.experimental.pallas import tpu as pltpu
from jax.sharding import PartitionSpec as P

epsilon = 1e-06


def fold_product(left, portion):
    return jnp.dot(left, portion, preferred_element_type=jnp.float32)


def gathered_weights(stream, mixed, out_weight, norm_gain, up_weight, down_weight):
    mixed_whole = lax.all_gather(mixed, "tp", axis=1, tiled=True)
    projected = fold_product(mixed_whole, lax.all_gather(out_weight, "fs", axis=0, tiled=True))
    resid = (stream.astype(jnp.float32) + projected).astype(jnp.bfloat16)
    widened = resid.astype(jnp.float32)
    resid_whole, gain_whole = (
        lax.all_gather(resid, "tp", axis=1, tiled=True),
        lax.all_gather(norm_gain, "tp", axis=0, tiled=True),
    )
    stream_wide = resid_whole.astype(jnp.float32)
    energy = jnp.mean(stream_wide * stream_wide, axis=1, keepdims=True)
    normed_whole = (
        stream_wide * lax.rsqrt(energy + epsilon) * gain_whole.astype(jnp.float32)
    ).astype(jnp.bfloat16)
    up_full = lax.all_gather(up_weight, "fs", axis=0, tiled=True)
    up_values = fold_product(normed_whole, up_full)
    activated = jnp.square(jax.nn.relu(up_values)).astype(jnp.bfloat16)
    partials = fold_product(activated, lax.all_gather(down_weight, "fs", axis=1, tiled=True))
    branch = lax.psum_scatter(partials, "tp", scatter_dimension=1, tiled=True)
    return (widened + branch).astype(jnp.bfloat16)


def dot_of(left, right):
    return jnp.dot(left, right, preferred_element_type=jnp.float32)


def first_projection_kernel(at, stacked, weight, near1, near2, near, far):
    half = near1.shape[1]
    mine = weight[:, pl.ds(pl.multiple_of(at[4] * half, half), half)]
    other = weight[:, pl.ds(pl.multiple_of((1 - at[4]) * half, half), half)]
    near[...] = (
        dot_of(stacked[at[0]], mine) + dot_of(stacked[at[1]], near1[...]) + dot_of(stacked[at[2]], near2[...])
    )
    far[...] = dot_of(stacked[at[0]], other)


def second_projection_kernel(at, stacked, near3, far1, far2, near, far, near_out, far_out):
    near_out[...] = near[...] + dot_of(stacked[at[3]], near3[...])
    far_out[...] = far[...] + dot_of(stacked[at[1]], far1[...]) + dot_of(stacked[at[2]], far2[...])


def last_projection_kernel(at, stacked, far3, near, far, stream, gain, resid, scaled):
    half = far3.shape[1]
    other = far[...] + dot_of(stacked[at[3]], far3[...])
    for side, value in ((at[4], near[...]), (1 - at[4], other)):
        columns = pl.ds(pl.multiple_of(side * half, half), half)
        kept = (stream[:, columns].astype(jnp.float32) + value).astype(jnp.bfloat16)
        resid[:, columns] = kept
        scaled[:, columns] = (kept.astype(jnp.float32) * gain[:, columns].astype(jnp.float32)).astype(jnp.bfloat16)


def mean_kernel(features, one, two, out):
    out[...] = (one[...] + two[...]) / features


def inverse_kernel(energy, out):
    out[...] = 1.0 / (energy[...] + epsilon)


def hidden_products(own, pair, others, weights, out):
    depth = own.shape[1]
    total = None
    for flip, block in enumerate((own, others, pair, others)):
        left = block[flip // 2] if flip % 2 else block[...]
        term = dot_of(left, weights[flip * depth : (flip + 1) * depth, :])
        total = term if total is None else total + term
    out[...] = jnp.square(jnp.maximum(total, 0.0)).astype(jnp.bfloat16)


def first_hidden_kernel(place, own, pair, others, *rest):
    near, far, out, weights = rest[:4], rest[4:6], rest[6], rest[7]
    depth, half = near[0].shape
    for slot, piece in enumerate(near):
        rows = pl.ds(pl.multiple_of(place[slot] * depth, depth), depth)
        weights[rows, :half] = piece[...]
        weights[rows, half:] = far[0][...] if slot == 0 else far[1][slot - 1]
    hidden_products(own, pair, others, weights, out)


def second_hidden_kernel(own, pair, others, weights, out):
    hidden_products(own, pair, others, weights, out)


def branch_products(own, other, weights, keep, give):
    depth = own.shape[1]
    for side, target in ((1, give), (0, keep)):
        value = dot_of(own, weights[side, :depth, :]) + dot_of(other, weights[side, depth:, :])
        target[...] = value.astype(target.dtype)


def first_branch_kernel(place, own, other, *rest):
    near, far, keep, give, weights = rest[:4], rest[4:8], rest[8], rest[9], rest[10]
    half = near[0].shape[0]
    tokens = keep.shape[0]
    for slot in range(len(near)):
        begin = pl.multiple_of(place[len(near) + slot] * (2 * half), 2 * half)
        weights[place[slot], pl.ds(begin, half), :] = near[slot][...]
        weights[place[slot], pl.ds(begin + half, half), :] = far[slot][...]
    branch_products(own[tokens:, :], other[tokens:, :], weights, keep, give)


def second_branch_kernel(own, other, weights, keep_one, give_one, keep_three, give_three):
    tokens = keep_one.shape[0]
    branch_products(own[:tokens, :], other[:tokens, :], weights, keep_one, give_one)
    branch_products(own[tokens:, :], other[tokens:, :], weights, keep_three, give_three)


def third_branch_kernel(own, other, weights, keep, give):
    tokens = keep.shape[0]
    branch_products(own[:tokens, :], other[:tokens, :], weights, keep, give)


def pair_sum_kernel(keep, got, out):
    out[...] = (keep[...] + got[...].astype(jnp.float32)).astype(out.dtype)


def cut_kernel(axis, at, whole, *rest):
    outs, sems = rest[:-1], rest[-1]
    copies = []
    for number, out in enumerate(outs):
        size = out.shape[axis]
        span = pl.ds(pl.multiple_of(at[number] * size, size), size)
        source = whole.at[span, :] if axis == 0 else whole.at[:, span]
        copies.append(pltpu.make_async_copy(source, out, sems.at[number]))
        copies[-1].start()
    for copy in copies:
        copy.wait()


def cut(whole, axis, size, starts):
    shape = tuple(size if i == axis else n for i, n in enumerate(whole.shape))
    out = jax.ShapeDtypeStruct(shape, whole.dtype)
    place = jnp.stack([jnp.asarray(x, jnp.int32) for x in starts])
    return pl.pallas_call(
        functools.partial(cut_kernel, axis),
        out_shape=[out] * len(starts),
        in_specs=[pl.BlockSpec(memory_space=pltpu.SMEM), pl.BlockSpec(memory_space=pltpu.HBM)],
        out_specs=[pl.BlockSpec(memory_space=pltpu.VMEM)] * len(starts),
        scratch_shapes=[pltpu.SemaphoreType.DMA((len(starts),))],
        compiler_params=pltpu.CompilerParams(vmem_limit_bytes=4 << 20),
        cost_estimate=pl.CostEstimate(flops=1024, bytes_accessed=1 << 20, transcendentals=0),
    )(place, whole)


def local_call(kernel, outs, *operands, flops, scratch=(), room=8):
    specs = [
        pl.BlockSpec(memory_space=pltpu.SMEM if x.dtype == jnp.int32 else pltpu.VMEM) for x in operands
    ]
    return pl.pallas_call(
        kernel,
        out_shape=outs,
        in_specs=specs,
        out_specs=jax.tree.map(lambda _: pl.BlockSpec(memory_space=pltpu.VMEM), outs),
        scratch_shapes=scratch,
        compiler_params=pltpu.CompilerParams(vmem_limit_bytes=room << 20),
        cost_estimate=pl.CostEstimate(flops=flops, bytes_accessed=1 << 20, transcendentals=0),
    )(*operands)


def gathered_tokens(parts, stream, mixed, out_weight, norm_gain, up_weight, down_weight):
    tokens, width = stream.shape
    half = width // 2
    unit = up_weight.shape[1] // parts
    part, row, column = lax.axis_index("grp"), lax.axis_index("fs"), lax.axis_index("tp")
    flips = (1, 2, 3)

    def along_rows(value, flip):
        return lax.ppermute(value, "fs", [(i, i ^ flip) for i in range(parts)])

    def across_parts(value):
        return lax.ppermute(value, "grp", [(0, 1), (1, 0)])

    def across_columns(value, flip):
        return lax.ppermute(value, "tp", [(i, i ^ flip) for i in range(parts)])

    at = jnp.stack([column ^ row ^ s for s in range(parts)] + [part]).astype(jnp.int32)
    (out_mine,) = cut(out_weight, 1, half, [part])
    out_near = {s: along_rows(out_mine, s) for s in (1, 2)}
    out_near[3] = along_rows(out_near[2], 1)
    flipped = [across_columns(mixed, flip) for flip in (1, 2, 3)]
    out_far = {s: across_parts(out_near[s]) for s in flips}
    sums = jax.ShapeDtypeStruct((tokens, half), jnp.float32)
    flops = 2 * tokens * width * half
    stacked = jnp.stack([mixed, *flipped])
    near, far = local_call(
        first_projection_kernel, (sums, sums), at, stacked, out_weight, out_near[1], out_near[2], flops=3 * flops
    )
    near, far = local_call(
        second_projection_kernel, (sums, sums),
        at, stacked, out_near[3], out_far[1], out_far[2], near, far,
        flops=3 * flops,
    )
    resid, scaled = local_call(
        last_projection_kernel,
        (jax.ShapeDtypeStruct((tokens, width), jnp.bfloat16),) * 2,
        at, stacked, out_far[3], near, far, stream, norm_gain.reshape(1, width),
        flops=flops,
    )
    widened = resid.astype(jnp.float32)
    power = jnp.sum(widened * widened, axis=1).reshape(-1, 128)
    power += across_columns(power, 1)
    small = jax.ShapeDtypeStruct(power.shape, jnp.float32)
    energy = local_call(
        functools.partial(mean_kernel, parts * width), small, power, across_columns(power, 2), flops=1024
    )
    inverse = local_call(inverse_kernel, small, energy, flops=1024)

    wanted = [2 * (row ^ s) + part for s in (0, *flips)] + [2 * row + 1 - part]
    up_mine, *up_sent, up_other = cut(up_weight, 1, unit // 2, wanted)
    up_near = {s: along_rows(piece, s) for s, piece in zip(flips, up_sent)}
    up_far = across_parts(jnp.stack([up_near[s] for s in (1, 2, 3)]))
    core = column % 2
    odd_one = (row ^ core) % 2
    down_near, down_far, sides, sources = [], [], [], []
    turns = ((0, 0), (0, 1), (2, 0), (2, 1))
    wanted = [2 * (row ^ (pair + (core ^ turn))) + part for pair, turn in turns]
    down_sent = cut(down_weight, 0, unit // 2, wanted)
    for number, (pair, turn) in enumerate(turns):
        moves = []
        for i in range(parts):
            for j in range(parts):
                moves.append((i * parts + j, (i ^ (pair + (j % 2 ^ turn))) * parts + j // 2 * 2 + i % 2))
        down_near.append(lax.ppermute(down_sent[number], ("fs", "tp"), moves))
        down_far.append(across_parts(down_near[-1]))
        sides.append(((row ^ (pair + odd_one)) != column).astype(jnp.int32))
        sources.append((odd_one ^ turn ^ core).astype(jnp.int32))
    down_place = jnp.stack(sides + sources)
    place = at[:parts]

    pairs = {0: across_columns(scaled, 2)}
    rows = {s: along_rows(scaled, s) for s in (1, 2)}
    rows[3] = along_rows(rows[2], 1)
    pairs |= {s: across_columns(rows[s], 2) for s in flips}
    even = jnp.concatenate([scaled, rows[2]])
    odd = jnp.concatenate([rows[1], rows[3]])
    even_pair = jnp.concatenate([pairs[0], pairs[2]])
    odd_pair = jnp.concatenate([pairs[1], pairs[3]])
    even_both = jnp.stack([even, even_pair])
    even_others = across_columns(even_both, 1)
    odd_others = across_columns(jnp.stack([odd, odd_pair]), 1)
    flops = 4 * tokens * parts * width * unit
    some = jax.ShapeDtypeStruct((2 * tokens, unit), jnp.bfloat16)
    hidden_even, up_whole = local_call(
        first_hidden_kernel,
        (some, jax.ShapeDtypeStruct((parts * width, unit), jnp.bfloat16)),
        place, even, even_pair, even_others,
        up_mine, up_near[1], up_near[2], up_near[3], up_other, up_far,
        flops=flops,
        room=14,
    )
    hidden_odd = local_call(second_hidden_kernel, some, odd, odd_pair, odd_others, up_whole, flops=flops, room=14)

    block = (tokens, width)
    pair_of = (jax.ShapeDtypeStruct(block, jnp.float32), jax.ShapeDtypeStruct(block, jnp.bfloat16))
    other_even = across_columns(hidden_even, 1)
    other_odd = across_columns(hidden_odd, 1)
    keep_two, give_two, down_whole = local_call(
        first_branch_kernel,
        (*pair_of, jax.ShapeDtypeStruct((2, 2 * unit, width), jnp.bfloat16)),
        down_place, hidden_even, other_even, *down_near, *down_far,
        flops=flops // 2,
        room=14,
    )
    keep_one, give_one, keep_three, give_three = local_call(
        second_branch_kernel, pair_of * 2, hidden_odd, other_odd, down_whole, flops=flops, room=14
    )
    keep_own, give_own = local_call(
        third_branch_kernel, pair_of, hidden_even, other_even, down_whole, flops=flops // 2, room=14
    )

    def summed(keep, give):
        out = jax.ShapeDtypeStruct(block, jnp.bfloat16)
        return local_call(pair_sum_kernel, out, keep, across_columns(give, 2), flops=1024)

    two = summed(keep_two, give_two)
    one = summed(keep_one, give_one)
    three = summed(keep_three, give_three)
    branch = keep_own + across_columns(give_own, 2)
    branch += along_rows(two, 2)
    branch += along_rows(one, 1)
    branch += along_rows(three, 3)
    return (widened + branch * inverse.reshape(tokens, 1)).astype(jnp.bfloat16)


def solution(mesh):
    shape = mesh.shape
    placed = (
        P(("grp", "fs"), "tp"),
        P(("grp", "fs"), "tp"),
        P("fs", "tp"),
        P("tp"),
        P("fs", "tp"),
        P("tp", "fs"),
    )

    cut = shape["grp"] == 2 and shape["fs"] == 4 and shape["tp"] == 4

    def body(*blocks):
        if not cut:
            return gathered_weights(*blocks)
        return gathered_tokens(shape["fs"], *blocks)

    return jax.shard_map(
        body, mesh=mesh, in_specs=placed, out_specs=P(("grp", "fs"), "tp"), check_vma=False
    )
```

time: 173 us -> 174 us (level)
  waiting for transfers between devices: 104 us -> 97.1 us
  starting transfers between devices: 51 us -> 45.1 us
  local copies, waits for them, and re-layouts: 5.32 us -> 10.4 us
  other arithmetic: 1.53 us -> 5.48 us
  Pallas kernels: 10.4 us -> 14.3 us
    ppermute x7 -> x8, waiting for transfers between devices: 14.2 us -> 31.9 us  [across_parts(): return lax.ppermute(value, 'grp', [(0, 1), (1, 0)])]
    ppermute x16, waiting for transfers between devices: 60.3 us -> 43.5 us  [the longest x12 39.8 us: along_rows(): return lax.ppermute(value, 'fs', [(i, i ^ flip) for i in range(parts)])]
    ppermute x16, starting transfers between devices: 30.4 us -> 22.3 us  [the longest x12 18.8 us: along_rows(): return lax.ppermute(value, 'fs', [(i, i ^ flip) for i in range(parts)])]
    ppermute x17, waiting for transfers between devices: 29.3 us -> 21.7 us  [across_columns(): return lax.ppermute(value, 'tp', [(i, i ^ flip) for i in range(parts)])]
    unnamed x10 -> x42, local copies, waits for them, and re-layouts: 2.03 us -> 9.43 us
    ppermute x17, starting transfers between devices: 10.8 us -> 14 us  [across_columns(): return lax.ppermute(value, 'tp', [(i, i ^ flip) for i in range(parts)])]
    dynamic_slice x3 -> x0, local copies, waits for them, and re-layouts: 2.49 us -> none  [the longest x2 2.35 us: columns_at(): return lax.dynamic_slice_in_dim(value, begin, size, 1)]
    pallas_call x17 -> x13, Pallas kernels: 10.4 us -> 12.8 us  [local_call(): pl.pallas_call(kernel, out_shape=outs, in_specs=specs, out_specs=jax.tree...]
  transfers between devices with their start and end apart: 40 -> 41, of which waited for: 22 -> 21; matrix products, arithmetic and copies ran while one was open for 2% -> 4% of each run, Pallas kernels for 4% -> 8%
where the time goes in v3:
time: 174 us; the launch traced here: 173 us
  waiting for transfers between devices  97.1 us (56%)
  starting transfers between devices  45.1 us (26%)
  Pallas kernels  14.3 us (8%)
  local copies, waits for them, and re-layouts  10.4 us (6%)
  other arithmetic  5.48 us (3%)
    ppermute x12, waiting for transfers between devices, along_rows(): return lax.ppermute(value, 'fs', [(i, i ^ flip) for i in range(parts)])  39.8 us
    ppermute x8, waiting for transfers between devices, across_parts(): return lax.ppermute(value, 'grp', [(0, 1), (1, 0)])  31.9 us
    ppermute x17, waiting for transfers between devices, across_columns(): return lax.ppermute(value, 'tp', [(i, i ^ flip) for i in range(parts)])  21.7 us
    ppermute x12, starting transfers between devices, along_rows(): return lax.ppermute(value, 'fs', [(i, i ^ flip) for i in range(parts)])  18.8 us
    ppermute x17, starting transfers between devices, across_columns(): return lax.ppermute(value, 'tp', [(i, i ^ flip) for i in range(parts)])  14 us
    pallas_call x13, Pallas kernels, local_call(): pl.pallas_call(kernel, out_shape=outs, in_specs=specs, out_specs=jax.tree...  12.8 us
    unnamed x42, local copies, waits for them, and re-layouts  9.43 us
    ppermute x8, starting transfers between devices, across_parts(): return lax.ppermute(value, 'grp', [(0, 1), (1, 0)])  8.85 us
  transfers between devices with their start and end apart: 41, of which 21 were waited for; matrix products, arithmetic and copies ran while one was open for 4% of the time, Pallas kernels for 8%

profile of v3, /device:TPU:0, one launch (start us, length us, event | category | flops | bytes accessed | tf_op | source)
XLA Modules:
  0.0 172.8 jit_solution(8666280398111142631)
XLA Ops:
  1.1 4.1 %collective-permute-start.3 = (bf16[512,256]{1,0:T(8,128)(2,1)S(1)}, bf16[512,256]{1,0:T(8,128)(2,1)S(1)}, u32[]{:S(2)}, u32[]{:S(2)}) collective-permute-start(bf16[512,256]{1,0:T(8,128)(2,1)S(1)} %shard_map.64), channel_id=1, source_target_pairs={{0,8},{4,12},{8,0},{12,4},{1,9},{5,13},{9,1},{13,5},{2,10},{6,14},... | collective-permute-start | bytes 786440 | tf_op jit(solution)/shard_map/ppermute | solution.py:184
  6.8 10.4 %collective-permute-done.3.near2 = bf16[512,256]{1,0:T(8,128)(2,1)S(1)} collective-permute-done((bf16[512,256]{1,0:T(8,128)(2,1)S(1)}, bf16[512,256]{1,0:T(8,128)(2,1)S(1)}, u32[]{:S(2)}, u32[]{:S(2)}) %collective-permute-start.3) | collective-permute-done | bytes 262176 | tf_op jit(solution)/shard_map/ppermute | solution.py:184
  21.4 3.2 %collective-permute-done.4.near3 = bf16[512,256]{1,0:T(8,128)(2,1)S(1)} collective-permute-done((bf16[512,256]{1,0:T(8,128)(2,1)S(1)}, bf16[512,256]{1,0:T(8,128)(2,1)S(1)}, u32[]{:S(2)}, u32[]{:S(2)}) %collective-permute-start.4) | collective-permute-done | bytes 262176 | tf_op jit(solution)/shard_map/ppermute | solution.py:184
  27.2 3.5 %collective-permute-done.2 = bf16[256,512]{1,0:T(8,128)(2,1)S(1)} collective-permute-done((bf16[256,512]{1,0:T(8,128)(2,1)}, bf16[256,512]{1,0:T(8,128)(2,1)S(1)}, u32[]{:S(2)}, u32[]{:S(2)}) %collective-permute-start.2) | collective-permute-done | bytes 262176 | tf_op jit(solution)/shard_map/ppermute | solution.py:190
  35.1 4.3 %collective-permute-done.5.far3 = bf16[512,256]{1,0:T(8,128)(2,1)S(1)} collective-permute-done((bf16[512,256]{1,0:T(8,128)(2,1)S(1)}, bf16[512,256]{1,0:T(8,128)(2,1)S(1)}, u32[]{:S(2)}, u32[]{:S(2)}) %collective-permute-start.5) | collective-permute-done | bytes 262176 | tf_op jit(solution)/shard_map/ppermute | solution.py:187
  40.9 3.4 %collective-permute-start.9 = (bf16[256,512]{1,0:T(8,128)(2,1)S(1)}, bf16[256,512]{1,0:T(8,128)(2,1)S(1)}, u32[]{:S(2)}, u32[]{:S(2)}) collective-permute-start(bf16[256,512]{1,0:T(8,128)(2,1)S(1)} %get-tuple-element.36), channel_id=1, source_target_pairs={{0,8},{4,12},{8,0},{12,4},{1,9},{5,13},{9,1},{13,5},{2,10},{6,14},... | collective-permute-start | bytes 786440 | tf_op jit(solution)/shard_map/ppermute | solution.py:184
  50.0 6.4 %collective-permute-done.9 = bf16[256,512]{1,0:T(8,128)(2,1)S(1)} collective-permute-done((bf16[256,512]{1,0:T(8,128)(2,1)S(1)}, bf16[256,512]{1,0:T(8,128)(2,1)S(1)}, u32[]{:S(2)}, u32[]{:S(2)}) %collective-permute-start.9) | collective-permute-done | bytes 262176 | tf_op jit(solution)/shard_map/ppermute | solution.py:184
  57.4 7.1 %collective-permute-done.29 = bf16[256,512]{1,0:T(8,128)(2,1)S(1)} collective-permute-done((bf16[256,512]{1,0:T(8,128)(2,1)S(1)}, bf16[256,512]{1,0:T(8,128)(2,1)S(1)}, u32[]{:S(2)}, u32[]{:S(2)}) %collective-permute-start.29) | collective-permute-done | bytes 262176 | tf_op jit(solution)/shard_map/ppermute | solution.py:184
  68.4 11.5 %collective-permute-done.30 = bf16[256,512]{1,0:T(8,128)(2,1)S(1)} collective-permute-done((bf16[256,512]{1,0:T(8,128)(2,1)S(1)}, bf16[256,512]{1,0:T(8,128)(2,1)S(1)}, u32[]{:S(2)}, u32[]{:S(2)}) %collective-permute-start.30) | collective-permute-done | bytes 262176 | tf_op jit(solution)/shard_map/ppermute | solution.py:184
  82.9 4.3 %collective-permute-done.32 = bf16[256,512]{1,0:T(8,128)(2,1)S(1)} collective-permute-done((bf16[256,512]{1,0:T(8,128)(2,1)S(1)}, bf16[256,512]{1,0:T(8,128)(2,1)S(1)}, u32[]{:S(2)}, u32[]{:S(2)}) %collective-permute-start.32) | collective-permute-done | bytes 262176 | tf_op jit(solution)/shard_map/ppermute | solution.py:190
  94.6 2.8 %collective-permute-start.19 = (bf16[256,512]{1,0:T(8,128)(2,1)S(1)}, bf16[256,512]{1,0:T(8,128)(2,1)}, u32[]{:S(2)}, u32[]{:S(2)}) collective-permute-start(bf16[256,512]{1,0:T(8,128)(2,1)S(1)} %get-tuple-element.44), channel_id=1, source_target_pairs={{0,4},{1,0},{2,6},{3,2},{4,1},{5,5},{6,3},{7,7},{8,12},{9,8},{10,1... | collective-permute-start | bytes 786440 | tf_op jit(solution)/shard_map/ppermute | solution.py:239
  97.5 12.8 %collective-permute-done.16.rest_5_ = bf16[3,512,256]{2,1,0:T(8,128)(2,1)} collective-permute-done((bf16[3,512,256]{2,1,0:T(8,128)(2,1)}, bf16[3,512,256]{2,1,0:T(8,128)(2,1)}, u32[]{:S(2)}, u32[]{:S(2)}) %collective-permute-start.16) | collective-permute-done | bytes 786464 | tf_op jit(solution)/shard_map/ppermute | solution.py:187
  114.7 2.5 %shard_map.69 = (bf16[512,512]{1,0:T(8,128)(2,1)S(1)}, bf16[2048,512]{1,0:T(8,128)(2,1)S(1)}) custom-call(s32[4]{0:T(128)S(1)} %pad_add_fusion.place, bf16[512,512]{1,0:T(8,128)(2,1)S(1)} %constant_dynamic-update-slice_fusion.own, bf16[512,512]{1,0:T(8,128)(2,1)S(1)} %constant_dynamic-update-slice_fusion.2.pair, bf16[2,512,512]{2,1,0:T(8,128)(2,1)S(1)} %copy-done.5, ...), custom_call_target="tpu_custom_call" | custom-call | flops 1073741824 | bytes 1048576 | tf_op jit(solution)/shard_map/pallas_call | solution.py:165
  117.4 2.5 %shard_map.74.own = bf16[512,512]{1,0:T(8,128)(2,1)S(1)} custom-call(bf16[512,512]{1,0:T(8,128)(2,1)S(1)} %constant_dynamic-update-slice_fusion.4.own, bf16[512,512]{1,0:T(8,128)(2,1)S(1)} %constant_dynamic-update-slice_fusion.6.pair, bf16[2,512,512]{2,1,0:T(8,128)(2,1)} %collective-permute-done.33.others, bf16[2048,512]{1,0:T(8,128)(2,1)S(1)} %get-tuple-element.52.weights), custom_call_target="tpu_custom_call" | custom-call | flops 1073741824 | bytes 1048576 | tf_op jit(solution)/shard_map/pallas_call | solution.py:165
  121.0 3.6 %collective-permute-done.21.rest_3_ = bf16[256,512]{1,0:T(8,128)(2,1)} collective-permute-done((bf16[256,512]{1,0:T(8,128)(2,1)S(1)}, bf16[256,512]{1,0:T(8,128)(2,1)}, u32[]{:S(2)}, u32[]{:S(2)}) %collective-permute-start.21) | collective-permute-done | bytes 262176 | tf_op jit(solution)/shard_map/ppermute | solution.py:239
  126.8 3.1 %collective-permute-done.23.rest_5_ = bf16[256,512]{1,0:T(8,128)(2,1)S(1)} collective-permute-done((bf16[256,512]{1,0:T(8,128)(2,1)}, bf16[256,512]{1,0:T(8,128)(2,1)S(1)}, u32[]{:S(2)}, u32[]{:S(2)}) %collective-permute-start.23) | collective-permute-done | bytes 262176 | tf_op jit(solution)/shard_map/ppermute | solution.py:187
  129.9 5.6 %collective-permute-done.24.rest_6_ = bf16[256,512]{1,0:T(8,128)(2,1)S(1)} collective-permute-done((bf16[256,512]{1,0:T(8,128)(2,1)}, bf16[256,512]{1,0:T(8,128)(2,1)S(1)}, u32[]{:S(2)}, u32[]{:S(2)}) %collective-permute-start.24) | collective-permute-done | bytes 262176 | tf_op jit(solution)/shard_map/ppermute | solution.py:187
  135.5 4.7 %collective-permute-done.25.rest_7_ = bf16[256,512]{1,0:T(8,128)(2,1)S(1)} collective-permute-done((bf16[256,512]{1,0:T(8,128)(2,1)}, bf16[256,512]{1,0:T(8,128)(2,1)S(1)}, u32[]{:S(2)}, u32[]{:S(2)}) %collective-permute-start.25) | collective-permute-done | bytes 262176 | tf_op jit(solution)/shard_map/ppermute | solution.py:187
  144.0 2.3 %shard_map.75 = (f32[256,512]{1,0:T(8,128)S(1)}, bf16[256,512]{1,0:T(8,128)(2,1)S(1)}, f32[256,512]{1,0:T(8,128)S(1)}, bf16[256,512]{1,0:T(8,128)(2,1)S(1)}) custom-call(bf16[512,512]{1,0:T(8,128)(2,1)S(1)} %shard_map.74.own, bf16[512,512]{1,0:T(8,128)(2,1)} %collective-permute-done.34.other, bf16[2,1024,512]{2,1,0:T(8,128)(2,1)S(1)} %get-tuple-element.47.weights), custom_call_target="tpu_custom_call" | custom-call | flops 1073741824 | bytes 1048576 | tf_op jit(solution)/shard_map/pallas_call | solution.py:165
  149.4 2.0 %collective-permute-done.27.got = bf16[256,512]{1,0:T(8,128)(2,1)S(1)} collective-permute-done((bf16[256,512]{1,0:T(8,128)(2,1)S(1)}, bf16[256,512]{1,0:T(8,128)(2,1)S(1)}, u32[]{:S(2)}, u32[]{:S(2)}) %collective-permute-start.27) | collective-permute-done | bytes 262176 | tf_op jit(solution)/shard_map/ppermute | solution.py:190
  151.5 2.7 %collective-permute-start.28 = (bf16[256,512]{1,0:T(8,128)(2,1)S(1)}, bf16[256,512]{1,0:T(8,128)(2,1)S(1)}, u32[]{:S(2)}, u32[]{:S(2)}) collective-permute-start(bf16[256,512]{1,0:T(8,128)(2,1)S(1)} %shard_map.73), channel_id=1, source_target_pairs={{0,8},{4,12},{8,0},{12,4},{1,9},{5,13},{9,1},{13,5},{2,10},{6,14},... | collective-permute-start | bytes 786440 | tf_op jit(solution)/shard_map/ppermute | solution.py:184
  154.2 2.8 %collective-permute-done.35.got = bf16[256,512]{1,0:T(8,128)(2,1)S(1)} collective-permute-done((bf16[256,512]{1,0:T(8,128)(2,1)S(1)}, bf16[256,512]{1,0:T(8,128)(2,1)S(1)}, u32[]{:S(2)}, u32[]{:S(2)}) %collective-permute-start.35) | collective-permute-done | bytes 262176 | tf_op jit(solution)/shard_map/ppermute | solution.py:190
  157.2 5.5 %collective-permute-done.37.got = bf16[256,512]{1,0:T(8,128)(2,1)S(1)} collective-permute-done((bf16[256,512]{1,0:T(8,128)(2,1)S(1)}, bf16[256,512]{1,0:T(8,128)(2,1)S(1)}, u32[]{:S(2)}, u32[]{:S(2)}) %collective-permute-start.37) | collective-permute-done | bytes 262176 | tf_op jit(solution)/shard_map/ppermute | solution.py:190
  162.7 3.1 %collective-permute-start.38 = (bf16[256,512]{1,0:T(8,128)(2,1)S(1)}, bf16[256,512]{1,0:T(8,128)(2,1)S(1)}, u32[]{:S(2)}, u32[]{:S(2)}) collective-permute-start(bf16[256,512]{1,0:T(8,128)(2,1)S(1)} %shard_map.77), channel_id=1, source_target_pairs={{0,12},{4,8},{8,4},{12,0},{1,13},{5,9},{9,5},{13,1},{2,14},{6,10},... | collective-permute-start | bytes 786440 | tf_op jit(solution)/shard_map/ppermute | solution.py:184
  (133 shorter events, 57.8 us)
Async XLA Ops:
  1.1 16.2 %collective-permute-start.3 = (bf16[512,256]{1,0:T(8,128)(2,1)S(1)}, bf16[512,256]{1,0:T(8,128)(2,1)S(1)}, u32[]{:S(2)}, u32[]{:S(2)}) collective-permute-start(bf16[512,256]{1,0:T(8,128)(2,1)S(1)} %shard_map.64), channel_id=1, source_target_pairs={{0,8},{4,12},{8,0},{12,4},{1,9},{5,13},{9,1},{13,5},{2,10},{6,14},... | collective-permute-start | bytes 786440 | tf_op jit(solution)/shard_map/ppermute | solution.py:184
  5.2 14.2 %collective-permute-start.6 = (bf16[512,256]{1,0:T(8,128)(2,1)S(1)}, bf16[512,256]{1,0:T(8,128)(2,1)S(1)}, u32[]{:S(2)}, u32[]{:S(2)}) collective-permute-start(bf16[512,256]{1,0:T(8,128)(2,1)S(1)} %shard_map.64), channel_id=1, source_target_pairs={{0,4},{4,0},{8,12},{12,8},{1,5},{5,1},{9,13},{13,9},{2,6},{6,2},{1... | collective-permute-start | bytes 786440 | tf_op jit(solution)/shard_map/ppermute | solution.py:184
  24.7 14.8 %collective-permute-start.5 = (bf16[512,256]{1,0:T(8,128)(2,1)S(1)}, bf16[512,256]{1,0:T(8,128)(2,1)S(1)}, u32[]{:S(2)}, u32[]{:S(2)}) collective-permute-start(bf16[512,256]{1,0:T(8,128)(2,1)S(1)} %collective-permute-done.4.near3), channel_id=1, source_target_pairs={{0,16},{16,0},{1,17},{17,1},{2,18},{18,2},{3,19},{19,3},{4,20},{20... | collective-permute-start | bytes 786440 | tf_op jit(solution)/shard_map/ppermute | solution.py:187
  40.9 15.5 %collective-permute-start.9 = (bf16[256,512]{1,0:T(8,128)(2,1)S(1)}, bf16[256,512]{1,0:T(8,128)(2,1)S(1)}, u32[]{:S(2)}, u32[]{:S(2)}) collective-permute-start(bf16[256,512]{1,0:T(8,128)(2,1)S(1)} %get-tuple-element.36), channel_id=1, source_target_pairs={{0,8},{4,12},{8,0},{12,4},{1,9},{5,13},{9,1},{13,5},{2,10},{6,14},... | collective-permute-start | bytes 786440 | tf_op jit(solution)/shard_map/ppermute | solution.py:184
  44.3 20.3 %collective-permute-start.29 = (bf16[256,512]{1,0:T(8,128)(2,1)S(1)}, bf16[256,512]{1,0:T(8,128)(2,1)S(1)}, u32[]{:S(2)}, u32[]{:S(2)}) collective-permute-start(bf16[256,512]{1,0:T(8,128)(2,1)S(1)} %get-tuple-element.36), channel_id=1, source_target_pairs={{0,4},{4,0},{8,12},{12,8},{1,5},{5,1},{9,13},{13,9},{2,6},{6,2},{1... | collective-permute-start | bytes 786440 | tf_op jit(solution)/shard_map/ppermute | solution.py:184
  44.3 20.3 %collective-permute-start.10 = (bf16[256,512]{1,0:T(8,128)(2,1)S(1)}, bf16[256,512]{1,0:T(8,128)(2,1)}, u32[]{:S(2)}, u32[]{:S(2)}) collective-permute-start(bf16[256,512]{1,0:T(8,128)(2,1)S(1)} %get-tuple-element.36), channel_id=1, source_target_pairs={{0,2},{1,3},{2,0},{3,1},{4,6},{5,7},{6,4},{7,5},{8,10},{9,11},{10,... | collective-permute-start | bytes 786440 | tf_op jit(solution)/shard_map/ppermute | solution.py:190
  48.2 40.1 %collective-permute-start.13 = (bf16[512,256]{1,0:T(8,128)(2,1)S(1)}, bf16[512,256]{1,0:T(8,128)(2,1)S(1)}, u32[]{:S(2)}, u32[]{:S(2)}) collective-permute-start(bf16[512,256]{1,0:T(8,128)(2,1)S(1)} %get-tuple-element.38), channel_id=1, source_target_pairs={{0,4},{4,0},{8,12},{12,8},{1,5},{5,1},{9,13},{13,9},{2,6},{6,2},{1... | collective-permute-start | bytes 786440 | tf_op jit(solution)/shard_map/ppermute | solution.py:184
  50.0 38.3 %collective-permute-start.14 = (bf16[512,256]{1,0:T(8,128)(2,1)S(1)}, bf16[512,256]{1,0:T(8,128)(2,1)S(1)}, u32[]{:S(2)}, u32[]{:S(2)}) collective-permute-start(bf16[512,256]{1,0:T(8,128)(2,1)S(1)} %get-tuple-element.39), channel_id=1, source_target_pairs={{0,8},{4,12},{8,0},{12,4},{1,9},{5,13},{9,1},{13,5},{2,10},{6,14},... | collective-permute-start | bytes 786440 | tf_op jit(solution)/shard_map/ppermute | solution.py:184
  64.6 15.4 %collective-permute-start.30 = (bf16[256,512]{1,0:T(8,128)(2,1)S(1)}, bf16[256,512]{1,0:T(8,128)(2,1)S(1)}, u32[]{:S(2)}, u32[]{:S(2)}) collective-permute-start(bf16[256,512]{1,0:T(8,128)(2,1)S(1)} %collective-permute-done.9), channel_id=1, source_target_pairs={{0,4},{4,0},{8,12},{12,8},{1,5},{5,1},{9,13},{13,9},{2,6},{6,2},{1... | collective-permute-start | bytes 786440 | tf_op jit(solution)/shard_map/ppermute | solution.py:184
  64.6 18.2 %collective-permute-start.31 = (bf16[256,512]{1,0:T(8,128)(2,1)S(1)}, bf16[256,512]{1,0:T(8,128)(2,1)S(1)}, u32[]{:S(2)}, u32[]{:S(2)}) collective-permute-start(bf16[256,512]{1,0:T(8,128)(2,1)S(1)} %collective-permute-done.29), channel_id=1, source_target_pairs={{0,2},{1,3},{2,0},{3,1},{4,6},{5,7},{6,4},{7,5},{8,10},{9,11},{10,... | collective-permute-start | bytes 786440 | tf_op jit(solution)/shard_map/ppermute | solution.py:190
  67.1 21.2 %collective-permute-start.15 = (bf16[512,256]{1,0:T(8,128)(2,1)S(1)}, bf16[512,256]{1,0:T(8,128)(2,1)S(1)}, u32[]{:S(2)}, u32[]{:S(2)}) collective-permute-start(bf16[512,256]{1,0:T(8,128)(2,1)S(1)} %get-tuple-element.40), channel_id=1, source_target_pairs={{0,12},{4,8},{8,4},{12,0},{1,13},{5,9},{9,5},{13,1},{2,14},{6,10},... | collective-permute-start | bytes 786440 | tf_op jit(solution)/shard_map/ppermute | solution.py:184
  82.8 27.5 %collective-permute-start.12 = (bf16[2,512,512]{2,1,0:T(8,128)(2,1)}, bf16[2,512,512]{2,1,0:T(8,128)(2,1)S(1)}, u32[]{:S(2)}, u32[]{:S(2)}) collective-permute-start(bf16[2,512,512]{2,1,0:T(8,128)(2,1)} %pad_maximum_fusion.1), channel_id=1, source_target_pairs={{0,1},{1,0},{2,3},{3,2},{4,5},{5,4},{6,7},{7,6},{8,9},{9,8},{10,11... | collective-permute-start | bytes 3145736 | tf_op jit(solution)/shard_map/ppermute | solution.py:190
  88.3 29.0 %collective-permute-start.33 = (bf16[2,512,512]{2,1,0:T(8,128)(2,1)}, bf16[2,512,512]{2,1,0:T(8,128)(2,1)}, u32[]{:S(2)}, u32[]{:S(2)}) collective-permute-start(bf16[2,512,512]{2,1,0:T(8,128)(2,1)} %pad_maximum_fusion.2), channel_id=1, source_target_pairs={{0,1},{1,0},{2,3},{3,2},{4,5},{5,4},{6,7},{7,6},{8,9},{9,8},{10,11... | collective-permute-start | bytes 3145736 | tf_op jit(solution)/shard_map/ppermute | solution.py:190
  90.1 20.3 %collective-permute-start.16 = (bf16[3,512,256]{2,1,0:T(8,128)(2,1)}, bf16[3,512,256]{2,1,0:T(8,128)(2,1)}, u32[]{:S(2)}, u32[]{:S(2)}) collective-permute-start(bf16[3,512,256]{2,1,0:T(8,128)(2,1)} %pad_maximum_fusion.3), channel_id=1, source_target_pairs={{0,16},{16,0},{1,17},{17,1},{2,18},{18,2},{3,19},{19,3},{4,20},{20... | collective-permute-start | bytes 2359304 | tf_op jit(solution)/shard_map/ppermute | solution.py:187
  94.6 25.3 %collective-permute-start.19 = (bf16[256,512]{1,0:T(8,128)(2,1)S(1)}, bf16[256,512]{1,0:T(8,128)(2,1)}, u32[]{:S(2)}, u32[]{:S(2)}) collective-permute-start(bf16[256,512]{1,0:T(8,128)(2,1)S(1)} %get-tuple-element.44), channel_id=1, source_target_pairs={{0,4},{1,0},{2,6},{3,2},{4,1},{5,5},{6,3},{7,7},{8,12},{9,8},{10,1... | collective-permute-start | bytes 786440 | tf_op jit(solution)/shard_map/ppermute | solution.py:239
  97.4 23.0 %collective-permute-start.20 = (bf16[256,512]{1,0:T(8,128)(2,1)S(1)}, bf16[256,512]{1,0:T(8,128)(2,1)}, u32[]{:S(2)}, u32[]{:S(2)}) collective-permute-start(bf16[256,512]{1,0:T(8,128)(2,1)S(1)} %get-tuple-element.45), channel_id=1, source_target_pairs={{0,8},{1,12},{2,10},{3,14},{4,13},{5,9},{6,15},{7,11},{8,0},{9,4},... | collective-permute-start | bytes 786440 | tf_op jit(solution)/shard_map/ppermute | solution.py:239
  110.3 14.3 %collective-permute-start.21 = (bf16[256,512]{1,0:T(8,128)(2,1)S(1)}, bf16[256,512]{1,0:T(8,128)(2,1)}, u32[]{:S(2)}, u32[]{:S(2)}) collective-permute-start(bf16[256,512]{1,0:T(8,128)(2,1)S(1)} %get-tuple-element.46), channel_id=1, source_target_pairs={{0,12},{1,8},{2,14},{3,10},{4,9},{5,13},{6,11},{7,15},{8,4},{9,0},... | collective-permute-start | bytes 786440 | tf_op jit(solution)/shard_map/ppermute | solution.py:239
  117.3 22.9 %collective-permute-start.17 = (bf16[512,512]{1,0:T(8,128)(2,1)S(1)}, bf16[512,512]{1,0:T(8,128)(2,1)S(1)}, u32[]{:S(2)}, u32[]{:S(2)}) collective-permute-start(bf16[512,512]{1,0:T(8,128)(2,1)S(1)} %get-tuple-element.42.own), channel_id=1, source_target_pairs={{0,1},{1,0},{2,3},{3,2},{4,5},{5,4},{6,7},{7,6},{8,9},{9,8},{10,11... | collective-permute-start | bytes 1572872 | tf_op jit(solution)/shard_map/ppermute | solution.py:190
  119.9 24.1 %collective-permute-start.34 = (bf16[512,512]{1,0:T(8,128)(2,1)S(1)}, bf16[512,512]{1,0:T(8,128)(2,1)}, u32[]{:S(2)}, u32[]{:S(2)}) collective-permute-start(bf16[512,512]{1,0:T(8,128)(2,1)S(1)} %shard_map.74.own), channel_id=1, source_target_pairs={{0,1},{1,0},{2,3},{3,2},{4,5},{5,4},{6,7},{7,6},{8,9},{9,8},{10,11... | collective-permute-start | bytes 1572872 | tf_op jit(solution)/shard_map/ppermute | solution.py:190
  125.2 15.0 %collective-permute-start.25 = (bf16[256,512]{1,0:T(8,128)(2,1)}, bf16[256,512]{1,0:T(8,128)(2,1)S(1)}, u32[]{:S(2)}, u32[]{:S(2)}) collective-permute-start(bf16[256,512]{1,0:T(8,128)(2,1)} %collective-permute-done.21.rest_3_), channel_id=1, source_target_pairs={{0,16},{16,0},{1,17},{17,1},{2,18},{18,2},{3,19},{19,3},{4,20},{20... | collective-permute-start | bytes 786440 | tf_op jit(solution)/shard_map/ppermute | solution.py:187
  146.6 16.0 %collective-permute-start.37 = (bf16[256,512]{1,0:T(8,128)(2,1)S(1)}, bf16[256,512]{1,0:T(8,128)(2,1)S(1)}, u32[]{:S(2)}, u32[]{:S(2)}) collective-permute-start(bf16[256,512]{1,0:T(8,128)(2,1)S(1)} %get-tuple-element.56), channel_id=1, source_target_pairs={{0,2},{1,3},{2,0},{3,1},{4,6},{5,7},{6,4},{7,5},{8,10},{9,11},{10,... | collective-permute-start | bytes 786440 | tf_op jit(solution)/shard_map/ppermute | solution.py:190
  149.1 21.7 %collective-permute-start.26 = (bf16[256,512]{1,0:T(8,128)(2,1)S(1)}, bf16[256,512]{1,0:T(8,128)(2,1)S(1)}, u32[]{:S(2)}, u32[]{:S(2)}) collective-permute-start(bf16[256,512]{1,0:T(8,128)(2,1)S(1)} %get-tuple-element.49), channel_id=1, source_target_pairs={{0,2},{1,3},{2,0},{3,1},{4,6},{5,7},{6,4},{7,5},{8,10},{9,11},{10,... | collective-permute-start | bytes 786440 | tf_op jit(solution)/shard_map/ppermute | solution.py:190
  151.5 19.3 %collective-permute-start.28 = (bf16[256,512]{1,0:T(8,128)(2,1)S(1)}, bf16[256,512]{1,0:T(8,128)(2,1)S(1)}, u32[]{:S(2)}, u32[]{:S(2)}) collective-permute-start(bf16[256,512]{1,0:T(8,128)(2,1)S(1)} %shard_map.73), channel_id=1, source_target_pairs={{0,8},{4,12},{8,0},{12,4},{1,9},{5,13},{9,1},{13,5},{2,10},{6,14},... | collective-permute-start | bytes 786440 | tf_op jit(solution)/shard_map/ppermute | solution.py:184
  157.1 14.8 %collective-permute-start.36 = (bf16[256,512]{1,0:T(8,128)(2,1)S(1)}, bf16[256,512]{1,0:T(8,128)(2,1)S(1)}, u32[]{:S(2)}, u32[]{:S(2)}) collective-permute-start(bf16[256,512]{1,0:T(8,128)(2,1)S(1)} %shard_map.76), channel_id=1, source_target_pairs={{0,4},{4,0},{8,12},{12,8},{1,5},{5,1},{9,13},{13,9},{2,6},{6,2},{1... | collective-permute-start | bytes 786440 | tf_op jit(solution)/shard_map/ppermute | solution.py:184
  (36 other events, 338.9 us)

commit v4 on v3

--- a/solution.py
+++ b/solution.py
@@ -40,31 +40,37 @@
     return jnp.dot(left, right, preferred_element_type=jnp.float32)
 
 
-def first_projection_kernel(at, stacked, weight, near1, near2, near, far):
+def most_projection_kernel(at, stacked, weight, near1, near2, near3, far1, far2, stream, near, far):
     half = near1.shape[1]
-    mine = weight[:, pl.ds(pl.multiple_of(at[4] * half, half), half)]
-    other = weight[:, pl.ds(pl.multiple_of((1 - at[4]) * half, half), half)]
-    near[...] = (
-        dot_of(stacked[at[0]], mine) + dot_of(stacked[at[1]], near1[...]) + dot_of(stacked[at[2]], near2[...])
-    )
-    far[...] = dot_of(stacked[at[0]], other)
-
-
-def second_projection_kernel(at, stacked, near3, far1, far2, near, far, near_out, far_out):
-    near_out[...] = near[...] + dot_of(stacked[at[3]], near3[...])
-    far_out[...] = far[...] + dot_of(stacked[at[1]], far1[...]) + dot_of(stacked[at[2]], far2[...])
-
-
-def last_projection_kernel(at, stacked, far3, near, far, stream, gain, resid, scaled):
+    mine = pl.ds(pl.multiple_of(at[4] * half, half), half)
+    other = pl.ds(pl.multiple_of((1 - at[4]) * half, half), half)
+    total = dot_of(stacked[at[0]], weight[:, mine])
+    for flip, piece in ((1, near1), (2, near2), (3, near3)):
+        total += dot_of(stacked[at[flip]], piece[...])
+    near[...] = stream[:, mine].astype(jnp.float32) + total
+    total = dot_of(stacked[at[0]], weight[:, other])
+    for flip, piece in ((1, far1), (2, far2)):
+        total += dot_of(stacked[at[flip]], piece[...])
+    far[...] = stream[:, other].astype(jnp.float32) + total
+
+
+def last_projection_kernel(at, stacked, far3, near, far, gain, resid, scaled):
     half = far3.shape[1]
-    other = far[...] + dot_of(stacked[at[3]], far3[...])
-    for side, value in ((at[4], near[...]), (1 - at[4], other)):
+    last = far[...] + dot_of(stacked[at[3]], far3[...])
+    for side, value in ((at[4], near[...]), (1 - at[4], last)):
         columns = pl.ds(pl.multiple_of(side * half, half), half)
-        kept = (stream[:, columns].astype(jnp.float32) + value).astype(jnp.bfloat16)
+        kept = value.astype(jnp.bfloat16)
         resid[:, columns] = kept
         scaled[:, columns] = (kept.astype(jnp.float32) * gain[:, columns].astype(jnp.float32)).astype(jnp.bfloat16)
 
 
+def stack_kernel(own_first, own_second, pair_first, pair_second, out):
+    tokens = own_first.shape[0]
+    for side, blocks in enumerate(((own_first, own_second), (pair_first, pair_second))):
+        for number, block in enumerate(blocks):
+            out[side, number * tokens : (number + 1) * tokens, :] = block[...]
+
+
 def mean_kernel(features, one, two, out):
     out[...] = (one[...] + two[...]) / features
 
@@ -73,57 +79,68 @@
     out[...] = 1.0 / (energy[...] + epsilon)
 
 
-def hidden_products(own, pair, others, weights, out):
-    depth = own.shape[1]
+def hidden_products(mine, others, weights, out):
+    depth = mine.shape[2]
     total = None
-    for flip, block in enumerate((own, others, pair, others)):
-        left = block[flip // 2] if flip % 2 else block[...]
+    for flip in range(4):
+        left = (others if flip % 2 else mine)[flip // 2]
         term = dot_of(left, weights[flip * depth : (flip + 1) * depth, :])
         total = term if total is None else total + term
     out[...] = jnp.square(jnp.maximum(total, 0.0)).astype(jnp.bfloat16)
 
 
-def first_hidden_kernel(place, own, pair, others, *rest):
+def first_hidden_kernel(place, mine, others, *rest):
     near, far, out, weights = rest[:4], rest[4:6], rest[6], rest[7]
     depth, half = near[0].shape
     for slot, piece in enumerate(near):
         rows = pl.ds(pl.multiple_of(place[slot] * depth, depth), depth)
         weights[rows, :half] = piece[...]
         weights[rows, half:] = far[0][...] if slot == 0 else far[1][slot - 1]
-    hidden_products(own, pair, others, weights, out)
-
-
-def second_hidden_kernel(own, pair, others, weights, out):
-    hidden_products(own, pair, others, weights, out)
-
-
-def branch_products(own, other, weights, keep, give):
+    hidden_products(mine, others, weights, out)
+
+
+def second_hidden_kernel(mine, others, weights, out):
+    hidden_products(mine, others, weights, out)
+
+
+def branch_products(place, own, other, last, weights, keep, give):
     depth = own.shape[1]
+    half = last.shape[0]
+    extra = dot_of(jnp.where(place[7] == 0, own[:, half:], other[:, half:]), last[...])
     for side, target in ((1, give), (0, keep)):
         value = dot_of(own, weights[side, :depth, :]) + dot_of(other, weights[side, depth:, :])
+        value += jnp.where(place[3] == side, extra, 0.0)
         target[...] = value.astype(target.dtype)
 
 
-def first_branch_kernel(place, own, other, *rest):
-    near, far, keep, give, weights = rest[:4], rest[4:8], rest[8], rest[9], rest[10]
-    half = near[0].shape[0]
+def place_piece(place, weights, slot, far, piece):
+    half = piece.shape[0]
+    begin = pl.multiple_of(place[4 + slot] * (2 * half) + far * half, half)
+    weights[place[slot], pl.ds(begin, half), :] = piece
+
+
+def place_kernel(place, *rest):
+    near, far, weights = rest[:4], rest[4:7], rest[7]
+    for side, pieces in enumerate((near, far)):
+        for slot, piece in enumerate(pieces):
+            place_piece(place, weights, slot, side, piece[...])
+    place_piece(place, weights, 3, 1, jnp.zeros_like(near[3]))
+
+
+def later_branch_kernel(place, own, other, last, weights, keep, give):
     tokens = keep.shape[0]
-    for slot in range(len(near)):
-        begin = pl.multiple_of(place[len(near) + slot] * (2 * half), 2 * half)
-        weights[place[slot], pl.ds(begin, half), :] = near[slot][...]
-        weights[place[slot], pl.ds(begin + half, half), :] = far[slot][...]
-    branch_products(own[tokens:, :], other[tokens:, :], weights, keep, give)
-
-
-def second_branch_kernel(own, other, weights, keep_one, give_one, keep_three, give_three):
+    branch_products(place, own[tokens:, :], other[tokens:, :], last, weights, keep, give)
+
+
+def both_branch_kernel(place, own, other, last, weights, keep_one, give_one, keep_three, give_three):
     tokens = keep_one.shape[0]
-    branch_products(own[:tokens, :], other[:tokens, :], weights, keep_one, give_one)
-    branch_products(own[tokens:, :], other[tokens:, :], weights, keep_three, give_three)
-
-
-def third_branch_kernel(own, other, weights, keep, give):
+    branch_products(place, own[:tokens, :], other[:tokens, :], last, weights, keep_one, give_one)
+    branch_products(place, own[tokens:, :], other[tokens:, :], last, weights, keep_three, give_three)
+
+
+def first_branch_kernel(place, own, other, last, weights, keep, give):
     tokens = keep.shape[0]
-    branch_products(own[:tokens, :], other[:tokens, :], weights, keep, give)
+    branch_products(place, own[:tokens, :], other[:tokens, :], last, weights, keep, give)
 
 
 def pair_sum_kernel(keep, got, out):
@@ -158,7 +175,7 @@
     )(place, whole)
 
 
-def local_call(kernel, outs, *operands, flops, scratch=(), room=8):
+def local_call(kernel, outs, *operands, flops, room=8):
     specs = [
         pl.BlockSpec(memory_space=pltpu.SMEM if x.dtype == jnp.int32 else pltpu.VMEM) for x in operands
     ]
@@ -167,7 +184,6 @@
         out_shape=outs,
         in_specs=specs,
         out_specs=jax.tree.map(lambda _: pl.BlockSpec(memory_space=pltpu.VMEM), outs),
-        scratch_shapes=scratch,
         compiler_params=pltpu.CompilerParams(vmem_limit_bytes=room << 20),
         cost_estimate=pl.CostEstimate(flops=flops, bytes_accessed=1 << 20, transcendentals=0),
     )(*operands)
@@ -199,25 +215,22 @@
     flops = 2 * tokens * width * half
     stacked = jnp.stack([mixed, *flipped])
     near, far = local_call(
-        first_projection_kernel, (sums, sums), at, stacked, out_weight, out_near[1], out_near[2], flops=3 * flops
-    )
-    near, far = local_call(
-        second_projection_kernel, (sums, sums),
-        at, stacked, out_near[3], out_far[1], out_far[2], near, far,
-        flops=3 * flops,
+        most_projection_kernel, (sums, sums),
+        at, stacked, out_weight, *(out_near[s] for s in flips), out_far[1], out_far[2], stream,
+        flops=7 * flops,
     )
     resid, scaled = local_call(
         last_projection_kernel,
         (jax.ShapeDtypeStruct((tokens, width), jnp.bfloat16),) * 2,
-        at, stacked, out_far[3], near, far, stream, norm_gain.reshape(1, width),
+        at, stacked, out_far[3], near, far, norm_gain.reshape(1, width),
         flops=flops,
     )
     widened = resid.astype(jnp.float32)
     power = jnp.sum(widened * widened, axis=1).reshape(-1, 128)
-    power += across_columns(power, 1)
+    power += across_columns(power, 2)
     small = jax.ShapeDtypeStruct(power.shape, jnp.float32)
     energy = local_call(
-        functools.partial(mean_kernel, parts * width), small, power, across_columns(power, 2), flops=1024
+        functools.partial(mean_kernel, parts * width), small, power, across_columns(power, 1), flops=1024
     )
     inverse = local_call(inverse_kernel, small, energy, flops=1024)
 
@@ -247,41 +260,43 @@
     rows = {s: along_rows(scaled, s) for s in (1, 2)}
     rows[3] = along_rows(rows[2], 1)
     pairs |= {s: across_columns(rows[s], 2) for s in flips}
-    even = jnp.concatenate([scaled, rows[2]])
-    odd = jnp.concatenate([rows[1], rows[3]])
-    even_pair = jnp.concatenate([pairs[0], pairs[2]])
-    odd_pair = jnp.concatenate([pairs[1], pairs[3]])
-    even_both = jnp.stack([even, even_pair])
-    even_others = across_columns(even_both, 1)
-    odd_others = across_columns(jnp.stack([odd, odd_pair]), 1)
+    both = jax.ShapeDtypeStruct((2, 2 * tokens, width), jnp.bfloat16)
+    even = local_call(stack_kernel, both, scaled, rows[2], pairs[0], pairs[2], flops=1024)
+    odd = local_call(stack_kernel, both, rows[1], rows[3], pairs[1], pairs[3], flops=1024)
+    even_others = across_columns(even, 1)
+    odd_others = across_columns(odd, 1)
     flops = 4 * tokens * parts * width * unit
     some = jax.ShapeDtypeStruct((2 * tokens, unit), jnp.bfloat16)
     hidden_even, up_whole = local_call(
         first_hidden_kernel,
         (some, jax.ShapeDtypeStruct((parts * width, unit), jnp.bfloat16)),
-        place, even, even_pair, even_others,
+        place, even, even_others,
         up_mine, up_near[1], up_near[2], up_near[3], up_other, up_far,
         flops=flops,
         room=14,
     )
-    hidden_odd = local_call(second_hidden_kernel, some, odd, odd_pair, odd_others, up_whole, flops=flops, room=14)
+    hidden_odd = local_call(second_hidden_kernel, some, odd, odd_others, up_whole, flops=flops, room=14)
 
     block = (tokens, width)
     pair_of = (jax.ShapeDtypeStruct(block, jnp.float32), jax.ShapeDtypeStruct(block, jnp.bfloat16))
     other_even = across_columns(hidden_even, 1)
     other_odd = across_columns(hidden_odd, 1)
-    keep_two, give_two, down_whole = local_call(
-        first_branch_kernel,
-        (*pair_of, jax.ShapeDtypeStruct((2, 2 * unit, width), jnp.bfloat16)),
-        down_place, hidden_even, other_even, *down_near, *down_far,
-        flops=flops // 2,
-        room=14,
+    whole = jax.ShapeDtypeStruct((2, 2 * unit, width), jnp.bfloat16)
+    down_most = local_call(place_kernel, whole, down_place, *down_near, *down_far[:3], flops=1024, room=14)
+    keep_two, give_two = local_call(
+        later_branch_kernel, pair_of,
+        down_place, hidden_even, other_even, down_far[3], down_most,
+        flops=flops // 2, room=14,
     )
     keep_one, give_one, keep_three, give_three = local_call(
-        second_branch_kernel, pair_of * 2, hidden_odd, other_odd, down_whole, flops=flops, room=14
+        both_branch_kernel, pair_of * 2,
+        down_place, hidden_odd, other_odd, down_far[3], down_most,
+        flops=flops, room=14,
     )
     keep_own, give_own = local_call(
-        third_branch_kernel, pair_of, hidden_even, other_even, down_whole, flops=flops // 2, room=14
+        first_branch_kernel, pair_of,
+        down_place, hidden_even, other_even, down_far[3], down_most,
+        flops=flops // 2, room=14,
     )
 
     def summed(keep, give):

time: 174 us -> 177 us (1.017)
  waiting for transfers between devices: 97.1 us -> 85.6 us
  starting transfers between devices: 45.1 us -> 55.5 us
  Pallas kernels: 14.3 us -> 18 us
  local copies, waits for them, and re-layouts: 10.4 us -> 13.6 us
  other arithmetic: 5.48 us -> 3.25 us
    ppermute x4, starting transfers between devices: 3.45 us -> 18.2 us  [gathered_tokens(): down_near.append(lax.ppermute(down_sent[number], ('fs', 'tp'), moves))]
    ppermute x8, waiting for transfers between devices: 31.9 us -> 23.5 us  [across_parts(): return lax.ppermute(value, 'grp', [(0, 1), (1, 0)])]
    pallas_call x13 -> x15, Pallas kernels: 12.8 us -> 16.5 us  [local_call(): pl.pallas_call(kernel, out_shape=outs, in_specs=specs, out_specs=jax.tree...]
    ppermute x4, waiting for transfers between devices: 3.66 us -> 0.3 us  [gathered_tokens(): down_near.append(lax.ppermute(down_sent[number], ('fs', 'tp'), moves))]
    unnamed x42 -> x50, local copies, waits for them, and re-layouts: 9.43 us -> 12.6 us
    ppermute x17, starting transfers between devices: 14 us -> 11.6 us  [across_columns(): return lax.ppermute(value, 'tp', [(i, i ^ flip) for i in range(parts)])]
    another operation x2 -> x0, other arithmetic: 2.18 us -> none  [the longest x1 1.11 us: gathered_tokens(): odd_others = across_columns(jnp.stack([odd, odd_pair]), 1)]
    ppermute x12, starting transfers between devices: 18.8 us -> 17 us  [along_rows(): return lax.ppermute(value, 'fs', [(i, i ^ flip) for i in range(parts)])]
  transfers between devices with their start and end apart: 41 -> 41, of which waited for: 21 -> 22; matrix products, arithmetic and copies ran while one was open for 4% -> 2% of each run, Pallas kernels for 8% -> 10%
where the time goes in v4:
time: 177 us; the launch traced here: 176 us
  waiting for transfers between devices  85.6 us (48%)
  starting transfers between devices  55.5 us (31%)
  Pallas kernels  18 us (10%)
  local copies, waits for them, and re-layouts  13.6 us (8%)
  other arithmetic  3.25 us (2%)
    ppermute x12, waiting for transfers between devices, along_rows(): return lax.ppermute(value, 'fs', [(i, i ^ flip) for i in range(parts)])  40.4 us
    ppermute x8, waiting for transfers between devices, across_parts(): return lax.ppermute(value, 'grp', [(0, 1), (1, 0)])  23.5 us
    ppermute x17, waiting for transfers between devices, across_columns(): return lax.ppermute(value, 'tp', [(i, i ^ flip) for i in range(parts)])  21.3 us
    ppermute x4, starting transfers between devices, gathered_tokens(): down_near.append(lax.ppermute(down_sent[number], ('fs', 'tp'), moves))  18.2 us
    ppermute x12, starting transfers between devices, along_rows(): return lax.ppermute(value, 'fs', [(i, i ^ flip) for i in range(parts)])  17 us
    pallas_call x15, Pallas kernels, local_call(): pl.pallas_call(kernel, out_shape=outs, in_specs=specs, out_specs=jax.tree...  16.5 us
    unnamed x50, local copies, waits for them, and re-layouts  12.6 us
    ppermute x17, starting transfers between devices, across_columns(): return lax.ppermute(value, 'tp', [(i, i ^ flip) for i in range(parts)])  11.6 us
  transfers between devices with their start and end apart: 41, of which 22 were waited for; matrix products, arithmetic and copies ran while one was open for 2% of the time, Pallas kernels for 10%

profile of v4, /device:TPU:0, one launch (start us, length us, event | category | flops | bytes accessed | tf_op | source)
XLA Modules:
  0.0 176.2 jit_solution(4522423208374410848)
XLA Ops:
  1.1 4.1 %collective-permute-start.3 = (bf16[512,256]{1,0:T(8,128)(2,1)S(1)}, bf16[512,256]{1,0:T(8,128)(2,1)S(1)}, u32[]{:S(2)}, u32[]{:S(2)}) collective-permute-start(bf16[512,256]{1,0:T(8,128)(2,1)S(1)} %shard_map.64), channel_id=1, source_target_pairs={{0,8},{4,12},{8,0},{12,4},{1,9},{5,13},{9,1},{13,5},{2,10},{6,14},... | collective-permute-start | bytes 786440 | tf_op jit(solution)/shard_map/ppermute | solution.py:200
  7.2 10.0 %collective-permute-done.3.near2 = bf16[512,256]{1,0:T(8,128)(2,1)S(1)} collective-permute-done((bf16[512,256]{1,0:T(8,128)(2,1)S(1)}, bf16[512,256]{1,0:T(8,128)(2,1)S(1)}, u32[]{:S(2)}, u32[]{:S(2)}) %collective-permute-start.3) | collective-permute-done | bytes 262176 | tf_op jit(solution)/shard_map/ppermute | solution.py:200
  21.4 3.3 %collective-permute-done.4.near3 = bf16[512,256]{1,0:T(8,128)(2,1)} collective-permute-done((bf16[512,256]{1,0:T(8,128)(2,1)S(1)}, bf16[512,256]{1,0:T(8,128)(2,1)}, u32[]{:S(2)}, u32[]{:S(2)}) %collective-permute-start.4) | collective-permute-done | bytes 262176 | tf_op jit(solution)/shard_map/ppermute | solution.py:200
  28.9 5.6 %collective-permute-done.8.far2 = bf16[512,256]{1,0:T(8,128)(2,1)} collective-permute-done((bf16[512,256]{1,0:T(8,128)(2,1)S(1)}, bf16[512,256]{1,0:T(8,128)(2,1)}, u32[]{:S(2)}, u32[]{:S(2)}) %collective-permute-start.8) | collective-permute-done | bytes 262176 | tf_op jit(solution)/shard_map/ppermute | solution.py:203
  36.3 3.2 %collective-permute-done.5.far3 = bf16[512,256]{1,0:T(8,128)(2,1)S(1)} collective-permute-done((bf16[512,256]{1,0:T(8,128)(2,1)}, bf16[512,256]{1,0:T(8,128)(2,1)S(1)}, u32[]{:S(2)}, u32[]{:S(2)}) %collective-permute-start.5) | collective-permute-done | bytes 262176 | tf_op jit(solution)/shard_map/ppermute | solution.py:203
  41.0 3.4 %collective-permute-start.9 = (bf16[256,512]{1,0:T(8,128)(2,1)S(1)}, bf16[256,512]{1,0:T(8,128)(2,1)S(1)}, u32[]{:S(2)}, u32[]{:S(2)}) collective-permute-start(bf16[256,512]{1,0:T(8,128)(2,1)S(1)} %get-tuple-element.31.own_first), channel_id=1, source_target_pairs={{0,8},{4,12},{8,0},{12,4},{1,9},{5,13},{9,1},{13,5},{2,10},{6,14},... | collective-permute-start | bytes 786440 | tf_op jit(solution)/shard_map/ppermute | solution.py:200
  44.4 11.8 %collective-permute-done.9.own_second = bf16[256,512]{1,0:T(8,128)(2,1)S(1)} collective-permute-done((bf16[256,512]{1,0:T(8,128)(2,1)S(1)}, bf16[256,512]{1,0:T(8,128)(2,1)S(1)}, u32[]{:S(2)}, u32[]{:S(2)}) %collective-permute-start.9) | collective-permute-done | bytes 262176 | tf_op jit(solution)/shard_map/ppermute | solution.py:200
  58.8 5.6 %collective-permute-done.30.own_second = bf16[256,512]{1,0:T(8,128)(2,1)} collective-permute-done((bf16[256,512]{1,0:T(8,128)(2,1)S(1)}, bf16[256,512]{1,0:T(8,128)(2,1)}, u32[]{:S(2)}, u32[]{:S(2)}) %collective-permute-start.30) | collective-permute-done | bytes 262176 | tf_op jit(solution)/shard_map/ppermute | solution.py:200
  68.8 2.4 %collective-permute-done.11.pair_second = bf16[256,512]{1,0:T(8,128)(2,1)} collective-permute-done((bf16[256,512]{1,0:T(8,128)(2,1)S(1)}, bf16[256,512]{1,0:T(8,128)(2,1)}, u32[]{:S(2)}, u32[]{:S(2)}) %collective-permute-start.11) | collective-permute-done | bytes 262176 | tf_op jit(solution)/shard_map/ppermute | solution.py:206
  74.3 2.4 %collective-permute-done.31.pair_first = bf16[256,512]{1,0:T(8,128)(2,1)S(1)} collective-permute-done((bf16[256,512]{1,0:T(8,128)(2,1)S(1)}, bf16[256,512]{1,0:T(8,128)(2,1)S(1)}, u32[]{:S(2)}, u32[]{:S(2)}) %collective-permute-start.31) | collective-permute-done | bytes 262176 | tf_op jit(solution)/shard_map/ppermute | solution.py:206
  77.4 3.9 %collective-permute-done.32.pair_second = bf16[256,512]{1,0:T(8,128)(2,1)} collective-permute-done((bf16[256,512]{1,0:T(8,128)(2,1)}, bf16[256,512]{1,0:T(8,128)(2,1)}, u32[]{:S(2)}, u32[]{:S(2)}) %collective-permute-start.32) | collective-permute-done | bytes 262176 | tf_op jit(solution)/shard_map/ppermute | solution.py:206
  84.3 3.8 %collective-permute-done.14.rest_2_ = bf16[512,256]{1,0:T(8,128)(2,1)S(1)} collective-permute-done((bf16[512,256]{1,0:T(8,128)(2,1)S(1)}, bf16[512,256]{1,0:T(8,128)(2,1)S(1)}, u32[]{:S(2)}, u32[]{:S(2)}) %collective-permute-start.14) | collective-permute-done | bytes 262176 | tf_op jit(solution)/shard_map/ppermute | solution.py:200
  94.3 3.2 %collective-permute-start.18 = (bf16[256,512]{1,0:T(8,128)(2,1)S(1)}, bf16[256,512]{1,0:T(8,128)(2,1)}, u32[]{:S(2)}, u32[]{:S(2)}) collective-permute-start(bf16[256,512]{1,0:T(8,128)(2,1)S(1)} %get-tuple-element.38), channel_id=1, source_target_pairs={{0,12},{1,8},{2,14},{3,10},{4,9},{5,13},{6,11},{7,15},{8,4},{9,0},... | collective-permute-start | bytes 786440 | tf_op jit(solution)/shard_map/ppermute | solution.py:252
  97.5 11.1 %collective-permute-start.21 = (bf16[256,512]{1,0:T(8,128)(2,1)S(1)}, bf16[256,512]{1,0:T(8,128)(2,1)}, u32[]{:S(2)}, u32[]{:S(2)}) collective-permute-start(bf16[256,512]{1,0:T(8,128)(2,1)S(1)} %get-tuple-element.40), channel_id=1, source_target_pairs={{0,4},{1,0},{2,6},{3,2},{4,1},{5,5},{6,3},{7,7},{8,12},{9,8},{10,1... | collective-permute-start | bytes 786440 | tf_op jit(solution)/shard_map/ppermute | solution.py:252
  108.6 3.2 %collective-permute-start.22 = (bf16[256,512]{1,0:T(8,128)(2,1)S(1)}, bf16[256,512]{1,0:T(8,128)(2,1)}, u32[]{:S(2)}, u32[]{:S(2)}) collective-permute-start(bf16[256,512]{1,0:T(8,128)(2,1)S(1)} %get-tuple-element.41), channel_id=1, source_target_pairs={{0,8},{1,12},{2,10},{3,14},{4,13},{5,9},{6,15},{7,11},{8,0},{9,4},... | collective-permute-start | bytes 786440 | tf_op jit(solution)/shard_map/ppermute | solution.py:252
  116.1 2.5 %shard_map.69 = (bf16[512,512]{1,0:T(8,128)(2,1)S(1)}, bf16[2048,512]{1,0:T(8,128)(2,1)S(1)}) custom-call(s32[4]{0:T(128)S(1)} %pad_add_fusion.place, bf16[2,512,512]{2,1,0:T(8,128)(2,1)S(1)} %shard_map.67.mine, bf16[2,512,512]{2,1,0:T(8,128)(2,1)S(1)} %copy-done.5, bf16[512,256]{1,0:T(8,128)(2,1)S(1)} %copy-done.13, ...), custom_call_target="tpu_custom_call" | custom-call | flops 1073741824 | bytes 1048576 | tf_op jit(solution)/shard_map/pallas_call | solution.py:182
  118.8 2.5 %shard_map.76.own = bf16[512,512]{1,0:T(8,128)(2,1)S(1)} custom-call(bf16[2,512,512]{2,1,0:T(8,128)(2,1)S(1)} %shard_map.75.mine, bf16[2,512,512]{2,1,0:T(8,128)(2,1)} %collective-permute-done.33.others, bf16[2048,512]{1,0:T(8,128)(2,1)S(1)} %get-tuple-element.46.weights), custom_call_target="tpu_custom_call" | custom-call | flops 1073741824 | bytes 1048576 | tf_op jit(solution)/shard_map/pallas_call | solution.py:182
  125.7 5.6 %collective-permute-done.24.rest_5_ = bf16[256,512]{1,0:T(8,128)(2,1)S(1)} collective-permute-done((bf16[256,512]{1,0:T(8,128)(2,1)}, bf16[256,512]{1,0:T(8,128)(2,1)S(1)}, u32[]{:S(2)}, u32[]{:S(2)}) %collective-permute-start.24) | collective-permute-done | bytes 262176 | tf_op jit(solution)/shard_map/ppermute | solution.py:203
  131.2 5.6 %collective-permute-done.25.rest_6_ = bf16[256,512]{1,0:T(8,128)(2,1)S(1)} collective-permute-done((bf16[256,512]{1,0:T(8,128)(2,1)}, bf16[256,512]{1,0:T(8,128)(2,1)S(1)}, u32[]{:S(2)}, u32[]{:S(2)}) %collective-permute-start.25) | collective-permute-done | bytes 262176 | tf_op jit(solution)/shard_map/ppermute | solution.py:203
  139.1 2.5 %collective-permute-done.19.last = bf16[256,512]{1,0:T(8,128)(2,1)S(1)} collective-permute-done((bf16[256,512]{1,0:T(8,128)(2,1)}, bf16[256,512]{1,0:T(8,128)(2,1)S(1)}, u32[]{:S(2)}, u32[]{:S(2)}) %collective-permute-start.19) | collective-permute-done | bytes 262176 | tf_op jit(solution)/shard_map/ppermute | solution.py:203
  144.5 2.5 %shard_map.77 = (f32[256,512]{1,0:T(8,128)S(1)}, bf16[256,512]{1,0:T(8,128)(2,1)S(1)}, f32[256,512]{1,0:T(8,128)S(1)}, bf16[256,512]{1,0:T(8,128)(2,1)S(1)}) custom-call(s32[8]{0:T(128)S(1)} %stack.123.place, bf16[512,512]{1,0:T(8,128)(2,1)S(1)} %shard_map.76.own, bf16[512,512]{1,0:T(8,128)(2,1)} %collective-permute-done.34.other, ...), custom_call_target="tpu_custom_call" | custom-call | flops 1073741824 | bytes 1048576 | tf_op jit(solution)/shard_map/pallas_call | solution.py:182
  154.4 3.4 %collective-permute-done.37.got = bf16[256,512]{1,0:T(8,128)(2,1)S(1)} collective-permute-done((bf16[256,512]{1,0:T(8,128)(2,1)S(1)}, bf16[256,512]{1,0:T(8,128)(2,1)S(1)}, u32[]{:S(2)}, u32[]{:S(2)}) %collective-permute-start.37) | collective-permute-done | bytes 262176 | tf_op jit(solution)/shard_map/ppermute | solution.py:206
  158.4 5.0 %collective-permute-done.35.got = bf16[256,512]{1,0:T(8,128)(2,1)S(1)} collective-permute-done((bf16[256,512]{1,0:T(8,128)(2,1)S(1)}, bf16[256,512]{1,0:T(8,128)(2,1)S(1)}, u32[]{:S(2)}, u32[]{:S(2)}) %collective-permute-start.35) | collective-permute-done | bytes 262176 | tf_op jit(solution)/shard_map/ppermute | solution.py:206
  170.8 4.4 %collective-permute-done.36 = bf16[256,512]{1,0:T(8,128)(2,1)S(1)} collective-permute-done((bf16[256,512]{1,0:T(8,128)(2,1)S(1)}, bf16[256,512]{1,0:T(8,128)(2,1)S(1)}, u32[]{:S(2)}, u32[]{:S(2)}) %collective-permute-start.36) | collective-permute-done | bytes 262176 | tf_op jit(solution)/shard_map/ppermute | solution.py:200
  (137 shorter events, 64.8 us)
Async XLA Ops:
  1.1 16.2 %collective-permute-start.3 = (bf16[512,256]{1,0:T(8,128)(2,1)S(1)}, bf16[512,256]{1,0:T(8,128)(2,1)S(1)}, u32[]{:S(2)}, u32[]{:S(2)}) collective-permute-start(bf16[512,256]{1,0:T(8,128)(2,1)S(1)} %shard_map.64), channel_id=1, source_target_pairs={{0,8},{4,12},{8,0},{12,4},{1,9},{5,13},{9,1},{13,5},{2,10},{6,14},... | collective-permute-start | bytes 786440 | tf_op jit(solution)/shard_map/ppermute | solution.py:200
  5.2 14.2 %collective-permute-start.6 = (bf16[512,256]{1,0:T(8,128)(2,1)S(1)}, bf16[512,256]{1,0:T(8,128)(2,1)}, u32[]{:S(2)}, u32[]{:S(2)}) collective-permute-start(bf16[512,256]{1,0:T(8,128)(2,1)S(1)} %shard_map.64), channel_id=1, source_target_pairs={{0,4},{4,0},{8,12},{12,8},{1,5},{5,1},{9,13},{13,9},{2,6},{6,2},{1... | collective-permute-start | bytes 786440 | tf_op jit(solution)/shard_map/ppermute | solution.py:200
  6.8 14.1 %collective-permute-start.2 = (bf16[256,512]{1,0:T(8,128)(2,1)}, bf16[256,512]{1,0:T(8,128)(2,1)S(1)}, u32[]{:S(2)}, u32[]{:S(2)}) collective-permute-start(bf16[256,512]{1,0:T(8,128)(2,1)} %param.7), channel_id=1, source_target_pairs={{0,3},{1,2},{2,1},{3,0},{4,7},{5,6},{6,5},{7,4},{8,11},{9,10},{10,... | collective-permute-start | bytes 786440 | tf_op jit(solution)/shard_map/ppermute | solution.py:206
  24.8 14.8 %collective-permute-start.5 = (bf16[512,256]{1,0:T(8,128)(2,1)}, bf16[512,256]{1,0:T(8,128)(2,1)S(1)}, u32[]{:S(2)}, u32[]{:S(2)}) collective-permute-start(bf16[512,256]{1,0:T(8,128)(2,1)} %collective-permute-done.4.near3), channel_id=1, source_target_pairs={{0,16},{16,0},{1,17},{17,1},{2,18},{18,2},{3,19},{19,3},{4,20},{20... | collective-permute-start | bytes 786440 | tf_op jit(solution)/shard_map/ppermute | solution.py:203
  41.0 15.2 %collective-permute-start.9 = (bf16[256,512]{1,0:T(8,128)(2,1)S(1)}, bf16[256,512]{1,0:T(8,128)(2,1)S(1)}, u32[]{:S(2)}, u32[]{:S(2)}) collective-permute-start(bf16[256,512]{1,0:T(8,128)(2,1)S(1)} %get-tuple-element.31.own_first), channel_id=1, source_target_pairs={{0,8},{4,12},{8,0},{12,4},{1,9},{5,13},{9,1},{13,5},{2,10},{6,14},... | collective-permute-start | bytes 786440 | tf_op jit(solution)/shard_map/ppermute | solution.py:200
  56.8 14.4 %collective-permute-start.11 = (bf16[256,512]{1,0:T(8,128)(2,1)S(1)}, bf16[256,512]{1,0:T(8,128)(2,1)}, u32[]{:S(2)}, u32[]{:S(2)}) collective-permute-start(bf16[256,512]{1,0:T(8,128)(2,1)S(1)} %collective-permute-done.9.own_second), channel_id=1, source_target_pairs={{0,2},{1,3},{2,0},{3,1},{4,6},{5,7},{6,4},{7,5},{8,10},{9,11},{10,... | collective-permute-start | bytes 786440 | tf_op jit(solution)/shard_map/ppermute | solution.py:206
  58.3 18.4 %collective-permute-start.31 = (bf16[256,512]{1,0:T(8,128)(2,1)S(1)}, bf16[256,512]{1,0:T(8,128)(2,1)S(1)}, u32[]{:S(2)}, u32[]{:S(2)}) collective-permute-start(bf16[256,512]{1,0:T(8,128)(2,1)S(1)} %collective-permute-done.29.own_first), channel_id=1, source_target_pairs={{0,2},{1,3},{2,0},{3,1},{4,6},{5,7},{6,4},{7,5},{8,10},{9,11},{10,... | collective-permute-start | bytes 786440 | tf_op jit(solution)/shard_map/ppermute | solution.py:206
  64.4 16.9 %collective-permute-start.32 = (bf16[256,512]{1,0:T(8,128)(2,1)}, bf16[256,512]{1,0:T(8,128)(2,1)}, u32[]{:S(2)}, u32[]{:S(2)}) collective-permute-start(bf16[256,512]{1,0:T(8,128)(2,1)} %collective-permute-done.30.own_second), channel_id=1, source_target_pairs={{0,2},{1,3},{2,0},{3,1},{4,6},{5,7},{6,4},{7,5},{8,10},{9,11},{10,... | collective-permute-start | bytes 786440 | tf_op jit(solution)/shard_map/ppermute | solution.py:206
  67.2 17.1 %collective-permute-start.13 = (bf16[512,256]{1,0:T(8,128)(2,1)S(1)}, bf16[512,256]{1,0:T(8,128)(2,1)S(1)}, u32[]{:S(2)}, u32[]{:S(2)}) collective-permute-start(bf16[512,256]{1,0:T(8,128)(2,1)S(1)} %get-tuple-element.33), channel_id=1, source_target_pairs={{0,4},{4,0},{8,12},{12,8},{1,5},{5,1},{9,13},{13,9},{2,6},{6,2},{1... | collective-permute-start | bytes 786440 | tf_op jit(solution)/shard_map/ppermute | solution.py:200
  67.5 20.6 %collective-permute-start.14 = (bf16[512,256]{1,0:T(8,128)(2,1)S(1)}, bf16[512,256]{1,0:T(8,128)(2,1)S(1)}, u32[]{:S(2)}, u32[]{:S(2)}) collective-permute-start(bf16[512,256]{1,0:T(8,128)(2,1)S(1)} %get-tuple-element.34), channel_id=1, source_target_pairs={{0,8},{4,12},{8,0},{12,4},{1,9},{5,13},{9,1},{13,5},{2,10},{6,14},... | collective-permute-start | bytes 786440 | tf_op jit(solution)/shard_map/ppermute | solution.py:200
  71.2 17.0 %collective-permute-start.15 = (bf16[512,256]{1,0:T(8,128)(2,1)S(1)}, bf16[512,256]{1,0:T(8,128)(2,1)S(1)}, u32[]{:S(2)}, u32[]{:S(2)}) collective-permute-start(bf16[512,256]{1,0:T(8,128)(2,1)S(1)} %get-tuple-element.35), channel_id=1, source_target_pairs={{0,12},{4,8},{8,4},{12,0},{1,13},{5,9},{9,5},{13,1},{2,14},{6,10},... | collective-permute-start | bytes 786440 | tf_op jit(solution)/shard_map/ppermute | solution.py:200
  77.4 34.5 %collective-permute-start.12 = (bf16[2,512,512]{2,1,0:T(8,128)(2,1)S(1)}, bf16[2,512,512]{2,1,0:T(8,128)(2,1)S(1)}, u32[]{:S(2)}, u32[]{:S(2)}) collective-permute-start(bf16[2,512,512]{2,1,0:T(8,128)(2,1)S(1)} %shard_map.67.mine), channel_id=1, source_target_pairs={{0,1},{1,0},{2,3},{3,2},{4,5},{5,4},{6,7},{7,6},{8,9},{9,8},{10,11... | collective-permute-start | bytes 3145736 | tf_op jit(solution)/shard_map/ppermute | solution.py:206
  84.2 34.4 %collective-permute-start.33 = (bf16[2,512,512]{2,1,0:T(8,128)(2,1)S(1)}, bf16[2,512,512]{2,1,0:T(8,128)(2,1)}, u32[]{:S(2)}, u32[]{:S(2)}) collective-permute-start(bf16[2,512,512]{2,1,0:T(8,128)(2,1)S(1)} %shard_map.75.mine), channel_id=1, source_target_pairs={{0,1},{1,0},{2,3},{3,2},{4,5},{5,4},{6,7},{7,6},{8,9},{9,8},{10,11... | collective-permute-start | bytes 3145736 | tf_op jit(solution)/shard_map/ppermute | solution.py:206
  89.8 18.8 %collective-permute-start.16 = (bf16[3,512,256]{2,1,0:T(8,128)(2,1)}, bf16[3,512,256]{2,1,0:T(8,128)(2,1)}, u32[]{:S(2)}, u32[]{:S(2)}) collective-permute-start(bf16[3,512,256]{2,1,0:T(8,128)(2,1)} %pad_maximum_fusion.1), channel_id=1, source_target_pairs={{0,16},{16,0},{1,17},{17,1},{2,18},{18,2},{3,19},{19,3},{4,20},{20... | collective-permute-start | bytes 2359304 | tf_op jit(solution)/shard_map/ppermute | solution.py:203
  94.3 27.0 %collective-permute-start.18 = (bf16[256,512]{1,0:T(8,128)(2,1)S(1)}, bf16[256,512]{1,0:T(8,128)(2,1)}, u32[]{:S(2)}, u32[]{:S(2)}) collective-permute-start(bf16[256,512]{1,0:T(8,128)(2,1)S(1)} %get-tuple-element.38), channel_id=1, source_target_pairs={{0,12},{1,8},{2,14},{3,10},{4,9},{5,13},{6,11},{7,15},{8,4},{9,0},... | collective-permute-start | bytes 786440 | tf_op jit(solution)/shard_map/ppermute | solution.py:252
  97.5 24.3 %collective-permute-start.21 = (bf16[256,512]{1,0:T(8,128)(2,1)S(1)}, bf16[256,512]{1,0:T(8,128)(2,1)}, u32[]{:S(2)}, u32[]{:S(2)}) collective-permute-start(bf16[256,512]{1,0:T(8,128)(2,1)S(1)} %get-tuple-element.40), channel_id=1, source_target_pairs={{0,4},{1,0},{2,6},{3,2},{4,1},{5,5},{6,3},{7,7},{8,12},{9,8},{10,1... | collective-permute-start | bytes 786440 | tf_op jit(solution)/shard_map/ppermute | solution.py:252
  108.6 14.2 %collective-permute-start.22 = (bf16[256,512]{1,0:T(8,128)(2,1)S(1)}, bf16[256,512]{1,0:T(8,128)(2,1)}, u32[]{:S(2)}, u32[]{:S(2)}) collective-permute-start(bf16[256,512]{1,0:T(8,128)(2,1)S(1)} %get-tuple-element.41), channel_id=1, source_target_pairs={{0,8},{1,12},{2,10},{3,14},{4,13},{5,9},{6,15},{7,11},{8,0},{9,4},... | collective-permute-start | bytes 786440 | tf_op jit(solution)/shard_map/ppermute | solution.py:252
  118.7 22.9 %collective-permute-start.17 = (bf16[512,512]{1,0:T(8,128)(2,1)S(1)}, bf16[512,512]{1,0:T(8,128)(2,1)S(1)}, u32[]{:S(2)}, u32[]{:S(2)}) collective-permute-start(bf16[512,512]{1,0:T(8,128)(2,1)S(1)} %get-tuple-element.37.own), channel_id=1, source_target_pairs={{0,1},{1,0},{2,3},{3,2},{4,5},{5,4},{6,7},{7,6},{8,9},{9,8},{10,11... | collective-permute-start | bytes 1572872 | tf_op jit(solution)/shard_map/ppermute | solution.py:206
  121.3 23.3 %collective-permute-start.34 = (bf16[512,512]{1,0:T(8,128)(2,1)S(1)}, bf16[512,512]{1,0:T(8,128)(2,1)}, u32[]{:S(2)}, u32[]{:S(2)}) collective-permute-start(bf16[512,512]{1,0:T(8,128)(2,1)S(1)} %shard_map.76.own), channel_id=1, source_target_pairs={{0,1},{1,0},{2,3},{3,2},{4,5},{5,4},{6,7},{7,6},{8,9},{9,8},{10,11... | collective-permute-start | bytes 1572872 | tf_op jit(solution)/shard_map/ppermute | solution.py:206
  122.8 14.0 %collective-permute-start.25 = (bf16[256,512]{1,0:T(8,128)(2,1)}, bf16[256,512]{1,0:T(8,128)(2,1)S(1)}, u32[]{:S(2)}, u32[]{:S(2)}) collective-permute-start(bf16[256,512]{1,0:T(8,128)(2,1)} %collective-permute-done.22.rest_2_), channel_id=1, source_target_pairs={{0,16},{16,0},{1,17},{17,1},{2,18},{18,2},{3,19},{19,3},{4,20},{20... | collective-permute-start | bytes 786440 | tf_op jit(solution)/shard_map/ppermute | solution.py:203
  124.6 17.0 %collective-permute-start.19 = (bf16[256,512]{1,0:T(8,128)(2,1)}, bf16[256,512]{1,0:T(8,128)(2,1)S(1)}, u32[]{:S(2)}, u32[]{:S(2)}) collective-permute-start(bf16[256,512]{1,0:T(8,128)(2,1)} %collective-permute-done.18.rest_3_), channel_id=1, source_target_pairs={{0,16},{16,0},{1,17},{17,1},{2,18},{18,2},{3,19},{19,3},{4,20},{20... | collective-permute-start | bytes 786440 | tf_op jit(solution)/shard_map/ppermute | solution.py:203
  147.6 15.8 %collective-permute-start.35 = (bf16[256,512]{1,0:T(8,128)(2,1)S(1)}, bf16[256,512]{1,0:T(8,128)(2,1)S(1)}, u32[]{:S(2)}, u32[]{:S(2)}) collective-permute-start(bf16[256,512]{1,0:T(8,128)(2,1)S(1)} %get-tuple-element.48), channel_id=1, source_target_pairs={{0,2},{1,3},{2,0},{3,1},{4,6},{5,7},{6,4},{7,5},{8,10},{9,11},{10,... | collective-permute-start | bytes 786440 | tf_op jit(solution)/shard_map/ppermute | solution.py:206
  150.5 18.9 %collective-permute-start.26 = (bf16[256,512]{1,0:T(8,128)(2,1)S(1)}, bf16[256,512]{1,0:T(8,128)(2,1)S(1)}, u32[]{:S(2)}, u32[]{:S(2)}) collective-permute-start(bf16[256,512]{1,0:T(8,128)(2,1)S(1)} %get-tuple-element.43), channel_id=1, source_target_pairs={{0,2},{1,3},{2,0},{3,1},{4,6},{5,7},{6,4},{7,5},{8,10},{9,11},{10,... | collective-permute-start | bytes 786440 | tf_op jit(solution)/shard_map/ppermute | solution.py:206
  152.2 18.6 %collective-permute-start.28 = (bf16[256,512]{1,0:T(8,128)(2,1)S(1)}, bf16[256,512]{1,0:T(8,128)(2,1)S(1)}, u32[]{:S(2)}, u32[]{:S(2)}) collective-permute-start(bf16[256,512]{1,0:T(8,128)(2,1)S(1)} %shard_map.74), channel_id=1, source_target_pairs={{0,8},{4,12},{8,0},{12,4},{1,9},{5,13},{9,1},{13,5},{2,10},{6,14},... | collective-permute-start | bytes 786440 | tf_op jit(solution)/shard_map/ppermute | solution.py:200
  (42 other events, 407.8 us)

commit v5 on v4

--- a/solution.py
+++ b/solution.py
@@ -127,9 +127,12 @@
     place_piece(place, weights, 3, 1, jnp.zeros_like(near[3]))
 
 
-def later_branch_kernel(place, own, other, last, weights, keep, give):
-    tokens = keep.shape[0]
-    branch_products(place, own[tokens:, :], other[tokens:, :], last, weights, keep, give)
+def later_branch_kernel(place, own, other, last, weights, *outs):
+    some = outs[0].shape[0]
+    begin = own.shape[0] // 2
+    for number in range(2):
+        rows = slice(begin + number * some, begin + (number + 1) * some)
+        branch_products(place, own[rows, :], other[rows, :], last, weights, *outs[2 * number : 2 * number + 2])
 
 
 def both_branch_kernel(place, own, other, last, weights, keep_one, give_one, keep_three, give_three):
@@ -283,8 +286,9 @@
     other_odd = across_columns(hidden_odd, 1)
     whole = jax.ShapeDtypeStruct((2, 2 * unit, width), jnp.bfloat16)
     down_most = local_call(place_kernel, whole, down_place, *down_near, *down_far[:3], flops=1024, room=14)
-    keep_two, give_two = local_call(
-        later_branch_kernel, pair_of,
+    half_of = tuple(jax.ShapeDtypeStruct((tokens // 2, width), x.dtype) for x in pair_of)
+    keep_two, give_two, keep_four, give_four = local_call(
+        later_branch_kernel, half_of * 2,
         down_place, hidden_even, other_even, down_far[3], down_most,
         flops=flops // 2, room=14,
     )
@@ -300,14 +304,15 @@
     )
 
     def summed(keep, give):
-        out = jax.ShapeDtypeStruct(block, jnp.bfloat16)
+        out = jax.ShapeDtypeStruct(keep.shape, jnp.bfloat16)
         return local_call(pair_sum_kernel, out, keep, across_columns(give, 2), flops=1024)
 
     two = summed(keep_two, give_two)
+    four = summed(keep_four, give_four)
     one = summed(keep_one, give_one)
     three = summed(keep_three, give_three)
     branch = keep_own + across_columns(give_own, 2)
-    branch += along_rows(two, 2)
+    branch += jnp.concatenate([along_rows(two, 2), along_rows(four, 2)])
     branch += along_rows(one, 1)
     branch += along_rows(three, 3)
     return (widened + branch * inverse.reshape(tokens, 1)).astype(jnp.bfloat16)

time: 177 us -> 184 us (1.040)
  waiting for transfers between devices: 85.6 us -> 90.2 us
  starting transfers between devices: 55.5 us -> 58.2 us
    ppermute x12 -> x13, waiting for transfers between devices: 40.4 us -> 45.5 us  [along_rows(): return lax.ppermute(value, 'fs', [(i, i ^ flip) for i in range(parts)])]
    ppermute x12 -> x13, starting transfers between devices: 17 us -> 18.7 us  [along_rows(): return lax.ppermute(value, 'fs', [(i, i ^ flip) for i in range(parts)])]
    ppermute x17 -> x18, starting transfers between devices: 11.6 us -> 12.6 us  [across_columns(): return lax.ppermute(value, 'tp', [(i, i ^ flip) for i in range(parts)])]
    ppermute x17 -> x18, waiting for transfers between devices: 21.3 us -> 20.6 us  [across_columns(): return lax.ppermute(value, 'tp', [(i, i ^ flip) for i in range(parts)])]
    pallas_call x15 -> x16, Pallas kernels: 16.5 us -> 16.5 us  [local_call(): pl.pallas_call(kernel, out_shape=outs, in_specs=specs, out_specs=jax.tree...]
  transfers between devices with their start and end apart: 41 -> 43, of which waited for: 22 -> 21; matrix products, arithmetic and copies ran while one was open for 2% -> 2% of each run, Pallas kernels for 10% -> 9%
where the time goes in v5:
time: 184 us
  waiting for transfers between devices  90.2 us (49%)
  starting transfers between devices  58.2 us (32%)
  Pallas kernels  18 us (10%)
  local copies, waits for them, and re-layouts  13.5 us (7%)
  other arithmetic  3.27 us (2%)
    ppermute x13, waiting for transfers between devices, along_rows(): return lax.ppermute(value, 'fs', [(i, i ^ flip) for i in range(parts)])  45.5 us
    ppermute x8, waiting for transfers between devices, across_parts(): return lax.ppermute(value, 'grp', [(0, 1), (1, 0)])  23.3 us
    ppermute x18, waiting for transfers between devices, across_columns(): return lax.ppermute(value, 'tp', [(i, i ^ flip) for i in range(parts)])  20.6 us
    ppermute x13, starting transfers between devices, along_rows(): return lax.ppermute(value, 'fs', [(i, i ^ flip) for i in range(parts)])  18.7 us
    ppermute x4, starting transfers between devices, gathered_tokens(): down_near.append(lax.ppermute(down_sent[number], ('fs', 'tp'), moves))  18.2 us
    pallas_call x16, Pallas kernels, local_call(): pl.pallas_call(kernel, out_shape=outs, in_specs=specs, out_specs=jax.tree...  16.5 us
    unnamed x50, local copies, waits for them, and re-layouts  12.6 us
    ppermute x18, starting transfers between devices, across_columns(): return lax.ppermute(value, 'tp', [(i, i ^ flip) for i in range(parts)])  12.6 us
  transfers between devices with their start and end apart: 43, of which 21 were waited for; matrix products, arithmetic and copies ran while one was open for 2% of the time, Pallas kernels for 9%

profile of v5, /device:TPU:0, one launch (start us, length us, event | category | flops | bytes accessed | tf_op | source)
XLA Modules:
  0.0 183.5 jit_solution(437435674118571542)
XLA Ops:
  1.1 4.1 %collective-permute-start.3 = (bf16[512,256]{1,0:T(8,128)(2,1)S(1)}, bf16[512,256]{1,0:T(8,128)(2,1)S(1)}, u32[]{:S(2)}, u32[]{:S(2)}) collective-permute-start(bf16[512,256]{1,0:T(8,128)(2,1)S(1)} %shard_map.64), channel_id=1, source_target_pairs={{0,8},{4,12},{8,0},{12,4},{1,9},{5,13},{9,1},{13,5},{2,10},{6,14},... | collective-permute-start | bytes 786440 | tf_op jit(solution)/shard_map/ppermute | solution.py:203
  7.2 10.0 %collective-permute-done.3.near2 = bf16[512,256]{1,0:T(8,128)(2,1)S(1)} collective-permute-done((bf16[512,256]{1,0:T(8,128)(2,1)S(1)}, bf16[512,256]{1,0:T(8,128)(2,1)S(1)}, u32[]{:S(2)}, u32[]{:S(2)}) %collective-permute-start.3) | collective-permute-done | bytes 262176 | tf_op jit(solution)/shard_map/ppermute | solution.py:203
  21.4 3.3 %collective-permute-done.4.near3 = bf16[512,256]{1,0:T(8,128)(2,1)} collective-permute-done((bf16[512,256]{1,0:T(8,128)(2,1)S(1)}, bf16[512,256]{1,0:T(8,128)(2,1)}, u32[]{:S(2)}, u32[]{:S(2)}) %collective-permute-start.4) | collective-permute-done | bytes 262176 | tf_op jit(solution)/shard_map/ppermute | solution.py:203
  28.9 5.6 %collective-permute-done.8.far2 = bf16[512,256]{1,0:T(8,128)(2,1)} collective-permute-done((bf16[512,256]{1,0:T(8,128)(2,1)S(1)}, bf16[512,256]{1,0:T(8,128)(2,1)}, u32[]{:S(2)}, u32[]{:S(2)}) %collective-permute-start.8) | collective-permute-done | bytes 262176 | tf_op jit(solution)/shard_map/ppermute | solution.py:206
  36.3 3.2 %collective-permute-done.5.far3 = bf16[512,256]{1,0:T(8,128)(2,1)S(1)} collective-permute-done((bf16[512,256]{1,0:T(8,128)(2,1)}, bf16[512,256]{1,0:T(8,128)(2,1)S(1)}, u32[]{:S(2)}, u32[]{:S(2)}) %collective-permute-start.5) | collective-permute-done | bytes 262176 | tf_op jit(solution)/shard_map/ppermute | solution.py:206
  41.0 3.4 %collective-permute-start.9 = (bf16[256,512]{1,0:T(8,128)(2,1)S(1)}, bf16[256,512]{1,0:T(8,128)(2,1)S(1)}, u32[]{:S(2)}, u32[]{:S(2)}) collective-permute-start(bf16[256,512]{1,0:T(8,128)(2,1)S(1)} %get-tuple-element.33.own_first), channel_id=1, source_target_pairs={{0,8},{4,12},{8,0},{12,4},{1,9},{5,13},{9,1},{13,5},{2,10},{6,14},... | collective-permute-start | bytes 786440 | tf_op jit(solution)/shard_map/ppermute | solution.py:203
  44.4 11.8 %collective-permute-done.9.own_second = bf16[256,512]{1,0:T(8,128)(2,1)S(1)} collective-permute-done((bf16[256,512]{1,0:T(8,128)(2,1)S(1)}, bf16[256,512]{1,0:T(8,128)(2,1)S(1)}, u32[]{:S(2)}, u32[]{:S(2)}) %collective-permute-start.9) | collective-permute-done | bytes 262176 | tf_op jit(solution)/shard_map/ppermute | solution.py:203
  58.8 5.6 %collective-permute-done.32.own_second = bf16[256,512]{1,0:T(8,128)(2,1)} collective-permute-done((bf16[256,512]{1,0:T(8,128)(2,1)S(1)}, bf16[256,512]{1,0:T(8,128)(2,1)}, u32[]{:S(2)}, u32[]{:S(2)}) %collective-permute-start.32) | collective-permute-done | bytes 262176 | tf_op jit(solution)/shard_map/ppermute | solution.py:203
  68.8 2.4 %collective-permute-done.11.pair_second = bf16[256,512]{1,0:T(8,128)(2,1)} collective-permute-done((bf16[256,512]{1,0:T(8,128)(2,1)S(1)}, bf16[256,512]{1,0:T(8,128)(2,1)}, u32[]{:S(2)}, u32[]{:S(2)}) %collective-permute-start.11) | collective-permute-done | bytes 262176 | tf_op jit(solution)/shard_map/ppermute | solution.py:209
  74.3 2.4 %collective-permute-done.33.pair_first = bf16[256,512]{1,0:T(8,128)(2,1)S(1)} collective-permute-done((bf16[256,512]{1,0:T(8,128)(2,1)S(1)}, bf16[256,512]{1,0:T(8,128)(2,1)S(1)}, u32[]{:S(2)}, u32[]{:S(2)}) %collective-permute-start.33) | collective-permute-done | bytes 262176 | tf_op jit(solution)/shard_map/ppermute | solution.py:209
  77.4 3.8 %collective-permute-done.34.pair_second = bf16[256,512]{1,0:T(8,128)(2,1)} collective-permute-done((bf16[256,512]{1,0:T(8,128)(2,1)}, bf16[256,512]{1,0:T(8,128)(2,1)}, u32[]{:S(2)}, u32[]{:S(2)}) %collective-permute-start.34) | collective-permute-done | bytes 262176 | tf_op jit(solution)/shard_map/ppermute | solution.py:209
  84.3 3.8 %collective-permute-done.14.rest_2_ = bf16[512,256]{1,0:T(8,128)(2,1)S(1)} collective-permute-done((bf16[512,256]{1,0:T(8,128)(2,1)S(1)}, bf16[512,256]{1,0:T(8,128)(2,1)S(1)}, u32[]{:S(2)}, u32[]{:S(2)}) %collective-permute-start.14) | collective-permute-done | bytes 262176 | tf_op jit(solution)/shard_map/ppermute | solution.py:203
  94.3 3.2 %collective-permute-start.18 = (bf16[256,512]{1,0:T(8,128)(2,1)S(1)}, bf16[256,512]{1,0:T(8,128)(2,1)}, u32[]{:S(2)}, u32[]{:S(2)}) collective-permute-start(bf16[256,512]{1,0:T(8,128)(2,1)S(1)} %get-tuple-element.40), channel_id=1, source_target_pairs={{0,12},{1,8},{2,14},{3,10},{4,9},{5,13},{6,11},{7,15},{8,4},{9,0},... | collective-permute-start | bytes 786440 | tf_op jit(solution)/shard_map/ppermute | solution.py:255
  97.6 11.1 %collective-permute-start.21 = (bf16[256,512]{1,0:T(8,128)(2,1)S(1)}, bf16[256,512]{1,0:T(8,128)(2,1)}, u32[]{:S(2)}, u32[]{:S(2)}) collective-permute-start(bf16[256,512]{1,0:T(8,128)(2,1)S(1)} %get-tuple-element.42), channel_id=1, source_target_pairs={{0,4},{1,0},{2,6},{3,2},{4,1},{5,5},{6,3},{7,7},{8,12},{9,8},{10,1... | collective-permute-start | bytes 786440 | tf_op jit(solution)/shard_map/ppermute | solution.py:255
  108.7 3.2 %collective-permute-start.22 = (bf16[256,512]{1,0:T(8,128)(2,1)S(1)}, bf16[256,512]{1,0:T(8,128)(2,1)}, u32[]{:S(2)}, u32[]{:S(2)}) collective-permute-start(bf16[256,512]{1,0:T(8,128)(2,1)S(1)} %get-tuple-element.43), channel_id=1, source_target_pairs={{0,8},{1,12},{2,10},{3,14},{4,13},{5,9},{6,15},{7,11},{8,0},{9,4},... | collective-permute-start | bytes 786440 | tf_op jit(solution)/shard_map/ppermute | solution.py:255
  116.1 2.5 %shard_map.69 = (bf16[512,512]{1,0:T(8,128)(2,1)S(1)}, bf16[2048,512]{1,0:T(8,128)(2,1)S(1)}) custom-call(s32[4]{0:T(128)S(1)} %pad_add_fusion.place, bf16[2,512,512]{2,1,0:T(8,128)(2,1)S(1)} %shard_map.67.mine, bf16[2,512,512]{2,1,0:T(8,128)(2,1)S(1)} %copy-done.5, bf16[512,256]{1,0:T(8,128)(2,1)S(1)} %copy-done.13, ...), custom_call_target="tpu_custom_call" | custom-call | flops 1073741824 | bytes 1048576 | tf_op jit(solution)/shard_map/pallas_call | solution.py:185
  118.7 2.5 %shard_map.77.own = bf16[512,512]{1,0:T(8,128)(2,1)S(1)} custom-call(bf16[2,512,512]{2,1,0:T(8,128)(2,1)S(1)} %shard_map.76.mine, bf16[2,512,512]{2,1,0:T(8,128)(2,1)} %collective-permute-done.35.others, bf16[2048,512]{1,0:T(8,128)(2,1)S(1)} %get-tuple-element.50.weights), custom_call_target="tpu_custom_call" | custom-call | flops 1073741824 | bytes 1048576 | tf_op jit(solution)/shard_map/pallas_call | solution.py:185
  125.7 5.1 %collective-permute-done.24.rest_5_ = bf16[256,512]{1,0:T(8,128)(2,1)S(1)} collective-permute-done((bf16[256,512]{1,0:T(8,128)(2,1)}, bf16[256,512]{1,0:T(8,128)(2,1)S(1)}, u32[]{:S(2)}, u32[]{:S(2)}) %collective-permute-start.24) | collective-permute-done | bytes 262176 | tf_op jit(solution)/shard_map/ppermute | solution.py:206
  130.8 5.6 %collective-permute-done.25.rest_6_ = bf16[256,512]{1,0:T(8,128)(2,1)S(1)} collective-permute-done((bf16[256,512]{1,0:T(8,128)(2,1)}, bf16[256,512]{1,0:T(8,128)(2,1)S(1)}, u32[]{:S(2)}, u32[]{:S(2)}) %collective-permute-start.25) | collective-permute-done | bytes 262176 | tf_op jit(solution)/shard_map/ppermute | solution.py:206
  138.6 2.8 %collective-permute-done.19.last = bf16[256,512]{1,0:T(8,128)(2,1)S(1)} collective-permute-done((bf16[256,512]{1,0:T(8,128)(2,1)}, bf16[256,512]{1,0:T(8,128)(2,1)S(1)}, u32[]{:S(2)}, u32[]{:S(2)}) %collective-permute-start.19) | collective-permute-done | bytes 262176 | tf_op jit(solution)/shard_map/ppermute | solution.py:206
  141.5 2.5 %shard_map.78 = (f32[256,512]{1,0:T(8,128)S(1)}, bf16[256,512]{1,0:T(8,128)(2,1)S(1)}, f32[256,512]{1,0:T(8,128)S(1)}, bf16[256,512]{1,0:T(8,128)(2,1)S(1)}) custom-call(s32[8]{0:T(128)S(1)} %stack.123.place, bf16[512,512]{1,0:T(8,128)(2,1)S(1)} %shard_map.77.own, bf16[512,512]{1,0:T(8,128)(2,1)} %collective-permute-done.36.other, ...), custom_call_target="tpu_custom_call" | custom-call | flops 1073741824 | bytes 1048576 | tf_op jit(solution)/shard_map/pallas_call | solution.py:185
  154.8 4.0 %collective-permute-done.37.got = bf16[256,512]{1,0:T(8,128)(2,1)S(1)} collective-permute-done((bf16[256,512]{1,0:T(8,128)(2,1)S(1)}, bf16[256,512]{1,0:T(8,128)(2,1)S(1)}, u32[]{:S(2)}, u32[]{:S(2)}) %collective-permute-start.37) | collective-permute-done | bytes 262176 | tf_op jit(solution)/shard_map/ppermute | solution.py:209
  161.3 6.0 %collective-permute-done.29.got = bf16[128,512]{1,0:T(8,128)(2,1)S(1)} collective-permute-done((bf16[128,512]{1,0:T(8,128)(2,1)S(1)}, bf16[128,512]{1,0:T(8,128)(2,1)S(1)}, u32[]{:S(2)}, u32[]{:S(2)}) %collective-permute-start.29) | collective-permute-done | bytes 131104 | tf_op jit(solution)/shard_map/ppermute | solution.py:209
  171.7 8.6 %collective-permute-done.30 = bf16[128,512]{1,0:T(8,128)(2,1)S(1)} collective-permute-done((bf16[128,512]{1,0:T(8,128)(2,1)S(1)}, bf16[128,512]{1,0:T(8,128)(2,1)S(1)}, u32[]{:S(2)}, u32[]{:S(2)}) %collective-permute-start.30) | collective-permute-done | bytes 131104 | tf_op jit(solution)/shard_map/ppermute | solution.py:203
  (142 shorter events, 66.5 us)
Async XLA Ops:
  1.1 16.2 %collective-permute-start.3 = (bf16[512,256]{1,0:T(8,128)(2,1)S(1)}, bf16[512,256]{1,0:T(8,128)(2,1)S(1)}, u32[]{:S(2)}, u32[]{:S(2)}) collective-permute-start(bf16[512,256]{1,0:T(8,128)(2,1)S(1)} %shard_map.64), channel_id=1, source_target_pairs={{0,8},{4,12},{8,0},{12,4},{1,9},{5,13},{9,1},{13,5},{2,10},{6,14},... | collective-permute-start | bytes 786440 | tf_op jit(solution)/shard_map/ppermute | solution.py:203
  5.2 14.2 %collective-permute-start.6 = (bf16[512,256]{1,0:T(8,128)(2,1)S(1)}, bf16[512,256]{1,0:T(8,128)(2,1)}, u32[]{:S(2)}, u32[]{:S(2)}) collective-permute-start(bf16[512,256]{1,0:T(8,128)(2,1)S(1)} %shard_map.64), channel_id=1, source_target_pairs={{0,4},{4,0},{8,12},{12,8},{1,5},{5,1},{9,13},{13,9},{2,6},{6,2},{1... | collective-permute-start | bytes 786440 | tf_op jit(solution)/shard_map/ppermute | solution.py:203
  24.8 14.8 %collective-permute-start.5 = (bf16[512,256]{1,0:T(8,128)(2,1)}, bf16[512,256]{1,0:T(8,128)(2,1)S(1)}, u32[]{:S(2)}, u32[]{:S(2)}) collective-permute-start(bf16[512,256]{1,0:T(8,128)(2,1)} %collective-permute-done.4.near3), channel_id=1, source_target_pairs={{0,16},{16,0},{1,17},{17,1},{2,18},{18,2},{3,19},{19,3},{4,20},{20... | collective-permute-start | bytes 786440 | tf_op jit(solution)/shard_map/ppermute | solution.py:206
  41.0 15.2 %collective-permute-start.9 = (bf16[256,512]{1,0:T(8,128)(2,1)S(1)}, bf16[256,512]{1,0:T(8,128)(2,1)S(1)}, u32[]{:S(2)}, u32[]{:S(2)}) collective-permute-start(bf16[256,512]{1,0:T(8,128)(2,1)S(1)} %get-tuple-element.33.own_first), channel_id=1, source_target_pairs={{0,8},{4,12},{8,0},{12,4},{1,9},{5,13},{9,1},{13,5},{2,10},{6,14},... | collective-permute-start | bytes 786440 | tf_op jit(solution)/shard_map/ppermute | solution.py:203
  56.8 14.4 %collective-permute-start.11 = (bf16[256,512]{1,0:T(8,128)(2,1)S(1)}, bf16[256,512]{1,0:T(8,128)(2,1)}, u32[]{:S(2)}, u32[]{:S(2)}) collective-permute-start(bf16[256,512]{1,0:T(8,128)(2,1)S(1)} %collective-permute-done.9.own_second), channel_id=1, source_target_pairs={{0,2},{1,3},{2,0},{3,1},{4,6},{5,7},{6,4},{7,5},{8,10},{9,11},{10,... | collective-permute-start | bytes 786440 | tf_op jit(solution)/shard_map/ppermute | solution.py:209
  58.3 18.4 %collective-permute-start.33 = (bf16[256,512]{1,0:T(8,128)(2,1)S(1)}, bf16[256,512]{1,0:T(8,128)(2,1)S(1)}, u32[]{:S(2)}, u32[]{:S(2)}) collective-permute-start(bf16[256,512]{1,0:T(8,128)(2,1)S(1)} %collective-permute-done.31.own_first), channel_id=1, source_target_pairs={{0,2},{1,3},{2,0},{3,1},{4,6},{5,7},{6,4},{7,5},{8,10},{9,11},{10,... | collective-permute-start | bytes 786440 | tf_op jit(solution)/shard_map/ppermute | solution.py:209
  64.4 16.9 %collective-permute-start.34 = (bf16[256,512]{1,0:T(8,128)(2,1)}, bf16[256,512]{1,0:T(8,128)(2,1)}, u32[]{:S(2)}, u32[]{:S(2)}) collective-permute-start(bf16[256,512]{1,0:T(8,128)(2,1)} %collective-permute-done.32.own_second), channel_id=1, source_target_pairs={{0,2},{1,3},{2,0},{3,1},{4,6},{5,7},{6,4},{7,5},{8,10},{9,11},{10,... | collective-permute-start | bytes 786440 | tf_op jit(solution)/shard_map/ppermute | solution.py:209
  67.2 17.1 %collective-permute-start.13 = (bf16[512,256]{1,0:T(8,128)(2,1)S(1)}, bf16[512,256]{1,0:T(8,128)(2,1)S(1)}, u32[]{:S(2)}, u32[]{:S(2)}) collective-permute-start(bf16[512,256]{1,0:T(8,128)(2,1)S(1)} %get-tuple-element.35), channel_id=1, source_target_pairs={{0,4},{4,0},{8,12},{12,8},{1,5},{5,1},{9,13},{13,9},{2,6},{6,2},{1... | collective-permute-start | bytes 786440 | tf_op jit(solution)/shard_map/ppermute | solution.py:203
  67.5 20.6 %collective-permute-start.14 = (bf16[512,256]{1,0:T(8,128)(2,1)S(1)}, bf16[512,256]{1,0:T(8,128)(2,1)S(1)}, u32[]{:S(2)}, u32[]{:S(2)}) collective-permute-start(bf16[512,256]{1,0:T(8,128)(2,1)S(1)} %get-tuple-element.36), channel_id=1, source_target_pairs={{0,8},{4,12},{8,0},{12,4},{1,9},{5,13},{9,1},{13,5},{2,10},{6,14},... | collective-permute-start | bytes 786440 | tf_op jit(solution)/shard_map/ppermute | solution.py:203
  71.2 17.0 %collective-permute-start.15 = (bf16[512,256]{1,0:T(8,128)(2,1)S(1)}, bf16[512,256]{1,0:T(8,128)(2,1)S(1)}, u32[]{:S(2)}, u32[]{:S(2)}) collective-permute-start(bf16[512,256]{1,0:T(8,128)(2,1)S(1)} %get-tuple-element.37), channel_id=1, source_target_pairs={{0,12},{4,8},{8,4},{12,0},{1,13},{5,9},{9,5},{13,1},{2,14},{6,10},... | collective-permute-start | bytes 786440 | tf_op jit(solution)/shard_map/ppermute | solution.py:203
  77.4 34.5 %collective-permute-start.12 = (bf16[2,512,512]{2,1,0:T(8,128)(2,1)S(1)}, bf16[2,512,512]{2,1,0:T(8,128)(2,1)S(1)}, u32[]{:S(2)}, u32[]{:S(2)}) collective-permute-start(bf16[2,512,512]{2,1,0:T(8,128)(2,1)S(1)} %shard_map.67.mine), channel_id=1, source_target_pairs={{0,1},{1,0},{2,3},{3,2},{4,5},{5,4},{6,7},{7,6},{8,9},{9,8},{10,11... | collective-permute-start | bytes 3145736 | tf_op jit(solution)/shard_map/ppermute | solution.py:209
  84.2 34.5 %collective-permute-start.35 = (bf16[2,512,512]{2,1,0:T(8,128)(2,1)S(1)}, bf16[2,512,512]{2,1,0:T(8,128)(2,1)}, u32[]{:S(2)}, u32[]{:S(2)}) collective-permute-start(bf16[2,512,512]{2,1,0:T(8,128)(2,1)S(1)} %shard_map.76.mine), channel_id=1, source_target_pairs={{0,1},{1,0},{2,3},{3,2},{4,5},{5,4},{6,7},{7,6},{8,9},{9,8},{10,11... | collective-permute-start | bytes 3145736 | tf_op jit(solution)/shard_map/ppermute | solution.py:209
  89.8 18.8 %collective-permute-start.16 = (bf16[3,512,256]{2,1,0:T(8,128)(2,1)}, bf16[3,512,256]{2,1,0:T(8,128)(2,1)}, u32[]{:S(2)}, u32[]{:S(2)}) collective-permute-start(bf16[3,512,256]{2,1,0:T(8,128)(2,1)} %pad_maximum_fusion.1), channel_id=1, source_target_pairs={{0,16},{16,0},{1,17},{17,1},{2,18},{18,2},{3,19},{19,3},{4,20},{20... | collective-permute-start | bytes 2359304 | tf_op jit(solution)/shard_map/ppermute | solution.py:206
  94.3 29.5 %collective-permute-start.18 = (bf16[256,512]{1,0:T(8,128)(2,1)S(1)}, bf16[256,512]{1,0:T(8,128)(2,1)}, u32[]{:S(2)}, u32[]{:S(2)}) collective-permute-start(bf16[256,512]{1,0:T(8,128)(2,1)S(1)} %get-tuple-element.40), channel_id=1, source_target_pairs={{0,12},{1,8},{2,14},{3,10},{4,9},{5,13},{6,11},{7,15},{8,4},{9,0},... | collective-permute-start | bytes 786440 | tf_op jit(solution)/shard_map/ppermute | solution.py:255
  97.6 23.7 %collective-permute-start.21 = (bf16[256,512]{1,0:T(8,128)(2,1)S(1)}, bf16[256,512]{1,0:T(8,128)(2,1)}, u32[]{:S(2)}, u32[]{:S(2)}) collective-permute-start(bf16[256,512]{1,0:T(8,128)(2,1)S(1)} %get-tuple-element.42), channel_id=1, source_target_pairs={{0,4},{1,0},{2,6},{3,2},{4,1},{5,5},{6,3},{7,7},{8,12},{9,8},{10,1... | collective-permute-start | bytes 786440 | tf_op jit(solution)/shard_map/ppermute | solution.py:255
  108.7 14.2 %collective-permute-start.22 = (bf16[256,512]{1,0:T(8,128)(2,1)S(1)}, bf16[256,512]{1,0:T(8,128)(2,1)}, u32[]{:S(2)}, u32[]{:S(2)}) collective-permute-start(bf16[256,512]{1,0:T(8,128)(2,1)S(1)} %get-tuple-element.43), channel_id=1, source_target_pairs={{0,8},{1,12},{2,10},{3,14},{4,13},{5,9},{6,15},{7,11},{8,0},{9,4},... | collective-permute-start | bytes 786440 | tf_op jit(solution)/shard_map/ppermute | solution.py:255
  121.2 20.2 %collective-permute-start.36 = (bf16[512,512]{1,0:T(8,128)(2,1)S(1)}, bf16[512,512]{1,0:T(8,128)(2,1)}, u32[]{:S(2)}, u32[]{:S(2)}) collective-permute-start(bf16[512,512]{1,0:T(8,128)(2,1)S(1)} %shard_map.77.own), channel_id=1, source_target_pairs={{0,1},{1,0},{2,3},{3,2},{4,5},{5,4},{6,7},{7,6},{8,9},{9,8},{10,11... | collective-permute-start | bytes 1572872 | tf_op jit(solution)/shard_map/ppermute | solution.py:209
  123.8 24.0 %collective-permute-start.17 = (bf16[512,512]{1,0:T(8,128)(2,1)S(1)}, bf16[512,512]{1,0:T(8,128)(2,1)S(1)}, u32[]{:S(2)}, u32[]{:S(2)}) collective-permute-start(bf16[512,512]{1,0:T(8,128)(2,1)S(1)} %get-tuple-element.39.own), channel_id=1, source_target_pairs={{0,1},{1,0},{2,3},{3,2},{4,5},{5,4},{6,7},{7,6},{8,9},{9,8},{10,11... | collective-permute-start | bytes 1572872 | tf_op jit(solution)/shard_map/ppermute | solution.py:209
  124.5 16.9 %collective-permute-start.19 = (bf16[256,512]{1,0:T(8,128)(2,1)}, bf16[256,512]{1,0:T(8,128)(2,1)S(1)}, u32[]{:S(2)}, u32[]{:S(2)}) collective-permute-start(bf16[256,512]{1,0:T(8,128)(2,1)} %collective-permute-done.18.rest_3_), channel_id=1, source_target_pairs={{0,16},{16,0},{1,17},{17,1},{2,18},{18,2},{3,19},{19,3},{4,20},{20... | collective-permute-start | bytes 786440 | tf_op jit(solution)/shard_map/ppermute | solution.py:206
  149.1 22.6 %collective-permute-start.26 = (bf16[256,512]{1,0:T(8,128)(2,1)S(1)}, bf16[256,512]{1,0:T(8,128)(2,1)S(1)}, u32[]{:S(2)}, u32[]{:S(2)}) collective-permute-start(bf16[256,512]{1,0:T(8,128)(2,1)S(1)} %get-tuple-element.45), channel_id=1, source_target_pairs={{0,2},{1,3},{2,0},{3,1},{4,6},{5,7},{6,4},{7,5},{8,10},{9,11},{10,... | collective-permute-start | bytes 786440 | tf_op jit(solution)/shard_map/ppermute | solution.py:209
  151.0 16.2 %collective-permute-start.29 = (bf16[128,512]{1,0:T(8,128)(2,1)S(1)}, bf16[128,512]{1,0:T(8,128)(2,1)S(1)}, u32[]{:S(2)}, u32[]{:S(2)}) collective-permute-start(bf16[128,512]{1,0:T(8,128)(2,1)S(1)} %get-tuple-element.49), channel_id=1, source_target_pairs={{0,2},{1,3},{2,0},{3,1},{4,6},{5,7},{6,4},{7,5},{8,10},{9,11},{10,... | collective-permute-start | bytes 393224 | tf_op jit(solution)/shard_map/ppermute | solution.py:209
  153.2 15.5 %collective-permute-start.27 = (bf16[128,512]{1,0:T(8,128)(2,1)S(1)}, bf16[128,512]{1,0:T(8,128)(2,1)S(1)}, u32[]{:S(2)}, u32[]{:S(2)}) collective-permute-start(bf16[128,512]{1,0:T(8,128)(2,1)S(1)} %get-tuple-element.47), channel_id=1, source_target_pairs={{0,2},{1,3},{2,0},{3,1},{4,6},{5,7},{6,4},{7,5},{8,10},{9,11},{10,... | collective-permute-start | bytes 393224 | tf_op jit(solution)/shard_map/ppermute | solution.py:209
  158.8 23.8 %collective-permute-start.40 = (bf16[256,512]{1,0:T(8,128)(2,1)S(1)}, bf16[256,512]{1,0:T(8,128)(2,1)S(1)}, u32[]{:S(2)}, u32[]{:S(2)}) collective-permute-start(bf16[256,512]{1,0:T(8,128)(2,1)S(1)} %shard_map.80), channel_id=1, source_target_pairs={{0,12},{4,8},{8,4},{12,0},{1,13},{5,9},{9,5},{13,1},{2,14},{6,10},... | collective-permute-start | bytes 786440 | tf_op jit(solution)/shard_map/ppermute | solution.py:203
  159.4 23.2 %collective-permute-start.38 = (bf16[256,512]{1,0:T(8,128)(2,1)S(1)}, bf16[256,512]{1,0:T(8,128)(2,1)S(1)}, u32[]{:S(2)}, u32[]{:S(2)}) collective-permute-start(bf16[256,512]{1,0:T(8,128)(2,1)S(1)} %shard_map.79), channel_id=1, source_target_pairs={{0,4},{4,0},{8,12},{12,8},{1,5},{5,1},{9,13},{13,9},{2,6},{6,2},{1... | collective-permute-start | bytes 786440 | tf_op jit(solution)/shard_map/ppermute | solution.py:203
  (44 other events, 441.7 us)
